TPU v7x, 512 devices: a whole 4x4x16 slice. The times are simulated.
512 devices in a mesh: sp: 128 (over z, x, core), tp: 4 (over y).
Axes of the slice: x: 4, y: 4, z: 16, core: 2. Of those that a mesh axis runs over, the one named last changes fastest.
Arguments:
- tokens: bfloat16 [65536, 2048], P(('sp', 'tp')), may hold values from -6 to 6
- norm_gain: float32 [2048], replicated, may hold values from 0.1 to 1.9
- pool_in_weight: bfloat16 [2048, 1024], P('sp', 'tp'), may hold values from -0.125 to 0.125
- query_weight: bfloat16 [2048, 1024], P('sp', 'tp'), may hold values from -0.125 to 0.125
- forget_weight: bfloat16 [2048, 1024], P('sp', 'tp'), may hold values from -0.125 to 0.125
- input_weight: bfloat16 [2048, 1024], P('sp', 'tp'), may hold values from -0.125 to 0.125
- forget_gap: float32 [1024], P('tp'), may hold values from 0 to 0.02
- decay_shift: float32 [8, 65536], P('tp', 'sp'), may hold values from -0.42 to 0
- out_gain: float32 [128], replicated, may hold values from 0.1 to 1.9
- pool_out_weight: bfloat16 [1024, 2048], P('tp', 'sp'), may hold values from -0.53033009 to 0.53033009
- recur_out_weight: bfloat16 [1024, 2048], P('tp', 'sp'), may hold values from -0.53033009 to 0.53033009
Outputs:
- mixed_out: bfloat16 [65536, 2048], P(('sp', 'tp'))
All inputs are finite; a program needn't handle non-finite values.
Results may differ from a plain program's by a relative error of at most 0.014.
Values may be sent and summed in bfloat16 or wider, within the bound.
No kernel may reach another device: no remote copies, remote signals or barrier semaphores. Data moves between devices by JAX's collectives and lax.ppermute only.
A program may use at most 64 MiB of HBM per device.

v0:
```python
import jax
import jax.numpy as jnp
from jax import lax
from jax.sharding import Mesh
from jax.sharding import PartitionSpec as P

GROUPS = 4
RDIM = 128
SPAN = 64
SP = ("sp_0", "sp_1", "sp_2")
SP_TP = ("sp_0", "sp_1", "sp_2", "tp")


EPSILON = 1e-06
EXACT_MATMUL = lax.Precision.HIGHEST


def laid_out(parts, dim):
    dims = list(parts.shape[1:])
    dims[dim] *= parts.shape[0]
    return jnp.moveaxis(parts, 0, dim).reshape(dims)


def gather_in_order(x, axes, turns):
    parts = x
    for k in turns:
        parts = lax.all_gather(parts, axes[k])
    done = turns[::-1]
    back = [done.index(k) for k in range(len(axes))]
    parts = parts.transpose(*back, *range(len(axes), parts.ndim))
    return parts.reshape(-1, *x.shape)


def gathered_by_axis(x, axes, turns, dim):
    return laid_out(gather_in_order(x, axes, turns), dim)


def sent_to_all(x, axis):
    copies = jnp.broadcast_to(x, (lax.axis_size(axis), *x.shape))
    return lax.all_to_all(copies, axis, split_axis=0, concat_axis=0, tiled=True)


def gathered_copies(x, axis, dim):
    return laid_out(sent_to_all(x, axis), dim)


def passed_along(block, axis, distance):
    devices = range(lax.axis_size(axis))
    route = [(i - distance, i) for i in devices if i - distance in devices]
    return lax.ppermute(block, axis, route)


def neutral_like(x, identity):
    return jax.tree.map(
        lambda part, zero: jnp.zeros_like(part) + jnp.asarray(zero, part.dtype), x, identity
    )


def entering(x, axes, combine, identity):
    before = start = neutral_like(x, identity)
    subtotal = x
    for axis in reversed(axes):
        devices, index = (lax.axis_size(axis), lax.axis_index(axis))
        pieces = jax.tree.map(lambda part: lax.all_gather(part, axis), subtotal)
        inside, subtotal = (start, start)
        for k in range(devices):
            passed = k < index
            subtotal = combine(subtotal, jax.tree.map(lambda part: part[k], pieces))
            inside = jax.tree.map(lambda new, old: jnp.where(passed, new, old), subtotal, inside)
        before = combine(inside, before)
    return before


def whole_of(x, axes, dim):
    far, near = axes
    parts = sent_to_all(sent_to_all(x, far), near)
    return laid_out(parts.swapaxes(0, 1).reshape(-1, *x.shape), dim)


def side_by_side(arrays, axis, dim, along):
    both = jnp.concatenate(arrays, axis=along)
    out, at, outs = (whole_of(both, axis, dim), 0, [])
    for a in arrays:
        outs.append(lax.slice_in_dim(out, at, at + a.shape[along], axis=along))
        at += a.shape[along]
    return tuple(outs)


def split_up(x, dim, devices):
    before, after = (x.shape[:dim], x.shape[dim + 1 :])
    return jnp.moveaxis(x.reshape(*before, devices, -1, *after), dim, 0)


def sum_at_owner(x, axis, dim):
    devices = lax.axis_size(axis)
    parts = lax.all_to_all(split_up(x, dim, devices), axis, 0, 0, tiled=True)
    return jnp.sum(parts.astype(jnp.float32), axis=0)


def window_sums(padded, levels, reach):
    length = padded.shape[0] - reach
    results = []
    running = padded
    for level in range(levels):
        width = 2**level
        running = running[width:] + running[:-width]
        offset = reach + 1 - 2 * width
        results.append(lax.slice_in_dim(running, offset, offset + length, axis=0))
    return results


def chain(earlier, later):
    return (earlier[0] * later[0], later[0][:, :, None] * earlier[1] + later[1])


def to_blocks(tensor, block_count, head_count):
    return tensor.reshape(block_count, SPAN, head_count, RDIM).transpose(0, 2, 1, 3)


def local(
    tokens,
    norm_gain,
    pool_in_weight,
    query_weight,
    forget_weight,
    input_weight,
    forget_gap,
    decay_shift,
    out_gain,
    pool_out_weight,
    recur_out_weight,
):
    pool_cols = pool_in_weight.shape[1]
    recur_cols = query_weight.shape[1]
    local_in = jnp.concatenate([pool_in_weight, query_weight, forget_weight, input_weight], axis=1)
    whole_in = gathered_by_axis(local_in, SP, (1, 0, 2), 0)
    floats = tokens.astype(jnp.float32)
    scale = lax.rsqrt(jnp.mean(floats * floats, axis=-1, keepdims=True) + EPSILON)
    normed = (floats * scale * norm_gain).astype(jnp.bfloat16)
    pool_weight = whole_in[:, :pool_cols]
    recur_weight = whole_in[:, pool_cols:]
    pooled_in = jnp.dot(
        gathered_copies(normed, "tp", 0), pool_weight, preferred_element_type=jnp.float32
    ).astype(jnp.bfloat16)
    recur_in = jnp.dot(
        gathered_copies(normed, "tp", 0), recur_weight, preferred_element_type=jnp.float32
    ).astype(jnp.bfloat16)
    query = recur_in[:, :recur_cols].astype(jnp.float32)
    forget_pre = recur_in[:, recur_cols : 2 * recur_cols].astype(jnp.float32)
    values = recur_in[:, 2 * recur_cols :].astype(jnp.float32)
    row_count = pooled_in.shape[0]
    head_count = recur_cols // RDIM
    block_count = row_count // SPAN
    gate_pre = forget_pre.reshape(row_count, head_count, RDIM)
    opened = forget_gap.reshape(head_count, RDIM) * jax.nn.sigmoid(-gate_pre)
    log_decay = jnp.log1p(-opened) + decay_shift.T[:, :, None]
    query_blocks = to_blocks(query, block_count, head_count)
    decay_blocks = to_blocks(log_decay, block_count, head_count)
    key_blocks = to_blocks(opened, block_count, head_count)
    value_blocks = to_blocks(values, block_count, head_count)
    causal = jnp.tril(jnp.ones((SPAN, SPAN), jnp.bool_))
    inner_block_output = jnp.cumsum(decay_blocks, axis=2)
    block_decay_total = inner_block_output[:, :, -1, :]
    decayed_query = query_blocks * jnp.exp(inner_block_output)
    scores = jnp.einsum(
        "bhtk,bhsk->bhts",
        decayed_query,
        key_blocks * jnp.exp(-inner_block_output),
        precision=EXACT_MATMUL,
    )
    scores = jnp.where(causal, scores, 0.0)
    received_output = jnp.einsum("bhts,bhsv->bhtv", scores, value_blocks, precision=EXACT_MATMUL)
    growth_factor = jnp.einsum(
        "bhsk,bhsv->bhkv",
        key_blocks * jnp.exp(block_decay_total[:, :, None, :] - inner_block_output),
        value_blocks,
        precision=EXACT_MATMUL,
    )
    fading = jnp.exp(block_decay_total)

    def carry_step(state_matrix, item):
        return (item[0][:, :, None] * state_matrix + item[1], state_matrix)

    empty_state = jnp.zeros((head_count, RDIM, RDIM), jnp.float32)
    local_state, block_starts = lax.scan(carry_step, empty_state, (fading, growth_factor))
    received_output = received_output + jnp.einsum(
        "bhtk,bhkv->bhtv", decayed_query, block_starts, precision=EXACT_MATMUL
    )
    earlier_total = jnp.cumsum(block_decay_total, axis=0) - block_decay_total
    decay_from_start = query_blocks * jnp.exp(inner_block_output + earlier_total[:, :, None, :])
    device_fade = jnp.exp(jnp.sum(block_decay_total, axis=0))
    reach = 2**GROUPS - 1
    rim = pooled_in[row_count - reach :]
    unit_fade = jnp.ones((head_count, RDIM), jnp.float32)
    previous = passed_along(rim, SP, 1)
    carried_fade, carried_state = entering(
        (device_fade, local_state), SP, chain, (unit_fade, empty_state)
    )
    received_output = received_output + jnp.einsum(
        "fuoy,uyi->fuoi", decay_from_start, carried_state, precision=EXACT_MATMUL
    )
    received_output = received_output.transpose(0, 2, 1, 3).reshape(row_count, head_count, RDIM)
    spread = lax.rsqrt(
        jnp.mean(received_output * received_output, axis=-1, keepdims=True) + EPSILON
    )
    recur_mixed = (
        (received_output * spread * out_gain).astype(jnp.bfloat16).reshape(row_count, recur_cols)
    )
    group = lax.axis_index("tp")
    padded = jnp.concatenate([previous, pooled_in], axis=0).astype(jnp.float32)
    results = window_sums(padded, GROUPS, reach)
    window_sum = results[GROUPS - 1]
    for level in range(GROUPS - 1):
        window_sum = jnp.where(group == level, results[level], window_sum)
    width = jnp.left_shift(jnp.int32(2), group)
    position = lax.axis_index(SP) * row_count + jnp.arange(row_count, dtype=jnp.int32)
    divisor = jnp.minimum(position + 1, width).astype(jnp.float32)[:, None]
    pool_mixed = (window_sum / divisor - pooled_in.astype(jnp.float32)).astype(jnp.bfloat16)
    out_pool, out_recur = side_by_side(
        (pool_out_weight, recur_out_weight), (("sp_0", "sp_1"), "sp_2"), 1, 0
    )
    partial_value = jnp.dot(pool_mixed, out_pool, preferred_element_type=jnp.float32)
    summed = sum_at_owner(
        (
            partial_value + jnp.dot(recur_mixed, out_recur, preferred_element_type=jnp.float32)
        ).astype(jnp.bfloat16),
        "tp",
        0,
    )
    return summed.astype(jnp.bfloat16)


def solution(mesh):
    split = Mesh(mesh.devices.reshape(16, 4, 2, mesh.shape["tp"]), ("sp_0", "sp_1", "sp_2", "tp"))
    in_specs = (
        P(SP_TP, None),
        P(),
        P(SP, "tp"),
        P(SP, "tp"),
        P(SP, "tp"),
        P(SP, "tp"),
        P("tp"),
        P("tp", SP),
        P(),
        P("tp", SP),
        P("tp", SP),
    )
    out_specs = P(SP_TP, None)
    return jax.shard_map(local, mesh=split, in_specs=in_specs, out_specs=out_specs, check_vma=False)
```

profile of v0, /device:TPU:6, one launch (start us, length us, event | category | flops | bytes accessed | tf_op | source)
XLA Modules:
  0.0 302.5 jit_solution(13963740435010623551)
XLA Ops:
  6.5 0.8 pad_maximum_fusion
  7.3 15.3 %all-gather = bf16[64,1024]{1,0:T(8,128)(2,1)} all-gather(bf16[16,1024]{1,0:T(8,128)(2,1)S(1)} %pad_maximum_fusion), channel_id=2, replica_groups=mesh['sp_0'=16,'sp_1'=4,'sp_2'=2,'tp'=4] {'sp_1'}, dimensions={0}, use_global_device_ids=true | all-gather | bytes 163840 | tf_op jit(solution)/shard_map/all_gather | solution.py:27
  22.7 74.3 %all-gather.14.cloned.1.call-done = bf16[64,16,1024]{2,1,0:T(8,128)(2,1)} async-done(((bf16[4,16,1024]{2,1,0:T(8,128)(2,1)}), bf16[64,16,1024]{2,1,0:T(8,128)(2,1)}) %all-gather.14.cloned.1.call-update) | async-done | bytes 2097168 | tf_op jit(solution)/shard_map/all_gather | solution.py:27
  97.1 0.2 fusion.7
  97.3 0.2 fusion.9
  97.5 1.6 broadcast_in_dim.48
  99.1 4.6 %all-to-all-start = ((bf16[4,128,2048]{2,1,0:T(8,128)(2,1)}), bf16[4,128,2048]{2,1,0:T(8,128)(2,1)}, u32[]{:S(2)}, u32[]{:S(2)}) async-start(bf16[4,128,2048]{2,1,0:T(8,128)(2,1)} %broadcast_in_dim.48), calls=%async_computation | async-start | bytes 4194304 | tf_op jit(solution)/shard_map/all_to_all | solution.py:40
  103.8 0.7 copy.48
  104.6 15.6 %all-gather.16.cloned.1.call-done = bf16[32,4,16,1024]{3,2,1,0:T(8,128)(2,1)} async-done(((bf16[16,4,16,1024]{3,2,1,0:T(8,128)(2,1)}), bf16[32,4,16,1024]{3,2,1,0:T(8,128)(2,1)}) %all-gather.16.cloned.1.call-update) | async-done | bytes 4194320 | tf_op jit(solution)/shard_map/all_gather | solution.py:27
  120.2 5.0 %copy.44 = bf16[16,4,2,16,1024]{4,3,2,1,0:T(8,128)(2,1)} copy(bf16[16,4,2,16,1024]{4,3,1,0,2:T(8,128)(2,1)} %bitcast.313) | data formatting | bytes 8388608 | tf_op jit(solution)/shard_map/transpose | solution.py:30
  125.2 1.1 broadcast_in_dim.49
  126.3 15.7 %all-to-all-start.1 = ((bf16[64,512,16]{1,2,0:T(8,128)(2,1)}), bf16[64,512,16]{1,2,0:T(8,128)(2,1)S(1)}, u32[]{:S(2)}, u32[]{:S(2)}) async-start(bf16[64,512,16]{1,2,0:T(8,128)(2,1)} %broadcast_in_dim.49), calls=%async_computation.1 | async-start | bytes 2097152 | tf_op jit(solution)/shard_map/all_to_all | solution.py:40
  142.1 4.3 %fusion.2 = bf16[512,768]{1,0:T(8,128)(2,1)S(1)} fusion(bf16[512,2048]{1,0:T(8,128)(2,1)} %bitcast, bf16[2048,1024]{1,0:T(8,128)(2,1)} %bitcast.311), kind=kOutput, calls=%fused_computation.6 | convolution fusion | flops 1611005952 | bytes 6029312 | tf_op jit(solution)/shard_map/dot_general | solution.py:145
  146.4 0.1 add_divide_fusion
  146.6 0.3 div.33
  146.9 0.2 copy-done.8
  147.0 1.3 fusion.16
  148.4 0.6 bitcast_exponential_fusion
  149.1 0.6 slice_reduce_fusion
  149.7 1.1 reshape.167
  150.7 2.6 bitcast_multiply_fusion.3
  153.3 1.0 fusion.19
  154.3 12.1 %while.13 = (s32[]{:T(128)}, f32[2,128,128]{2,1,0:T(8,128)S(1)}, f32[8,2,128,128]{3,2,1,0:T(8,128)}, f32[8,2,128]{2,0,1:T(8,128)}, f32[8,2,128,128]{3,2,1,0:T(8,128)S(1)}, /*index=5*/s32[]{:T(128)}, s32[]{:T(128)}) while((s32[]{:T(128)}, f32[2,128,128]{2,1,0:T(8,128)S(1)}, f32[8,2,128,128]{3,2,1,0:T(8,128)}, ...), condition=%wide.region_3.4_spmd.clone, body=%wide.region_2.3_spmd.clone.sunk | while | flops 131075 | bytes 658540 | solution.py:185
  154.4 0.7 constant_dynamic-slice_fusion.2
  155.1 0.7 bitcast_dynamic-update-slice_fusion.2
  155.9 0.7 constant_dynamic-slice_fusion.2
  156.6 0.7 bitcast_dynamic-update-slice_fusion.2
  157.4 0.7 constant_dynamic-slice_fusion.2
  158.1 0.7 bitcast_dynamic-update-slice_fusion.2
  158.9 0.7 constant_dynamic-slice_fusion.2
  159.6 0.7 bitcast_dynamic-update-slice_fusion.2
  160.4 0.7 constant_dynamic-slice_fusion.2
  161.1 0.7 bitcast_dynamic-update-slice_fusion.2
  161.9 0.7 constant_dynamic-slice_fusion.2
  162.6 0.7 bitcast_dynamic-update-slice_fusion.2
  163.4 0.7 constant_dynamic-slice_fusion.2
  164.1 0.7 bitcast_dynamic-update-slice_fusion.2
  164.9 0.7 constant_dynamic-slice_fusion.2
  165.6 0.7 bitcast_dynamic-update-slice_fusion.2
  166.4 1.8 all-gather.6
  168.3 6.7 %all-gather.7 = f32[4,2,128]{2,1,0:T(2,128)S(1)} all-gather(f32[1,2,128]{2,1,0:T(2,128)S(1)} %fusion.183), channel_id=7, replica_groups=mesh['sp_0'=16,'sp_1'=4,'sp_2'=2,'tp'=4] {'sp_1'}, dimensions={0}, use_global_device_ids=true | all-gather | bytes 5120 | tf_op jit(solution)/shard_map/all_gather | solution.py:64
  175.0 2.0 all-gather.4
  177.1 14.2 %all_gather.55 = f32[4,2,128,128]{3,2,1,0:T(8,128)S(1)} all-gather(f32[1,2,128,128]{3,2,1,0:T(8,128)S(1)} %bitcast_add_fusion.5), channel_id=1, replica_groups=mesh['sp_0'=16,'sp_1'=4,'sp_2'=2,'tp'=4] {'sp_1'}, dimensions={0}, use_global_device_ids=true | all-gather | bytes 655360 | tf_op jit(solution)/shard_map/all_gather | solution.py:64
  191.3 0.9 multiply_add_fusion
  192.3 5.4 %all-to-all-done.1 = bf16[64,512,16]{1,2,0:T(8,128)(2,1)S(1)} async-done(((bf16[64,512,16]{1,2,0:T(8,128)(2,1)}), bf16[64,512,16]{1,2,0:T(8,128)(2,1)S(1)}, u32[]{:S(2)}, u32[]{:S(2)}) %all-to-all-start.1) | async-done | bytes 1048608 | tf_op jit(solution)/shard_map/all_to_all | solution.py:40
  197.7 0.3 broadcast_in_dim.50
  198.0 5.4 %all_to_all.21 = bf16[2,64,512,16]{2,3,1,0:T(8,128)(2,1)S(1)} all-to-all(bf16[2,64,512,16]{2,3,1,0:T(8,128)(2,1)S(1)} %broadcast_in_dim.50), channel_id=1, replica_groups=mesh['sp_0'=16,'sp_1'=4,'sp_2'=2,'tp'=4] {'sp_2'}, dimensions={0} | all-to-all | bytes 4194304 | tf_op jit(solution)/shard_map/all_to_all | solution.py:40
  203.4 0.2 copy.45
  203.6 0.2 fusion.185
  203.8 2.6 convolution_convert_fusion
  206.4 2.0 collective-permute-start
  208.4 26.4 %all_gather.52 = f32[16,2,128]{2,1,0:T(2,128)S(1)} all-gather(f32[1,2,128]{2,1,0:T(2,128)S(1)} %get-tuple-element.114), channel_id=1, replica_groups=mesh['sp_0'=16,'sp_1'=4,'sp_2'=2,'tp'=4] {'sp_0'}, dimensions={0}, use_global_device_ids=true | all-gather | bytes 17408 | tf_op jit(solution)/shard_map/all_gather | solution.py:64
  234.8 1.2 convolution_select_fusion
  236.0 0.4 fusion.33
  236.7 2.8 fusion.28
  239.5 27.5 %all-gather.12.cloned.1.call-done = f32[16,2,128,128]{3,2,1,0:T(8,128)} async-done(((f32[1,2,128,128]{3,2,1,0:T(8,128)}), f32[16,2,128,128]{3,2,1,0:T(8,128)}) %all-gather.12.cloned.1.call-update) | async-done | bytes 2097168 | tf_op jit(solution)/shard_map/all_gather | solution.py:64
  267.0 3.4 %convolution_bitcast_fusion = f32[8,64,2,128]{3,1,2,0:T(8,128)S(1)} fusion(f32[8,2,64,128]{3,0,1,2:T(8,128)} %get-tuple-element.90, f32[16,2,128,128]{3,2,1,0:T(8,128)} %all-gather.12.cloned.1.call-done, f32[4,2,128,128]{3,2,1,0:T(8,128)S(1)} %all_gather.55, f32[4,128,128]{2,1,0:T(8,128)S(1)} %all-gather.4, f32[2,128]{1,0:T(2,128)S(1)} %get-tuple-element.119, ...), kind=kOutput, calls=%fused_computation.13 | convolution fusion | flops 203522048 | bytes 3956758 | tf_op jit(solution)/shard_map/fuoy,uyi->fuoi/dot_general | solution.py:199
  270.5 1.3 multiply_reduce_fusion
  271.8 0.2 multiply_convert_fusion
  272.0 0.3 copy.56
  272.3 0.3 copy-done
  272.7 0.8 add_convert_fusion
  273.4 21.2 %all_to_all.22 = bf16[4,128,2048]{2,1,0:T(8,128)(2,1)S(1)} all-to-all(bf16[4,128,2048]{2,1,0:T(8,128)(2,1)S(1)} %bitcast.310), channel_id=1, replica_groups=mesh['sp_0'=16,'sp_1'=4,'sp_2'=2,'tp'=4] {'tp'}, dimensions={0} | all-to-all | bytes 4194304 | tf_op jit(solution)/shard_map/all_to_all | solution.py:96
  294.6 1.3 reduce_sum.42
  (58 shorter events, 1.8 us)
Async XLA Ops:
  6.5 90.5 %copy-start.1 = (bf16[128,2048]{1,0:T(8,128)(2,1)S(1)}, bf16[128,2048]{1,0:T(8,128)(2,1)}, u32[]{:S(2)}) copy-start(bf16[128,2048]{1,0:T(8,128)(2,1)} %param.13) | copy-start | bytes 1572868
  6.5 90.7 %copy-start.3 = (f32[2048]{0:T(1024)S(1)}, f32[2048]{0:T(1024)}, u32[]{:S(2)}) copy-start(f32[2048]{0:T(1024)} %param.14) | copy-start | bytes 24580
  6.5 90.5 %all-gather.14.cloned.1.call-start = ((), (), s32[]{:S(2)}) async-start(), calls=%async_computation.5 | async-start | bytes 2228224 | tf_op jit(solution)/shard_map/all_gather | solution.py:27
  22.7 97.5 %all-gather.16.cloned.1.call-start = ((), (), s32[]{:S(2)}) async-start(), calls=%async_computation.6 | async-start | bytes 6291456 | tf_op jit(solution)/shard_map/all_gather | solution.py:27
  99.1 4.7 %copy-start.6 = (f32[2,512]{1,0:T(2,128)S(1)}, f32[2,512]{1,0:T(2,128)}, u32[]{:S(2)}) copy-start(f32[2,512]{1,0:T(2,128)} %param.20) | copy-start | bytes 12292
  99.1 5.5 %copy-start.4 = (bf16[256,16]{0,1:T(8,128)(2,1)S(1)}, bf16[256,16]{0,1:T(8,128)(2,1)}, u32[]{:S(2)}) copy-start(bf16[256,16]{0,1:T(8,128)(2,1)} %param.23) | copy-start | bytes 24580
  99.1 5.5 %copy-start.5 = (bf16[256,16]{0,1:T(8,128)(2,1)S(1)}, bf16[256,16]{0,1:T(8,128)(2,1)}, u32[]{:S(2)}) copy-start(bf16[256,16]{0,1:T(8,128)(2,1)} %param.22) | copy-start | bytes 24580
  99.1 26.1 %all-to-all-start = ((bf16[4,128,2048]{2,1,0:T(8,128)(2,1)}), bf16[4,128,2048]{2,1,0:T(8,128)(2,1)}, u32[]{:S(2)}, u32[]{:S(2)}) async-start(bf16[4,128,2048]{2,1,0:T(8,128)(2,1)} %broadcast_in_dim.48), calls=%async_computation | async-start | bytes 4194304 | tf_op jit(solution)/shard_map/all_to_all | solution.py:40
  126.3 71.4 %all-to-all-start.1 = ((bf16[64,512,16]{1,2,0:T(8,128)(2,1)}), bf16[64,512,16]{1,2,0:T(8,128)(2,1)S(1)}, u32[]{:S(2)}, u32[]{:S(2)}) async-start(bf16[64,512,16]{1,2,0:T(8,128)(2,1)} %broadcast_in_dim.49), calls=%async_computation.1 | async-start | bytes 2097152 | tf_op jit(solution)/shard_map/all_to_all | solution.py:40
  142.0 125.0 %all-gather.12.cloned.1.call-start = ((), (), s32[]{:S(2)}) async-start(), calls=%async_computation.4 | async-start | bytes 2228224 | tf_op jit(solution)/shard_map/all_gather | solution.py:64
  146.4 0.7 copy-start.8
  154.3 12.1 %copy-start.7 = (f32[2,128]{1,0:T(2,128)S(1)}, f32[2,128]{1,0:T(2,128)}, u32[]{:S(2)}) copy-start(f32[2,128]{1,0:T(2,128)} %get-tuple-element.95) | copy-start | bytes 3076
  206.4 30.1 %collective-permute-start = (bf16[15,256]{1,0:T(8,128)(2,1)S(1)}, bf16[15,256]{1,0:T(8,128)(2,1)S(1)}, u32[]{:S(2)}, u32[]{:S(2)}) collective-permute-start(bf16[15,256]{1,0:T(8,128)(2,1)S(1)} %slice.276), channel_id=1, source_target_pairs={{0,4},{4,8},{8,12},{12,16},{16,20},{20,24},{24,28},{28,32},{32,36}... | collective-permute-start | bytes 23048 | tf_op jit(solution)/shard_map/ppermute | solution.py:50
  267.0 3.5 %copy-start.2 = (f32[8,2,128,128]{3,2,1,0:T(8,128)S(1)}, f32[8,2,128,128]{3,2,1,0:T(8,128)}, u32[]{:S(2)}) copy-start(f32[8,2,128,128]{3,2,1,0:T(8,128)} %get-tuple-element.33) | copy-start | bytes 3145732
  270.5 1.4 copy-start.9
  270.5 2.2 copy-start
Sparse Core Ops, SparseCore 0:
  22.8 74.1 all-gather.13
  99.1 21.0 all-gather.15
  192.3 74.6 all-gather.11
where the time goes:
time: 303 us; the launch traced here: 302 us
  waiting for transfers between devices  123 us (41%)
  blocking collectives  93 us (31%)
  starting transfers between devices  22.4 us (7%)
  local copies, waits for them, and re-layouts  17.7 us (6%)
  matrix products  17.7 us (6%)
  other arithmetic  14.9 us (5%)
  between operations  13.5 us (4%)
    all_gather x2, waiting for transfers between devices, gather_in_order(): parts = lax.all_gather(parts, axes[k])  89.9 us
    all_gather x5, blocking collectives, entering(): pieces = jax.tree.map(lambda part: lax.all_gather(part, axis), subtotal)  51.1 us
    all_gather x1, waiting for transfers between devices, entering(): pieces = jax.tree.map(lambda part: lax.all_gather(part, axis), subtotal)  27.5 us
    all_to_all x1, blocking collectives, sum_at_owner(): parts = lax.all_to_all(split_up(x, dim, devices), axis, 0, 0, tiled=True)  21.2 us
    all_to_all x2, starting transfers between devices, sent_to_all(): return lax.all_to_all(copies, axis, split_axis=0, concat_axis=0, tiled=True)  20.3 us
    all_gather x1, blocking collectives, gather_in_order(): parts = lax.all_gather(parts, axes[k])  15.3 us
  transfers between devices with their start and end apart: 6, of which 4 were waited for; matrix products, arithmetic and copies ran while one was open for 13% of the time, Pallas kernels for 0%

commit v1 on v0

v1 whole, which is shorter than its diff:
```python
import jax
import jax.numpy as jnp
from jax import lax
from jax.experimental import pallas as pl
from jax.experimental.pallas import tpu as pltpu
from jax.sharding import Mesh
from jax.sharding import PartitionSpec as P


GROUPS = 4
RDIM = 128
CHUNK = 128
RIM = 16
SP = ("sp_0", "sp_1", "sp_2")
SP_TP = ("sp_0", "sp_1", "sp_2", "tp")
EPSILON = 1e-06
BF = jnp.bfloat16
F32 = jnp.float32
NT = (((1,), (1,)), ((), ()))
TN = (((0,), (0,)), ((), ()))
NN = (((1,), (0,)), ((), ()))


def dot(a, b, dims=NN):
    return lax.dot_general(a, b, dims, preferred_element_type=F32)


def halves(x):
    high = x.astype(BF)
    return high, (x - high.astype(F32)).astype(BF)


def dot_wide(a, b, dims=NN):
    ah, al = halves(a)
    bh, bl = halves(b)
    return dot(ah, bh, dims) + (dot(ah, bl, dims) + dot(al, bh, dims))


def dot_left(a, b, dims=NN):
    ah, al = halves(a)
    return dot(ah, b, dims) + dot(al, b, dims)


def sent_to_all(x, axis):
    copies = jnp.broadcast_to(x, (lax.axis_size(axis), *x.shape))
    return lax.all_to_all(copies, axis, split_axis=0, concat_axis=0, tiled=True)


def ring_gather(x, axis):
    n = lax.axis_size(axis)
    up = [(i, (i + 1) % n) for i in range(n)]
    down = [(i, (i - 1) % n) for i in range(n)]
    half = x.shape[0] // 2
    before = lax.ppermute(x, axis, up)
    after = lax.ppermute(x, axis, down)
    far_low = lax.ppermute(before[:half], axis, up)
    far_high = lax.ppermute(after[half:], axis, down)
    return x, before, after, far_low, far_high


def places(index, n):
    return [index, lax.rem(index + n - 1, n), lax.rem(index + 1, n), lax.rem(index + 2, n)]


def assemble(info_ref, mine_ref, other_ref, whole_ref):
    core = info_ref[0]
    nx, nz, rows, _ = mine_ref.shape
    spots = places(info_ref[3], nx)

    def put(z, carry):
        for k, spot in enumerate(spots):
            at = ((z * nx + spot) * 2) * rows
            here = pl.ds(pl.multiple_of(at + core * rows, rows), rows)
            there = pl.ds(pl.multiple_of(at + (1 - core) * rows, rows), rows)
            whole_ref[here, :] = mine_ref[k, z]
            whole_ref[there, :] = other_ref[k, z]
        return carry

    lax.fori_loop(0, nz, put, 0)


def state_kernel(
    info_ref,
    own_ref,
    before_ref,
    after_ref,
    low_ref,
    high_ref,
    gain_ref,
    mine_ref,
    other_ref,
    gap_ref,
    shift_ref,
    normed_ref,
    values_ref,
    opened_ref,
    cum_ref,
    growth_ref,
    payload_ref,
    whole_ref,
    both_ref,
):
    rows, _ = normed_ref.shape
    cols = gap_ref.shape[1]
    assemble(info_ref, mine_ref, other_ref, whole_ref)
    block = own_ref.shape[0]
    own, before, after, far = places(info_ref[1], rows // block)

    def norm(from_ref, start, i):
        floats = from_ref[pl.ds(pl.multiple_of(i * 32, 32), 32), :].astype(F32)
        scale = lax.rsqrt(jnp.mean(floats * floats, axis=-1, keepdims=True) + EPSILON)
        at = pl.ds(pl.multiple_of(start + i * 32, 32), 32)
        normed_ref[at, :] = (floats * scale * gain_ref[...]).astype(BF)

    def norm_all(i, carry):
        for from_ref, place in ((own_ref, own), (before_ref, before), (after_ref, after)):
            norm(from_ref, place * block, i)
        return carry

    def norm_far(i, carry):
        norm(low_ref, far * block, i)
        norm(high_ref, far * block + block // 2, i)
        return carry

    lax.fori_loop(0, block // 32, norm_all, 0)
    lax.fori_loop(0, block // 64, norm_far, 0)
    both_ref[...] = dot(normed_ref[...], whole_ref[...])
    row = lax.broadcasted_iota(jnp.int32, (CHUNK, CHUNK), 0)
    col = lax.broadcasted_iota(jnp.int32, (CHUNK, CHUNK), 1)
    tril = (row >= col).astype(BF)
    heads = cols // RDIM
    for h in range(heads):
        lanes = slice(h * RDIM, (h + 1) * RDIM)
        state = jnp.zeros((RDIM, RDIM), F32)
        faded = jnp.zeros((1, RDIM), F32)
        for c in range(rows // CHUNK):
            at = slice(c * CHUNK, (c + 1) * CHUNK)
            pre = both_ref[at, lanes].astype(BF).astype(F32)
            values = both_ref[at, cols + h * RDIM : cols + (h + 1) * RDIM].astype(BF)
            opened = gap_ref[:, lanes] / (1.0 + jnp.exp(pre))
            decay = jnp.log1p(-opened) + shift_ref[at, h : h + 1]
            d0, d1 = halves(decay)
            d2 = (decay - d0.astype(F32) - d1.astype(F32)).astype(BF)
            cum = dot(tril, d0) + (dot(tril, d1) + dot(tril, d2))
            total = cum[CHUNK - 1 :, :]
            growth = dot_left_t(values, opened * jnp.exp(total - cum))
            values_ref[at, lanes] = values
            opened_ref[at, lanes] = opened
            cum_ref[at, lanes] = cum
            growth_ref[c, :, lanes] = growth
            state = state * jnp.exp(total) + growth
            faded = faded + total
        payload_ref[:, lanes] = state
        payload_ref[:, cols + h * RDIM : cols + (h + 1) * RDIM] = jnp.broadcast_to(faded, (RDIM, RDIM))


def dot_left_t(values, key):
    kh, kl = halves(key)
    return dot(values, kh, TN) + dot(values, kl, TN)


def scan_kernel(got_ref, start_ref):
    rows, cols = start_ref.shape
    per = rows // lax.axis_size(SP)
    state = got_ref[:, :cols]
    fade = jnp.exp(got_ref[:, cols:])
    index = lax.broadcasted_iota(jnp.int32, (rows, cols), 0)
    step = per
    while step < rows:
        inside = index >= step
        before = jnp.where(inside, pltpu.roll(state, step, 0), 0.0)
        earlier = jnp.where(inside, pltpu.roll(fade, step, 0), 1.0)
        state = fade * before + state
        fade = fade * earlier
        step *= 2
    start_ref[...] = jnp.where(index >= per, pltpu.roll(state, per, 0), 0.0)


def inner_kernel(
    info_ref,
    normed_ref,
    mine_ref,
    other_ref,
    values_ref,
    opened_ref,
    cum_ref,
    pooled_ref,
    decayed_ref,
    heard_ref,
    whole_ref,
    both_ref,
):
    rows, cols = values_ref.shape
    assemble(info_ref, mine_ref, other_ref, whole_ref)
    both_ref[...] = dot(normed_ref[...], whole_ref[...])
    pooled_ref[...] = both_ref[:, cols:].astype(BF)
    row = lax.broadcasted_iota(jnp.int32, (CHUNK, CHUNK), 0)
    col = lax.broadcasted_iota(jnp.int32, (CHUNK, CHUNK), 1)
    for h in range(cols // RDIM):
        lanes = slice(h * RDIM, (h + 1) * RDIM)
        for c in range(rows // CHUNK):
            at = slice(c * CHUNK, (c + 1) * CHUNK)
            cum = cum_ref[at, lanes]
            query = both_ref[at, lanes].astype(BF).astype(F32) * jnp.exp(cum)
            key = opened_ref[at, lanes] * jnp.exp(-cum)
            scores = jnp.where(row >= col, dot_wide(query, key, NT), 0.0)
            decayed_ref[at, lanes] = query
            heard_ref[at, lanes] = dot_left(scores, values_ref[at, lanes])


def final_kernel(
    info_ref,
    start_ref,
    growth_ref,
    cum_ref,
    decayed_ref,
    heard_ref,
    pooled_ref,
    rim_ref,
    gain_ref,
    mine_ref,
    other_ref,
    part_ref,
    whole_ref,
    mixed_ref,
):
    rows, cols = cum_ref.shape
    assemble(info_ref, mine_ref, other_ref, whole_ref)
    group = info_ref[1]
    padded = jnp.concatenate([rim_ref[...], pooled_ref[...]], axis=0).astype(F32)
    running = padded
    chosen = None
    for level in range(GROUPS):
        running = running + pltpu.roll(running, 2**level, 0)
        chosen = running if chosen is None else jnp.where(group == level, running, chosen)
    width = jnp.left_shift(jnp.int32(2), group)
    position = info_ref[2] + lax.broadcasted_iota(jnp.int32, (rows, cols), 0)
    divisor = jnp.minimum(position + 1, width).astype(F32)
    mixed_ref[:, :cols] = (chosen[RIM:] / divisor - padded[RIM:]).astype(BF)
    for h in range(cols // RDIM):
        lanes = slice(h * RDIM, (h + 1) * RDIM)
        state = start_ref[:, lanes]
        for c in range(rows // CHUNK):
            at = slice(c * CHUNK, (c + 1) * CHUNK)
            heard = heard_ref[at, lanes] + dot_wide(decayed_ref[at, lanes], state, NT)
            spread = lax.rsqrt(jnp.mean(heard * heard, axis=-1, keepdims=True) + EPSILON)
            mixed_ref[at, cols + h * RDIM : cols + (h + 1) * RDIM] = (
                heard * spread * gain_ref[...]
            ).astype(BF)
            total = cum_ref[(c + 1) * CHUNK - 1 : (c + 1) * CHUNK, lanes]
            state = state * jnp.exp(total) + growth_ref[c, :, lanes]

    def out(i, carry):
        at = pl.ds(pl.multiple_of(i * 256, 256), 256)
        part_ref[:, at] = dot(mixed_ref[...], whole_ref[at, :], NT).astype(BF)
        return carry

    lax.fori_loop(0, part_ref.shape[1] // 256, out, 0)


VMEM = pl.BlockSpec(memory_space=pltpu.VMEM)
SMEM = pl.BlockSpec(memory_space=pltpu.SMEM)


def call(kernel, outs, scratch, flops, moved, *args):
    return pl.pallas_call(
        kernel,
        out_shape=outs,
        in_specs=[SMEM if a.dtype == jnp.int32 else VMEM for a in args],
        out_specs=jax.tree.map(lambda _: VMEM, outs),
        scratch_shapes=scratch,
        cost_estimate=pl.CostEstimate(flops=flops, bytes_accessed=moved, transcendentals=0),
    )(*args)


def shape(dims, dtype):
    return jax.ShapeDtypeStruct(dims, dtype)


def stacked(pieces):
    own, before, after, low, high = pieces
    far = jnp.concatenate([low, high], axis=0)
    return jnp.stack([own, before, after, far])


def over_cores(x):
    return lax.ppermute(x, "sp_2", [(0, 1), (1, 0)])


def layer(
    tokens,
    norm_gain,
    pool_in_weight,
    query_weight,
    forget_weight,
    input_weight,
    forget_gap,
    decay_shift,
    out_gain,
    pool_out_weight,
    recur_out_weight,
):
    width = tokens.shape[1]
    cols = query_weight.shape[1]
    tp = lax.axis_size("tp")
    rows = tokens.shape[0] * tp
    devices = lax.axis_size(SP)
    core = lax.axis_index("sp_2")
    group = lax.axis_index("tp")
    info = jnp.stack([core, group, lax.axis_index(SP) * rows, lax.axis_index("sp_1")]).astype(jnp.int32)

    pieces = ring_gather(tokens, "tp")
    first = jnp.concatenate([forget_weight, input_weight], axis=1)
    second = jnp.concatenate(
        [query_weight, pool_in_weight, pool_out_weight.T, recur_out_weight.T], axis=1
    )
    first_z = sent_to_all(first, "sp_0")
    second_z = sent_to_all(second, "sp_0")
    first_zx = stacked(ring_gather(first_z, "sp_1"))
    first_other = over_cores(first_zx)
    in_zx = stacked(ring_gather(second_z[..., : 2 * cols], "sp_1"))
    in_other = over_cores(in_zx)
    out_zx = stacked(ring_gather(second_z[..., 2 * cols :], "sp_1"))
    out_other = over_cores(out_zx)

    normed, values, opened, cum, growth, payload = call(
        state_kernel,
        [
            shape((rows, width), BF),
            shape((rows, cols), BF),
            shape((rows, cols), F32),
            shape((rows, cols), F32),
            shape((rows // CHUNK, RDIM, cols), F32),
            shape((RDIM, 2 * cols), F32),
        ],
        [pltpu.VMEM((width, 2 * cols), BF), pltpu.VMEM((rows, 2 * cols), F32)],
        4 * rows * width * cols,
        8 << 20,
        info,
        *pieces,
        norm_gain[None, :],
        first_zx,
        first_other,
        forget_gap[None, :],
        decay_shift.T,
    )

    got = lax.all_to_all(payload, SP, split_axis=0, concat_axis=0, tiled=True)
    start = call(scan_kernel, shape((RDIM, cols), F32), [], 1 << 22, 1 << 20, got)
    start = lax.all_to_all(start, SP, split_axis=0, concat_axis=0, tiled=True)
    pooled, decayed, heard = call(
        inner_kernel,
        [shape((rows, cols), BF), shape((rows, cols), F32), shape((rows, cols), F32)],
        [pltpu.VMEM((width, 2 * cols), BF), pltpu.VMEM((rows, 2 * cols), F32)],
        4 * rows * width * cols,
        8 << 20,
        info,
        normed,
        in_zx,
        in_other,
        values,
        opened,
        cum,
    )
    order = [(i - 1, i) for i in range(1, devices)]
    rim = lax.ppermute(pooled[rows - RIM :], SP, order)
    part = call(
        final_kernel,
        shape((rows, width), BF),
        [pltpu.VMEM((width, 2 * cols), BF), pltpu.VMEM((rows, 2 * cols), BF)],
        4 * rows * width * cols,
        8 << 20,
        info,
        start,
        growth,
        cum,
        decayed,
        heard,
        pooled,
        rim,
        out_gain[None, :],
        out_zx,
        out_other,
    )
    parts = lax.all_to_all(
        part.reshape(tp, rows // tp, width), "tp", split_axis=0, concat_axis=0, tiled=True
    )
    return jnp.sum(parts.astype(F32), axis=0).astype(BF)


def solution(mesh):
    split = Mesh(mesh.devices.reshape(16, 4, 2, mesh.shape["tp"]), ("sp_0", "sp_1", "sp_2", "tp"))
    in_specs = (
        P(SP_TP, None),
        P(),
        P(SP, "tp"),
        P(SP, "tp"),
        P(SP, "tp"),
        P(SP, "tp"),
        P("tp"),
        P("tp", SP),
        P(),
        P("tp", SP),
        P("tp", SP),
    )
    out_specs = P(SP_TP, None)
    return jax.shard_map(layer, mesh=split, in_specs=in_specs, out_specs=out_specs, check_vma=False)
```

time: 303 us -> 234 us (0.77)
  starting transfers between devices: 22.4 us -> 109 us
  waiting for transfers between devices: 123 us -> 46.8 us
  blocking collectives: 93 us -> 30.5 us
  Pallas kernels: 0 us -> 24.3 us
  matrix products: 17.7 us -> 0 us
  between operations: 13.5 us -> 0.47 us
  other arithmetic: 14.9 us -> 6.79 us
  local copies, waits for them, and re-layouts: 17.7 us -> 14.4 us
    all_gather x3 -> x0, waiting for transfers between devices: 117 us -> none  [the longest x2 89.9 us: gather_in_order(): parts = lax.all_gather(parts, axes[k])]
    all_gather x6 -> x0, blocking collectives: 66.4 us -> none  [the longest x5 51.1 us: entering(): pieces = jax.tree.map(lambda part: lax.all_gather(part, axis), subtotal)]
    ppermute x1 -> x20, starting transfers between devices: 2.04 us -> 65.6 us  [the longest x4 18.9 us: ring_gather(): far_low = lax.ppermute(before[:half], axis, up)]
    pallas_call x0 -> x4, Pallas kernels: none -> 24.3 us  [call(): pl.pallas_call(kernel, out_shape=outs, in_specs=[SMEM if a.dtype == jnp.i...]
    all_to_all x0 -> x2, starting transfers between devices: none -> 22.7 us  [the longest x1 15.6 us: layer(): got = lax.all_to_all(payload, SP, split_axis=0, concat_axis=0, tiled=True)]
    all_to_all x0 -> x2, waiting for transfers between devices: none -> 20.5 us  [the longest x1 13.9 us: layer(): got = lax.all_to_all(payload, SP, split_axis=0, concat_axis=0, tiled=True)]
    dot_general x9 -> x0, matrix products: 17.7 us -> none  [the longest x1 4.31 us: local(): jnp.dot(gathered_copies(normed, 'tp', 0), recur_weight, preferred_element...]
    all_to_all x2, waiting for transfers between devices: 5.41 us -> 17.6 us  [sent_to_all(): return lax.all_to_all(copies, axis, split_axis=0, concat_axis=0, tiled=True)]
  transfers between devices with their start and end apart: 6 -> 24, of which waited for: 4 -> 7; matrix products, arithmetic and copies ran while one was open for 13% -> 7% of each run, Pallas kernels for 0% -> 7%
where the time goes in v1:
time: 234 us; the launch traced here: 233 us
  starting transfers between devices  109 us (47%)
  waiting for transfers between devices  46.8 us (20%)
  blocking collectives  30.5 us (13%)
  Pallas kernels  24.3 us (10%)
  local copies, waits for them, and re-layouts  14.4 us (6%)
  other arithmetic  6.79 us (3%)
    all_to_all x1, blocking collectives, layer(): lax.all_to_all(part.reshape(tp, rows // tp, width), 'tp', split_axis=0, c...  30.5 us
    pallas_call x4, Pallas kernels, call(): pl.pallas_call(kernel, out_shape=outs, in_specs=[SMEM if a.dtype == jnp.i...  24.3 us
    all_to_all x2, starting transfers between devices, sent_to_all(): return lax.all_to_all(copies, axis, split_axis=0, concat_axis=0, tiled=True)  21 us
    ppermute x4, starting transfers between devices, ring_gather(): far_low = lax.ppermute(before[:half], axis, up)  18.9 us
    ppermute x4, starting transfers between devices, ring_gather(): before = lax.ppermute(x, axis, up)  18.8 us
    all_to_all x2, waiting for transfers between devices, sent_to_all(): return lax.all_to_all(copies, axis, split_axis=0, concat_axis=0, tiled=True)  17.6 us
    all_to_all x1, starting transfers between devices, layer(): got = lax.all_to_all(payload, SP, split_axis=0, concat_axis=0, tiled=True)  15.6 us
    all_to_all x1, waiting for transfers between devices, layer(): got = lax.all_to_all(payload, SP, split_axis=0, concat_axis=0, tiled=True)  13.9 us
  transfers between devices with their start and end apart: 24, of which 7 were waited for; matrix products, arithmetic and copies ran while one was open for 7% of the time, Pallas kernels for 7%

profile of v1, /device:TPU:6, one launch (start us, length us, event | category | flops | bytes accessed | tf_op | source)
XLA Modules:
  0.0 232.6 jit_solution(12092353341990442390)
XLA Ops:
  0.0 0.7 pad_maximum_fusion.4
  0.7 0.7 broadcast_in_dim.16
  1.4 15.2 %all-to-all-start = ((bf16[16,16,512]{2,1,0:T(8,128)(2,1)}), bf16[16,16,512]{2,1,0:T(8,128)(2,1)S(1)}, u32[]{:S(2)}, u32[]{:S(2)}) async-start(bf16[16,16,512]{2,1,0:T(8,128)(2,1)} %broadcast_in_dim.16), calls=%async_computation | async-start | bytes 524288 | tf_op jit(solution)/shard_map/all_to_all | solution.py:46
  16.6 0.8 pad_maximum_fusion.3
  17.4 17.6 %all-to-all-done = bf16[16,16,512]{2,1,0:T(8,128)(2,1)S(1)} async-done(((bf16[16,16,512]{2,1,0:T(8,128)(2,1)}), bf16[16,16,512]{2,1,0:T(8,128)(2,1)S(1)}, u32[]{:S(2)}, u32[]{:S(2)}) %all-to-all-start) | async-done | bytes 262176 | tf_op jit(solution)/shard_map/all_to_all | solution.py:46
  35.0 0.9 broadcast_in_dim.18
  35.9 5.8 %all-to-all-start.3 = ((bf16[16,16,1024]{2,1,0:T(8,128)(2,1)}), bf16[16,16,1024]{2,1,0:T(8,128)(2,1)S(1)}, u32[]{:S(2)}, u32[]{:S(2)}) async-start(bf16[16,16,1024]{2,1,0:T(8,128)(2,1)} %broadcast_in_dim.18), calls=%async_computation.3 | async-start | bytes 1048576 | tf_op jit(solution)/shard_map/all_to_all | solution.py:46
  41.7 2.7 %collective-permute-start.5 = (bf16[16,16,512]{2,1,0:T(8,128)(2,1)S(1)}, bf16[16,16,512]{2,1,0:T(8,128)(2,1)S(1)}, u32[]{:S(2)}, u32[]{:S(2)}) collective-permute-start(bf16[16,16,512]{2,1,0:T(8,128)(2,1)S(1)} %all-to-all-done), channel_id=1, source_target_pairs={{0,24},{8,0},{16,8},{24,16},{1,25},{9,1},{17,9},{25,17},{2,26},{10... | collective-permute-start | bytes 786440 | tf_op jit(solution)/shard_map/ppermute | solution.py:55
  44.4 4.3 %collective-permute-start.4 = (bf16[16,16,512]{2,1,0:T(8,128)(2,1)S(1)}, bf16[16,16,512]{2,1,0:T(8,128)(2,1)S(1)}, u32[]{:S(2)}, u32[]{:S(2)}) collective-permute-start(bf16[16,16,512]{2,1,0:T(8,128)(2,1)S(1)} %all-to-all-done), channel_id=1, source_target_pairs={{0,8},{8,16},{16,24},{24,0},{1,9},{9,17},{17,25},{25,1},{2,10},{10... | collective-permute-start | bytes 786440 | tf_op jit(solution)/shard_map/ppermute | solution.py:54
  48.7 3.7 %collective-permute-done.5 = bf16[16,16,512]{2,1,0:T(8,128)(2,1)S(1)} collective-permute-done((bf16[16,16,512]{2,1,0:T(8,128)(2,1)S(1)}, bf16[16,16,512]{2,1,0:T(8,128)(2,1)S(1)}, u32[]{:S(2)}, u32[]{:S(2)}) %collective-permute-start.5) | collective-permute-done | bytes 262176 | tf_op jit(solution)/shard_map/ppermute | solution.py:55
  52.5 1.9 collective-permute-start.7
  54.4 5.1 %collective-permute-start.6 = (bf16[8,16,512]{2,1,0:T(8,128)(2,1)S(1)}, bf16[8,16,512]{2,1,0:T(8,128)(2,1)S(1)}, u32[]{:S(2)}, u32[]{:S(2)}) collective-permute-start(bf16[8,16,512]{2,1,0:T(8,128)(2,1)S(1)} %slice.46), channel_id=1, source_target_pairs={{0,8},{8,16},{16,24},{24,0},{1,9},{9,17},{17,25},{25,1},{2,10},{10... | collective-permute-start | bytes 393224 | tf_op jit(solution)/shard_map/ppermute | solution.py:56
  59.6 1.0 collective-permute-done.7
  60.6 1.5 collective-permute-done.6
  62.1 0.1 pad_maximum_fusion.mine_ref
  62.3 0.0 copy-start.10
  62.3 2.1 collective-permute-start.8
  64.3 3.5 %collective-permute-start = (bf16[128,2048]{1,0:T(8,128)(2,1)}, bf16[128,2048]{1,0:T(8,128)(2,1)S(1)}, u32[]{:S(2)}, u32[]{:S(2)}) collective-permute-start(bf16[128,2048]{1,0:T(8,128)(2,1)} %own_ref.1), channel_id=1, source_target_pairs={{0,1},{1,2},{2,3},{3,0},{4,5},{5,6},{6,7},{7,4},{8,9},{9,10},{10,1... | collective-permute-start | bytes 1572872 | tf_op jit(solution)/shard_map/ppermute | solution.py:54
  67.8 3.6 %collective-permute-start.1 = (bf16[128,2048]{1,0:T(8,128)(2,1)}, bf16[128,2048]{1,0:T(8,128)(2,1)S(1)}, u32[]{:S(2)}, u32[]{:S(2)}) collective-permute-start(bf16[128,2048]{1,0:T(8,128)(2,1)} %own_ref.1), channel_id=1, source_target_pairs={{0,3},{1,0},{2,1},{3,2},{4,7},{5,4},{6,5},{7,6},{8,11},{9,8},{10,9... | collective-permute-start | bytes 1572872 | tf_op jit(solution)/shard_map/ppermute | solution.py:55
  71.4 0.8 slice_bitcast_fusion
  72.2 2.0 collective-permute-start.10
  74.3 5.5 %collective-permute-start.9 = (bf16[16,16,512]{2,1,0:T(8,128)(2,1)S(1)}, bf16[16,16,512]{2,1,0:T(8,128)(2,1)}, u32[]{:S(2)}, u32[]{:S(2)}) collective-permute-start(bf16[16,16,512]{2,1,0:T(8,128)(2,1)S(1)} %get-tuple-element.26), channel_id=1, source_target_pairs={{0,8},{8,16},{16,24},{24,0},{1,9},{9,17},{17,25},{25,1},{2,10},{10... | collective-permute-start | bytes 786440 | tf_op jit(solution)/shard_map/ppermute | solution.py:54
  79.7 2.3 collective-permute-done.before_ref
  82.0 1.9 collective-permute-start.16
  84.0 0.0 collective-permute-done.1.after_ref
  84.0 5.6 %collective-permute-start.15 = (bf16[16,16,512]{2,1,0:T(8,128)(2,1)}, bf16[16,16,512]{2,1,0:T(8,128)(2,1)S(1)}, u32[]{:S(2)}, u32[]{:S(2)}) collective-permute-start(bf16[16,16,512]{2,1,0:T(8,128)(2,1)} %get-tuple-element.25), channel_id=1, source_target_pairs={{0,8},{8,16},{16,24},{24,0},{1,9},{9,17},{17,25},{25,1},{2,10},{10... | collective-permute-start | bytes 786440 | tf_op jit(solution)/shard_map/ppermute | solution.py:54
  89.6 0.7 slice.44
  90.3 0.7 slice.45
  91.0 3.5 %collective-permute-start.2 = (bf16[64,2048]{1,0:T(8,128)(2,1)}, bf16[64,2048]{1,0:T(8,128)(2,1)}, u32[]{:S(2)}, u32[]{:S(2)}) collective-permute-start(bf16[64,2048]{1,0:T(8,128)(2,1)} %slice.44), channel_id=1, source_target_pairs={{0,1},{1,2},{2,3},{3,0},{4,5},{5,6},{6,7},{7,4},{8,9},{9,10},{10,1... | collective-permute-start | bytes 786440 | tf_op jit(solution)/shard_map/ppermute | solution.py:56
  94.5 3.6 %collective-permute-start.3 = (bf16[64,2048]{1,0:T(8,128)(2,1)}, bf16[64,2048]{1,0:T(8,128)(2,1)}, u32[]{:S(2)}, u32[]{:S(2)}) collective-permute-start(bf16[64,2048]{1,0:T(8,128)(2,1)} %slice.45), channel_id=1, source_target_pairs={{0,3},{1,0},{2,1},{3,2},{4,7},{5,4},{6,5},{7,6},{8,11},{9,8},{10,9... | collective-permute-start | bytes 786440 | tf_op jit(solution)/shard_map/ppermute | solution.py:57
  98.1 0.7 slice.50
  98.7 0.9 slice.49
  99.7 1.9 collective-permute-start.12
  101.6 5.1 %collective-permute-start.11 = (bf16[8,16,512]{2,1,0:T(8,128)(2,1)S(1)}, bf16[8,16,512]{2,1,0:T(8,128)(2,1)}, u32[]{:S(2)}, u32[]{:S(2)}) collective-permute-start(bf16[8,16,512]{2,1,0:T(8,128)(2,1)S(1)} %slice.49), channel_id=1, source_target_pairs={{0,8},{8,16},{16,24},{24,0},{1,9},{9,17},{17,25},{25,1},{2,10},{10... | collective-permute-start | bytes 393224 | tf_op jit(solution)/shard_map/ppermute | solution.py:56
  106.7 0.6 pad_add_fusion.info_ref
  107.3 0.9 copy.13
  108.2 0.7 slice.53
  108.9 0.7 slice.52
  109.5 1.9 collective-permute-start.18
  111.4 5.1 %collective-permute-start.17 = (bf16[8,16,512]{2,1,0:T(8,128)(2,1)}, bf16[8,16,512]{2,1,0:T(8,128)(2,1)}, u32[]{:S(2)}, u32[]{:S(2)}) collective-permute-start(bf16[8,16,512]{2,1,0:T(8,128)(2,1)} %slice.52), channel_id=1, source_target_pairs={{0,8},{8,16},{16,24},{24,0},{1,9},{9,17},{17,25},{25,1},{2,10},{10... | collective-permute-start | bytes 393224 | tf_op jit(solution)/shard_map/ppermute | solution.py:56
  116.6 7.8 %shard_map.109 = (bf16[512,2048]{1,0:T(8,128)(2,1)}, bf16[512,256]{1,0:T(8,128)(2,1)}, f32[512,256]{1,0:T(8,128)}, f32[512,256]{1,0:T(8,128)}, f32[4,128,256]{2,1,0:T(8,128)}, /*index=5*/f32[128,512]{1,0:T(8,128)}) custom-call(s32[4]{0:T(128)} %pad_add_fusion.info_ref, bf16[128,2048]{1,0:T(8,128)(2,1)} %own_ref.1, bf16[128,2048]{1,0:T(8,128)(2,1)} %copy-done.3, ...), custom_call_target="tpu_custom_call" | custom-call | flops 1073741824 | bytes 8388608 | tf_op jit(solution)/shard_map/pallas_call | solution.py:266
  124.4 2.0 copy.14
  126.4 15.6 %all-to-all-start.1 = ((f32[128,1,512]{2,1,0:T(1,128)}), f32[128,1,512]{2,1,0:T(1,128)S(1)}, u32[]{:S(2)}, u32[]{:S(2)}) async-start(f32[128,1,512]{2,1,0:T(1,128)} %copy.14), calls=%async_computation.1 | async-start | bytes 524288 | tf_op jit(solution)/shard_map/all_to_all | solution.py:348
  142.1 1.0 maximum_bitcast_fusion.1
  143.1 1.2 pad_maximum_fusion.1.mine_ref
  144.2 2.0 collective-permute-start.13
  146.3 1.0 maximum_bitcast_fusion.2
  147.3 0.1 pad_maximum_fusion.2.mine_ref
  147.4 2.3 collective-permute-start.19
  149.8 13.9 %all-to-all-done.1 = f32[128,1,512]{2,1,0:T(1,128)S(1)} async-done(((f32[128,1,512]{2,1,0:T(1,128)}), f32[128,1,512]{2,1,0:T(1,128)S(1)}, u32[]{:S(2)}, u32[]{:S(2)}) %all-to-all-start.1) | async-done | bytes 262176 | tf_op jit(solution)/shard_map/all_to_all | solution.py:348
  163.7 0.7 copy.20
  164.4 1.8 shard_map.110
  166.2 1.7 copy.15
  167.9 7.1 %all-to-all-start.2 = ((f32[128,1,256]{2,1,0:T(1,128)}), f32[128,1,256]{2,1,0:T(1,128)S(1)}, u32[]{:S(2)}, u32[]{:S(2)}) async-start(f32[128,1,256]{2,1,0:T(1,128)} %copy.15), calls=%async_computation.2 | async-start | bytes 262144 | tf_op jit(solution)/shard_map/all_to_all | solution.py:350
  175.0 6.8 %shard_map.111 = (bf16[512,256]{1,0:T(8,128)(2,1)}, f32[512,256]{1,0:T(8,128)}, f32[512,256]{1,0:T(8,128)}) custom-call(s32[4]{0:T(128)} %pad_add_fusion.info_ref, bf16[512,2048]{1,0:T(8,128)(2,1)} %get-tuple-element.17.normed_ref, bf16[4,16,16,512]{3,2,1,0:T(8,128)(2,1)} %copy-done.2, bf16[4,16,16,512]{3,2,1,0:T(8,128)(2,1)} %collective-permute-done.13.other_ref, ...), custom_call_target="tpu_custom_call" | custom-call | flops 1073741824 | bytes 8388608 | tf_op jit(solution)/shard_map/pallas_call | solution.py:266
  181.8 0.7 slice.40
  182.5 2.0 collective-permute-start.14
  184.5 6.6 %all-to-all-done.2 = f32[128,1,256]{2,1,0:T(1,128)S(1)} async-done(((f32[128,1,256]{2,1,0:T(1,128)}), f32[128,1,256]{2,1,0:T(1,128)S(1)}, u32[]{:S(2)}, u32[]{:S(2)}) %all-to-all-start.2) | async-done | bytes 131104 | tf_op jit(solution)/shard_map/all_to_all | solution.py:350
  191.1 0.7 copy.21
  191.8 1.0 copy-done.5
  192.8 0.0 copy-done.9
  192.8 8.0 %shard_map.112 = bf16[512,2048]{1,0:T(8,128)(2,1)} custom-call(s32[4]{0:T(128)} %pad_add_fusion.info_ref, f32[128,256]{1,0:T(8,128)} %bitcast.45, f32[4,128,256]{2,1,0:T(8,128)} %get-tuple-element.15.growth_ref, f32[512,256]{1,0:T(8,128)} %get-tuple-element.16.cum_ref, f32[512,256]{1,0:T(8,128)} %get-tuple-element.20.decayed_ref, ...), custom_call_target="tpu_custom_call" | custom-call | flops 1073741824 | bytes 8388608 | tf_op jit(solution)/shard_map/pallas_call | solution.py:266
  200.8 30.5 %all_to_all.37 = bf16[4,128,2048]{2,1,0:T(8,128)(2,1)S(1)} all-to-all(bf16[4,128,2048]{2,1,0:T(8,128)(2,1)} %bitcast.36), channel_id=1, replica_groups=mesh['sp_0'=16,'sp_1'=4,'sp_2'=2,'tp'=4] {'tp'}, dimensions={0} | all-to-all | bytes 4194304 | tf_op jit(solution)/shard_map/all_to_all | solution.py:385
  231.3 1.3 reduce_sum.12
  (38 shorter events, 0.1 us)
Async XLA Ops:
  1.4 33.6 %all-to-all-start = ((bf16[16,16,512]{2,1,0:T(8,128)(2,1)}), bf16[16,16,512]{2,1,0:T(8,128)(2,1)S(1)}, u32[]{:S(2)}, u32[]{:S(2)}) async-start(bf16[16,16,512]{2,1,0:T(8,128)(2,1)} %broadcast_in_dim.16), calls=%async_computation | async-start | bytes 524288 | tf_op jit(solution)/shard_map/all_to_all | solution.py:46
  35.9 35.5 %all-to-all-start.3 = ((bf16[16,16,1024]{2,1,0:T(8,128)(2,1)}), bf16[16,16,1024]{2,1,0:T(8,128)(2,1)S(1)}, u32[]{:S(2)}, u32[]{:S(2)}) async-start(bf16[16,16,1024]{2,1,0:T(8,128)(2,1)} %broadcast_in_dim.18), calls=%async_computation.3 | async-start | bytes 1048576 | tf_op jit(solution)/shard_map/all_to_all | solution.py:46
  41.7 10.8 %collective-permute-start.5 = (bf16[16,16,512]{2,1,0:T(8,128)(2,1)S(1)}, bf16[16,16,512]{2,1,0:T(8,128)(2,1)S(1)}, u32[]{:S(2)}, u32[]{:S(2)}) collective-permute-start(bf16[16,16,512]{2,1,0:T(8,128)(2,1)S(1)} %all-to-all-done), channel_id=1, source_target_pairs={{0,24},{8,0},{16,8},{24,16},{1,25},{9,1},{17,9},{25,17},{2,26},{10... | collective-permute-start | bytes 786440 | tf_op jit(solution)/shard_map/ppermute | solution.py:55
  44.4 10.0 %collective-permute-start.4 = (bf16[16,16,512]{2,1,0:T(8,128)(2,1)S(1)}, bf16[16,16,512]{2,1,0:T(8,128)(2,1)S(1)}, u32[]{:S(2)}, u32[]{:S(2)}) collective-permute-start(bf16[16,16,512]{2,1,0:T(8,128)(2,1)S(1)} %all-to-all-done), channel_id=1, source_target_pairs={{0,8},{8,16},{16,24},{24,0},{1,9},{9,17},{17,25},{25,1},{2,10},{10... | collective-permute-start | bytes 786440 | tf_op jit(solution)/shard_map/ppermute | solution.py:54
  52.5 8.1 %collective-permute-start.7 = (bf16[8,16,512]{2,1,0:T(8,128)(2,1)S(1)}, bf16[8,16,512]{2,1,0:T(8,128)(2,1)S(1)}, u32[]{:S(2)}, u32[]{:S(2)}) collective-permute-start(bf16[8,16,512]{2,1,0:T(8,128)(2,1)S(1)} %slice.47), channel_id=1, source_target_pairs={{0,24},{8,0},{16,8},{24,16},{1,25},{9,1},{17,9},{25,17},{2,26},{10... | collective-permute-start | bytes 393224 | tf_op jit(solution)/shard_map/ppermute | solution.py:57
  54.4 7.6 %collective-permute-start.6 = (bf16[8,16,512]{2,1,0:T(8,128)(2,1)S(1)}, bf16[8,16,512]{2,1,0:T(8,128)(2,1)S(1)}, u32[]{:S(2)}, u32[]{:S(2)}) collective-permute-start(bf16[8,16,512]{2,1,0:T(8,128)(2,1)S(1)} %slice.46), channel_id=1, source_target_pairs={{0,8},{8,16},{16,24},{24,0},{1,9},{9,17},{17,25},{25,1},{2,10},{10... | collective-permute-start | bytes 393224 | tf_op jit(solution)/shard_map/ppermute | solution.py:56
  62.2 54.3 %copy-start = (bf16[4,16,16,512]{3,2,1,0:T(8,128)(2,1)}, bf16[4,16,16,512]{3,2,1,0:T(8,128)(2,1)S(1)}, u32[]{:S(2)}) copy-start(bf16[4,16,16,512]{3,2,1,0:T(8,128)(2,1)S(1)} %pad_maximum_fusion.mine_ref) | copy-start | bytes 3145732
  62.3 45.1 %copy-start.10 = (f32[2,512]{1,0:T(2,128)S(1)}, f32[2,512]{1,0:T(2,128)}, u32[]{:S(2)}) copy-start(f32[2,512]{1,0:T(2,128)} %param.18) | copy-start | bytes 12292
  62.3 54.3 %collective-permute-start.8 = (bf16[4,16,16,512]{3,2,1,0:T(8,128)(2,1)S(1)}, bf16[4,16,16,512]{3,2,1,0:T(8,128)(2,1)}, u32[]{:S(2)}, u32[]{:S(2)}) collective-permute-start(bf16[4,16,16,512]{3,2,1,0:T(8,128)(2,1)S(1)} %pad_maximum_fusion.mine_ref), channel_id=1, source_target_pairs={{0,4},{4,0},{1,5},{5,1},{2,6},{6,2},{3,7},{7,3},{8,12},{12,8},{9,1... | collective-permute-start | bytes 3145736 | tf_op jit(solution)/shard_map/ppermute | solution.py:287
  64.3 17.7 %collective-permute-start = (bf16[128,2048]{1,0:T(8,128)(2,1)}, bf16[128,2048]{1,0:T(8,128)(2,1)S(1)}, u32[]{:S(2)}, u32[]{:S(2)}) collective-permute-start(bf16[128,2048]{1,0:T(8,128)(2,1)} %own_ref.1), channel_id=1, source_target_pairs={{0,1},{1,2},{2,3},{3,0},{4,5},{5,6},{6,7},{7,4},{8,9},{9,10},{10,1... | collective-permute-start | bytes 1572872 | tf_op jit(solution)/shard_map/ppermute | solution.py:54
  67.8 16.2 %collective-permute-start.1 = (bf16[128,2048]{1,0:T(8,128)(2,1)}, bf16[128,2048]{1,0:T(8,128)(2,1)S(1)}, u32[]{:S(2)}, u32[]{:S(2)}) collective-permute-start(bf16[128,2048]{1,0:T(8,128)(2,1)} %own_ref.1), channel_id=1, source_target_pairs={{0,3},{1,0},{2,1},{3,2},{4,7},{5,4},{6,5},{7,6},{8,11},{9,8},{10,9... | collective-permute-start | bytes 1572872 | tf_op jit(solution)/shard_map/ppermute | solution.py:55
  72.2 18.7 %collective-permute-start.10 = (bf16[16,16,512]{2,1,0:T(8,128)(2,1)S(1)}, bf16[16,16,512]{2,1,0:T(8,128)(2,1)S(1)}, u32[]{:S(2)}, u32[]{:S(2)}) collective-permute-start(bf16[16,16,512]{2,1,0:T(8,128)(2,1)S(1)} %get-tuple-element.26), channel_id=1, source_target_pairs={{0,24},{8,0},{16,8},{24,16},{1,25},{9,1},{17,9},{25,17},{2,26},{10... | collective-permute-start | bytes 786440 | tf_op jit(solution)/shard_map/ppermute | solution.py:55
  74.3 20.2 %collective-permute-start.9 = (bf16[16,16,512]{2,1,0:T(8,128)(2,1)S(1)}, bf16[16,16,512]{2,1,0:T(8,128)(2,1)}, u32[]{:S(2)}, u32[]{:S(2)}) collective-permute-start(bf16[16,16,512]{2,1,0:T(8,128)(2,1)S(1)} %get-tuple-element.26), channel_id=1, source_target_pairs={{0,8},{8,16},{16,24},{24,0},{1,9},{9,17},{17,25},{25,1},{2,10},{10... | collective-permute-start | bytes 786440 | tf_op jit(solution)/shard_map/ppermute | solution.py:54
  82.0 34.6 %copy-start.3 = (bf16[128,2048]{1,0:T(8,128)(2,1)}, bf16[128,2048]{1,0:T(8,128)(2,1)S(1)}, u32[]{:S(2)}) copy-start(bf16[128,2048]{1,0:T(8,128)(2,1)S(1)} %collective-permute-done.before_ref) | copy-start | bytes 1572868
  82.0 17.6 %collective-permute-start.16 = (bf16[16,16,512]{2,1,0:T(8,128)(2,1)}, bf16[16,16,512]{2,1,0:T(8,128)(2,1)S(1)}, u32[]{:S(2)}, u32[]{:S(2)}) collective-permute-start(bf16[16,16,512]{2,1,0:T(8,128)(2,1)} %get-tuple-element.25), channel_id=1, source_target_pairs={{0,24},{8,0},{16,8},{24,16},{1,25},{9,1},{17,9},{25,17},{2,26},{10... | collective-permute-start | bytes 786440 | tf_op jit(solution)/shard_map/ppermute | solution.py:55
  84.0 32.6 %copy-start.4 = (bf16[128,2048]{1,0:T(8,128)(2,1)}, bf16[128,2048]{1,0:T(8,128)(2,1)S(1)}, u32[]{:S(2)}) copy-start(bf16[128,2048]{1,0:T(8,128)(2,1)S(1)} %collective-permute-done.1.after_ref) | copy-start | bytes 1572868
  84.0 17.6 %collective-permute-start.15 = (bf16[16,16,512]{2,1,0:T(8,128)(2,1)}, bf16[16,16,512]{2,1,0:T(8,128)(2,1)S(1)}, u32[]{:S(2)}, u32[]{:S(2)}) collective-permute-start(bf16[16,16,512]{2,1,0:T(8,128)(2,1)} %get-tuple-element.25), channel_id=1, source_target_pairs={{0,8},{8,16},{16,24},{24,0},{1,9},{9,17},{17,25},{25,1},{2,10},{10... | collective-permute-start | bytes 786440 | tf_op jit(solution)/shard_map/ppermute | solution.py:54
  91.0 33.4 %copy-start.8 = (bf16[16,16,512]{2,1,0:T(8,128)(2,1)}, bf16[16,16,512]{2,1,0:T(8,128)(2,1)S(1)}, u32[]{:S(2)}) copy-start(bf16[16,16,512]{2,1,0:T(8,128)(2,1)S(1)} %collective-permute-done.10) | copy-start | bytes 786436
  91.0 18.5 %collective-permute-start.2 = (bf16[64,2048]{1,0:T(8,128)(2,1)}, bf16[64,2048]{1,0:T(8,128)(2,1)}, u32[]{:S(2)}, u32[]{:S(2)}) collective-permute-start(bf16[64,2048]{1,0:T(8,128)(2,1)} %slice.44), channel_id=1, source_target_pairs={{0,1},{1,2},{2,3},{3,0},{4,5},{5,6},{6,7},{7,4},{8,9},{9,10},{10,1... | collective-permute-start | bytes 786440 | tf_op jit(solution)/shard_map/ppermute | solution.py:56
  94.5 17.0 %collective-permute-start.3 = (bf16[64,2048]{1,0:T(8,128)(2,1)}, bf16[64,2048]{1,0:T(8,128)(2,1)}, u32[]{:S(2)}, u32[]{:S(2)}) collective-permute-start(bf16[64,2048]{1,0:T(8,128)(2,1)} %slice.45), channel_id=1, source_target_pairs={{0,3},{1,0},{2,1},{3,2},{4,7},{5,4},{6,5},{7,6},{8,11},{9,8},{10,9... | collective-permute-start | bytes 786440 | tf_op jit(solution)/shard_map/ppermute | solution.py:57
  99.7 42.4 %collective-permute-start.12 = (bf16[8,16,512]{2,1,0:T(8,128)(2,1)}, bf16[8,16,512]{2,1,0:T(8,128)(2,1)}, u32[]{:S(2)}, u32[]{:S(2)}) collective-permute-start(bf16[8,16,512]{2,1,0:T(8,128)(2,1)} %slice.50), channel_id=1, source_target_pairs={{0,24},{8,0},{16,8},{24,16},{1,25},{9,1},{17,9},{25,17},{2,26},{10... | collective-permute-start | bytes 393224 | tf_op jit(solution)/shard_map/ppermute | solution.py:57
  101.6 22.8 %copy-start.6 = (bf16[16,16,512]{2,1,0:T(8,128)(2,1)}, bf16[16,16,512]{2,1,0:T(8,128)(2,1)S(1)}, u32[]{:S(2)}) copy-start(bf16[16,16,512]{2,1,0:T(8,128)(2,1)S(1)} %collective-permute-done.15) | copy-start | bytes 786436
  101.6 40.4 %collective-permute-start.11 = (bf16[8,16,512]{2,1,0:T(8,128)(2,1)S(1)}, bf16[8,16,512]{2,1,0:T(8,128)(2,1)}, u32[]{:S(2)}, u32[]{:S(2)}) collective-permute-start(bf16[8,16,512]{2,1,0:T(8,128)(2,1)S(1)} %slice.49), channel_id=1, source_target_pairs={{0,8},{8,16},{16,24},{24,0},{1,9},{9,17},{17,25},{25,1},{2,10},{10... | collective-permute-start | bytes 393224 | tf_op jit(solution)/shard_map/ppermute | solution.py:56
  109.5 36.8 %collective-permute-start.18 = (bf16[8,16,512]{2,1,0:T(8,128)(2,1)}, bf16[8,16,512]{2,1,0:T(8,128)(2,1)}, u32[]{:S(2)}, u32[]{:S(2)}) collective-permute-start(bf16[8,16,512]{2,1,0:T(8,128)(2,1)} %slice.53), channel_id=1, source_target_pairs={{0,24},{8,0},{16,8},{24,16},{1,25},{9,1},{17,9},{25,17},{2,26},{10... | collective-permute-start | bytes 393224 | tf_op jit(solution)/shard_map/ppermute | solution.py:57
  111.4 34.8 %collective-permute-start.17 = (bf16[8,16,512]{2,1,0:T(8,128)(2,1)}, bf16[8,16,512]{2,1,0:T(8,128)(2,1)}, u32[]{:S(2)}, u32[]{:S(2)}) collective-permute-start(bf16[8,16,512]{2,1,0:T(8,128)(2,1)} %slice.52), channel_id=1, source_target_pairs={{0,8},{8,16},{16,24},{24,0},{1,9},{9,17},{17,25},{25,1},{2,10},{10... | collective-permute-start | bytes 393224 | tf_op jit(solution)/shard_map/ppermute | solution.py:56
  124.4 22.9 %copy-start.7 = (bf16[16,16,512]{2,1,0:T(8,128)(2,1)S(1)}, bf16[16,16,512]{2,1,0:T(8,128)(2,1)}, u32[]{:S(2)}) copy-start(bf16[16,16,512]{2,1,0:T(8,128)(2,1)} %copy-done.6) | copy-start | bytes 786436
  126.4 37.3 %all-to-all-start.1 = ((f32[128,1,512]{2,1,0:T(1,128)}), f32[128,1,512]{2,1,0:T(1,128)S(1)}, u32[]{:S(2)}, u32[]{:S(2)}) async-start(f32[128,1,512]{2,1,0:T(1,128)} %copy.14), calls=%async_computation.1 | async-start | bytes 524288 | tf_op jit(solution)/shard_map/all_to_all | solution.py:348
  144.2 30.8 %copy-start.2 = (bf16[4,16,16,512]{3,2,1,0:T(8,128)(2,1)}, bf16[4,16,16,512]{3,2,1,0:T(8,128)(2,1)S(1)}, u32[]{:S(2)}) copy-start(bf16[4,16,16,512]{3,2,1,0:T(8,128)(2,1)S(1)} %pad_maximum_fusion.1.mine_ref) | copy-start | bytes 3145732
  144.2 30.7 %collective-permute-start.13 = (bf16[4,16,16,512]{3,2,1,0:T(8,128)(2,1)S(1)}, bf16[4,16,16,512]{3,2,1,0:T(8,128)(2,1)}, u32[]{:S(2)}, u32[]{:S(2)}) collective-permute-start(bf16[4,16,16,512]{3,2,1,0:T(8,128)(2,1)S(1)} %pad_maximum_fusion.1.mine_ref), channel_id=1, source_target_pairs={{0,4},{4,0},{1,5},{5,1},{2,6},{6,2},{3,7},{7,3},{8,12},{12,8},{9,1... | collective-permute-start | bytes 3145736 | tf_op jit(solution)/shard_map/ppermute | solution.py:287
  147.4 34.4 %copy-start.1 = (bf16[4,16,16,512]{3,2,1,0:T(8,128)(2,1)}, bf16[4,16,16,512]{3,2,1,0:T(8,128)(2,1)S(1)}, u32[]{:S(2)}) copy-start(bf16[4,16,16,512]{3,2,1,0:T(8,128)(2,1)S(1)} %pad_maximum_fusion.2.mine_ref) | copy-start | bytes 3145732
  147.4 44.3 %collective-permute-start.19 = (bf16[4,16,16,512]{3,2,1,0:T(8,128)(2,1)S(1)}, bf16[4,16,16,512]{3,2,1,0:T(8,128)(2,1)S(1)}, u32[]{:S(2)}, u32[]{:S(2)}) collective-permute-start(bf16[4,16,16,512]{3,2,1,0:T(8,128)(2,1)S(1)} %pad_maximum_fusion.2.mine_ref), channel_id=1, source_target_pairs={{0,4},{4,0},{1,5},{5,1},{2,6},{6,2},{3,7},{7,3},{8,12},{12,8},{9,1... | collective-permute-start | bytes 3145736 | tf_op jit(solution)/shard_map/ppermute | solution.py:287
  167.9 23.3 %all-to-all-start.2 = ((f32[128,1,256]{2,1,0:T(1,128)}), f32[128,1,256]{2,1,0:T(1,128)S(1)}, u32[]{:S(2)}, u32[]{:S(2)}) async-start(f32[128,1,256]{2,1,0:T(1,128)} %copy.15), calls=%async_computation.2 | async-start | bytes 262144 | tf_op jit(solution)/shard_map/all_to_all | solution.py:350
  182.5 9.3 %collective-permute-start.14 = (bf16[16,256]{1,0:T(8,128)(2,1)S(1)}, bf16[16,256]{1,0:T(8,128)(2,1)S(1)}, u32[]{:S(2)}, u32[]{:S(2)}) collective-permute-start(bf16[16,256]{1,0:T(8,128)(2,1)S(1)} %slice.40), channel_id=1, source_target_pairs={{0,4},{4,8},{8,12},{12,16},{16,20},{20,24},{24,28},{28,32},{32,36}... | collective-permute-start | bytes 24584 | tf_op jit(solution)/shard_map/ppermute | solution.py:366
  191.8 1.0 copy-start.5
  191.8 1.0 copy-start.9

commit v2 on v1

--- a/solution.py
+++ b/solution.py
@@ -11,8 +11,11 @@
 RDIM = 128
 CHUNK = 128
 RIM = 16
-SP = ("sp_0", "sp_1", "sp_2")
-SP_TP = ("sp_0", "sp_1", "sp_2", "tp")
+FAR, NEAR, ACROSS, CORE = "sp_f", "sp_n", "sp_x", "sp_c"
+DEPTH = (FAR, NEAR)
+PLANE = (ACROSS, CORE)
+SP = (FAR, NEAR, ACROSS, CORE)
+SP_TP = (FAR, NEAR, ACROSS, CORE, "tp")
 EPSILON = 1e-06
 BF = jnp.bfloat16
 F32 = jnp.float32
@@ -62,21 +65,31 @@
     return [index, lax.rem(index + n - 1, n), lax.rem(index + 1, n), lax.rem(index + 2, n)]
 
 
-def assemble(info_ref, mine_ref, other_ref, whole_ref):
-    core = info_ref[0]
-    nx, nz, rows, _ = mine_ref.shape
-    spots = places(info_ref[3], nx)
-
-    def put(z, carry):
-        for k, spot in enumerate(spots):
-            at = ((z * nx + spot) * 2) * rows
-            here = pl.ds(pl.multiple_of(at + core * rows, rows), rows)
-            there = pl.ds(pl.multiple_of(at + (1 - core) * rows, rows), rows)
-            whole_ref[here, :] = mine_ref[k, z]
-            whole_ref[there, :] = other_ref[k, z]
-        return carry
-
-    lax.fori_loop(0, nz, put, 0)
+def fetches(core, mine_ref, other_ref, lanes, whole_ref, sems):
+    nx, near = mine_ref.shape[:2]
+    copies = []
+    for x in range(nx):
+        for n in range(near):
+            for side, from_ref in enumerate((mine_ref, other_ref)):
+                to = core if side == 0 else 1 - core
+                copies.append(
+                    pltpu.make_async_copy(
+                        from_ref.at[x, n, :, :, lanes],
+                        whole_ref.at[:, n, x, to],
+                        sems.at[len(copies)],
+                    )
+                )
+    return copies
+
+
+def started(copies):
+    for copy in copies:
+        copy.start()
+
+
+def finished(copies):
+    for copy in copies:
+        copy.wait()
 
 
 def state_kernel(
@@ -98,11 +111,13 @@
     growth_ref,
     payload_ref,
     whole_ref,
+    sems,
     both_ref,
 ):
     rows, _ = normed_ref.shape
     cols = gap_ref.shape[1]
-    assemble(info_ref, mine_ref, other_ref, whole_ref)
+    copies = fetches(info_ref[0], mine_ref, other_ref, slice(0, 2 * cols), whole_ref, sems)
+    started(copies)
     block = own_ref.shape[0]
     own, before, after, far = places(info_ref[1], rows // block)
 
@@ -124,7 +139,8 @@
 
     lax.fori_loop(0, block // 32, norm_all, 0)
     lax.fori_loop(0, block // 64, norm_far, 0)
-    both_ref[...] = dot(normed_ref[...], whole_ref[...])
+    finished(copies)
+    both_ref[...] = dot(normed_ref[...], whole_ref[...].reshape(-1, 2 * cols))
     row = lax.broadcasted_iota(jnp.int32, (CHUNK, CHUNK), 0)
     col = lax.broadcasted_iota(jnp.int32, (CHUNK, CHUNK), 1)
     tril = (row >= col).astype(BF)
@@ -159,21 +175,33 @@
     return dot(values, kh, TN) + dot(values, kl, TN)
 
 
-def scan_kernel(got_ref, start_ref):
-    rows, cols = start_ref.shape
-    per = rows // lax.axis_size(SP)
-    state = got_ref[:, :cols]
-    fade = jnp.exp(got_ref[:, cols:])
-    index = lax.broadcasted_iota(jnp.int32, (rows, cols), 0)
-    step = per
-    while step < rows:
-        inside = index >= step
-        before = jnp.where(inside, pltpu.roll(state, step, 0), 0.0)
-        earlier = jnp.where(inside, pltpu.roll(fade, step, 0), 1.0)
-        state = fade * before + state
-        fade = fade * earlier
-        step *= 2
-    start_ref[...] = jnp.where(index >= per, pltpu.roll(state, per, 0), 0.0)
+def plane_kernel(got_ref, before_ref, faded_ref, total_ref):
+    rows = got_ref.shape[1]
+    cols = before_ref.shape[2]
+    state = jnp.zeros((rows, cols), F32)
+    faded = jnp.zeros((1, cols), F32)
+    for d in range(got_ref.shape[0]):
+        fade = got_ref[d, :1, cols:]
+        before_ref[d] = state
+        faded_ref[d : d + 1, :] = faded
+        state = state * jnp.exp(fade) + got_ref[d, :, :cols]
+        faded = faded + fade
+    high = faded.astype(BF).astype(F32)
+    row = lax.broadcasted_iota(jnp.int32, (16, cols), 0)
+    total_ref[:rows, :] = state.astype(BF)
+    total_ref[rows:, :] = jnp.where(row == 0, high, jnp.where(row == 1, faded - high, 0.0)).astype(BF)
+
+
+def depth_kernel(info_ref, totals_ref, before_ref, faded_ref, start_ref):
+    planes = totals_ref.shape[0]
+    devices, rows, cols = before_ref.shape
+    state = jnp.zeros((rows, cols), F32)
+    for z in range(planes):
+        got = totals_ref[z].astype(F32)
+        fade = got[rows : rows + 1] + got[rows + 1 : rows + 2]
+        state = jnp.where(z < info_ref[4], state * jnp.exp(fade) + got[:rows], state)
+    for d in range(devices):
+        start_ref[d] = before_ref[d] + jnp.exp(faded_ref[d : d + 1, :]) * state
 
 
 def inner_kernel(
@@ -188,11 +216,14 @@
     decayed_ref,
     heard_ref,
     whole_ref,
+    sems,
     both_ref,
 ):
     rows, cols = values_ref.shape
-    assemble(info_ref, mine_ref, other_ref, whole_ref)
-    both_ref[...] = dot(normed_ref[...], whole_ref[...])
+    copies = fetches(info_ref[0], mine_ref, other_ref, slice(2 * cols, 4 * cols), whole_ref, sems)
+    started(copies)
+    finished(copies)
+    both_ref[...] = dot(normed_ref[...], whole_ref[...].reshape(-1, 2 * cols))
     pooled_ref[...] = both_ref[:, cols:].astype(BF)
     row = lax.broadcasted_iota(jnp.int32, (CHUNK, CHUNK), 0)
     col = lax.broadcasted_iota(jnp.int32, (CHUNK, CHUNK), 1)
@@ -222,10 +253,12 @@
     other_ref,
     part_ref,
     whole_ref,
+    sems,
     mixed_ref,
 ):
     rows, cols = cum_ref.shape
-    assemble(info_ref, mine_ref, other_ref, whole_ref)
+    copies = fetches(info_ref[0], mine_ref, other_ref, slice(0, 2 * cols), whole_ref, sems)
+    started(copies)
     group = info_ref[1]
     padded = jnp.concatenate([rim_ref[...], pooled_ref[...]], axis=0).astype(F32)
     running = padded
@@ -250,23 +283,24 @@
             total = cum_ref[(c + 1) * CHUNK - 1 : (c + 1) * CHUNK, lanes]
             state = state * jnp.exp(total) + growth_ref[c, :, lanes]
 
-    def out(i, carry):
-        at = pl.ds(pl.multiple_of(i * 256, 256), 256)
-        part_ref[:, at] = dot(mixed_ref[...], whole_ref[at, :], NT).astype(BF)
-        return carry
-
-    lax.fori_loop(0, part_ref.shape[1] // 256, out, 0)
+    finished(copies)
+    far = whole_ref.shape[0]
+    step = part_ref.shape[1] // far
+    for f in range(far):
+        weight = whole_ref[f].reshape(step, 2 * cols)
+        part_ref[:, f * step : (f + 1) * step] = dot(mixed_ref[...], weight, NT).astype(BF)
 
 
 VMEM = pl.BlockSpec(memory_space=pltpu.VMEM)
 SMEM = pl.BlockSpec(memory_space=pltpu.SMEM)
+HBM = pl.BlockSpec(memory_space=pltpu.HBM)
 
 
 def call(kernel, outs, scratch, flops, moved, *args):
     return pl.pallas_call(
         kernel,
         out_shape=outs,
-        in_specs=[SMEM if a.dtype == jnp.int32 else VMEM for a in args],
+        in_specs=[SMEM if a.dtype == jnp.int32 else HBM if a.ndim == 5 else VMEM for a in args],
         out_specs=jax.tree.map(lambda _: VMEM, outs),
         scratch_shapes=scratch,
         cost_estimate=pl.CostEstimate(flops=flops, bytes_accessed=moved, transcendentals=0),
@@ -277,14 +311,18 @@
     return jax.ShapeDtypeStruct(dims, dtype)
 
 
-def stacked(pieces):
-    own, before, after, low, high = pieces
-    far = jnp.concatenate([low, high], axis=0)
-    return jnp.stack([own, before, after, far])
+def side_by_side(*arrays):
+    width = sum(a.shape[1] for a in arrays)
+    total, at = None, 0
+    for a in arrays:
+        padded = jnp.pad(a, ((0, 0), (at, width - at - a.shape[1])))
+        total = padded if total is None else total + padded
+        at += a.shape[1]
+    return total
 
 
 def over_cores(x):
-    return lax.ppermute(x, "sp_2", [(0, 1), (1, 0)])
+    return lax.ppermute(x, CORE, [(0, 1), (1, 0)])
 
 
 def layer(
@@ -305,23 +343,36 @@
     tp = lax.axis_size("tp")
     rows = tokens.shape[0] * tp
     devices = lax.axis_size(SP)
-    core = lax.axis_index("sp_2")
-    group = lax.axis_index("tp")
-    info = jnp.stack([core, group, lax.axis_index(SP) * rows, lax.axis_index("sp_1")]).astype(jnp.int32)
+    info = jnp.stack(
+        [
+            lax.axis_index(CORE),
+            lax.axis_index("tp"),
+            lax.axis_index(SP) * rows,
+            lax.axis_index(ACROSS),
+            lax.axis_index(DEPTH),
+        ]
+    ).astype(jnp.int32)
 
     pieces = ring_gather(tokens, "tp")
-    first = jnp.concatenate([forget_weight, input_weight], axis=1)
-    second = jnp.concatenate(
-        [query_weight, pool_in_weight, pool_out_weight.T, recur_out_weight.T], axis=1
-    )
-    first_z = sent_to_all(first, "sp_0")
-    second_z = sent_to_all(second, "sp_0")
-    first_zx = stacked(ring_gather(first_z, "sp_1"))
-    first_other = over_cores(first_zx)
-    in_zx = stacked(ring_gather(second_z[..., : 2 * cols], "sp_1"))
-    in_other = over_cores(in_zx)
-    out_zx = stacked(ring_gather(second_z[..., 2 * cols :], "sp_1"))
-    out_other = over_cores(out_zx)
+    weights = side_by_side(
+        forget_weight,
+        input_weight,
+        query_weight,
+        pool_in_weight,
+        pool_out_weight.T,
+        recur_out_weight.T,
+    )
+    weights = sent_to_all(weights, FAR)
+    weights = sent_to_all(weights, NEAR)
+    inner = sent_to_all(weights[..., : 4 * cols], ACROSS)
+    inner_other = over_cores(inner)
+    outer = sent_to_all(weights[..., 4 * cols :], ACROSS)
+    outer_other = over_cores(outer)
+    blocks = outer.shape[2], outer.shape[1], outer.shape[0], 2, outer.shape[3], 2 * cols
+    whole = [
+        pltpu.VMEM(blocks, BF),
+        pltpu.SemaphoreType.DMA((2 * outer.shape[0] * outer.shape[1],)),
+    ]
 
     normed, values, opened, cum, growth, payload = call(
         state_kernel,
@@ -333,31 +384,58 @@
             shape((rows // CHUNK, RDIM, cols), F32),
             shape((RDIM, 2 * cols), F32),
         ],
-        [pltpu.VMEM((width, 2 * cols), BF), pltpu.VMEM((rows, 2 * cols), F32)],
+        [*whole, pltpu.VMEM((rows, 2 * cols), F32)],
         4 * rows * width * cols,
         8 << 20,
         info,
         *pieces,
         norm_gain[None, :],
-        first_zx,
-        first_other,
+        inner,
+        inner_other,
         forget_gap[None, :],
         decay_shift.T,
     )
 
-    got = lax.all_to_all(payload, SP, split_axis=0, concat_axis=0, tiled=True)
-    start = call(scan_kernel, shape((RDIM, cols), F32), [], 1 << 22, 1 << 20, got)
-    start = lax.all_to_all(start, SP, split_axis=0, concat_axis=0, tiled=True)
+    plane = lax.axis_size(PLANE)
+    slab = RDIM // plane
+    got = lax.all_to_all(payload, PLANE, split_axis=0, concat_axis=0, tiled=True)
+    before, faded, total = call(
+        plane_kernel,
+        [
+            shape((plane, slab, cols), F32),
+            shape((plane, cols), F32),
+            shape((slab + 16, cols), BF),
+        ],
+        [],
+        1 << 20,
+        1 << 19,
+        got.reshape(plane, slab, 2 * cols),
+    )
+    totals = sent_to_all(total, DEPTH)
+    start = call(
+        depth_kernel,
+        shape((plane, slab, cols), F32),
+        [],
+        1 << 20,
+        1 << 19,
+        info,
+        totals,
+        before,
+        faded,
+    )
+    start = lax.all_to_all(
+        start.reshape(RDIM, cols), PLANE, split_axis=0, concat_axis=0, tiled=True
+    )
     pooled, decayed, heard = call(
         inner_kernel,
         [shape((rows, cols), BF), shape((rows, cols), F32), shape((rows, cols), F32)],
-        [pltpu.VMEM((width, 2 * cols), BF), pltpu.VMEM((rows, 2 * cols), F32)],
+        [*whole, pltpu.VMEM((rows, 2 * cols), F32)],
         4 * rows * width * cols,
         8 << 20,
         info,
         normed,
-        in_zx,
-        in_other,
+        inner,
+        inner_other,
         values,
         opened,
         cum,
@@ -367,7 +445,7 @@
     part = call(
         final_kernel,
         shape((rows, width), BF),
-        [pltpu.VMEM((width, 2 * cols), BF), pltpu.VMEM((rows, 2 * cols), BF)],
+        [*whole, pltpu.VMEM((rows, 2 * cols), BF)],
         4 * rows * width * cols,
         8 << 20,
         info,
@@ -379,8 +457,8 @@
         pooled,
         rim,
         out_gain[None, :],
-        out_zx,
-        out_other,
+        outer,
+        outer_other,
     )
     parts = lax.all_to_all(
         part.reshape(tp, rows // tp, width), "tp", split_axis=0, concat_axis=0, tiled=True
@@ -389,7 +467,7 @@
 
 
 def solution(mesh):
-    split = Mesh(mesh.devices.reshape(16, 4, 2, mesh.shape["tp"]), ("sp_0", "sp_1", "sp_2", "tp"))
+    split = Mesh(mesh.devices.reshape(4, 4, 4, 2, mesh.shape["tp"]), SP_TP)
     in_specs = (
         P(SP_TP, None),
         P(),

time: 234 us -> 242 us (1.034)
  blocking collectives: 30.5 us -> 113 us
  starting transfers between devices: 109 us -> 40.9 us
  local copies, waits for them, and re-layouts: 14.4 us -> 8.79 us
  other arithmetic: 6.79 us -> 2.09 us
  waiting for transfers between devices: 46.8 us -> 49.5 us
    all_to_all x0 -> x3, blocking collectives: none -> 82.4 us  [sent_to_all(): return lax.all_to_all(copies, axis, split_axis=0, concat_axis=0, tiled=True)]
    ppermute x4 -> x1, starting transfers between devices: 18.9 us -> 2.19 us  [ring_gather(): far_low = lax.ppermute(before[:half], axis, up)]
    ppermute x4 -> x1, starting transfers between devices: 18.8 us -> 3.48 us  [ring_gather(): before = lax.ppermute(x, axis, up)]
    all_to_all x2, waiting for transfers between devices: 20.5 us -> 5.4 us  [the longest x1 5.4 us: layer(): lax.all_to_all(payload, PLANE, split_axis=0, concat_axis=0, tiled=True)]
    all_to_all x2, starting transfers between devices: 22.7 us -> 10.8 us  [the longest x1 5.43 us: layer(): lax.all_to_all(payload, PLANE, split_axis=0, concat_axis=0, tiled=True)]
    all_to_all x2, starting transfers between devices: 21 us -> 10.2 us  [sent_to_all(): return lax.all_to_all(copies, axis, split_axis=0, concat_axis=0, tiled=True)]
    all_to_all x2, waiting for transfers between devices: 17.6 us -> 26.8 us  [sent_to_all(): return lax.all_to_all(copies, axis, split_axis=0, concat_axis=0, tiled=True)]
    ppermute x4 -> x1, waiting for transfers between devices: 2.32 us -> 10.4 us  [ring_gather(): before = lax.ppermute(x, axis, up)]
  transfers between devices with their start and end apart: 24 -> 11, of which waited for: 7 -> 7; matrix products, arithmetic and copies ran while one was open for 7% -> 2% of each run, Pallas kernels for 7% -> 5%
where the time goes in v2:
time: 242 us; the launch traced here: 240 us
  blocking collectives  113 us (47%)
  waiting for transfers between devices  49.5 us (20%)
  starting transfers between devices  40.9 us (17%)
  Pallas kernels  25.4 us (10%)
  local copies, waits for them, and re-layouts  8.79 us (4%)
    all_to_all x3, blocking collectives, sent_to_all(): return lax.all_to_all(copies, axis, split_axis=0, concat_axis=0, tiled=True)  82.4 us
    all_to_all x1, blocking collectives, layer(): lax.all_to_all(part.reshape(tp, rows // tp, width), 'tp', split_axis=0, c...  30.9 us
    all_to_all x2, waiting for transfers between devices, sent_to_all(): return lax.all_to_all(copies, axis, split_axis=0, concat_axis=0, tiled=True)  26.8 us
    pallas_call x5, Pallas kernels, call(): pl.pallas_call(kernel, out_shape=outs, in_specs=[SMEM if a.dtype == jnp.i...  25.4 us
    ppermute x1, waiting for transfers between devices, ring_gather(): before = lax.ppermute(x, axis, up)  10.4 us
    all_to_all x2, starting transfers between devices, sent_to_all(): return lax.all_to_all(copies, axis, split_axis=0, concat_axis=0, tiled=True)  10.2 us
    all_to_all x1, starting transfers between devices, layer(): lax.all_to_all(payload, PLANE, split_axis=0, concat_axis=0, tiled=True)  5.43 us
    all_to_all x1, waiting for transfers between devices, layer(): lax.all_to_all(payload, PLANE, split_axis=0, concat_axis=0, tiled=True)  5.4 us
  transfers between devices with their start and end apart: 11, of which 7 were waited for; matrix products, arithmetic and copies ran while one was open for 2% of the time, Pallas kernels for 5%

profile of v2, /device:TPU:6, one launch (start us, length us, event | category | flops | bytes accessed | tf_op | source)
XLA Modules:
  0.0 240.2 jit_solution(7608856897141819965)
XLA Ops:
  0.0 0.8 pad_add_fusion
  0.8 31.8 %all_to_all.47 = bf16[4,16,1536]{2,1,0:T(8,128)(2,1)S(1)} all-to-all(bf16[4,16,1536]{2,1,0:T(8,128)(2,1)S(1)} %broadcast_in_dim.25), channel_id=1, replica_groups=mesh['sp_f'=4,'sp_n'=4,'sp_x'=4,'sp_c'=2,'tp'=4] {'sp_f'}, dimensions={0} | all-to-all | bytes 393216 | tf_op jit(solution)/shard_map/all_to_all | solution.py:49
  32.6 0.1 broadcast_in_dim.26
  32.7 22.9 %all_to_all.48 = bf16[4,4,16,1536]{3,2,1,0:T(8,128)(2,1)S(1)} all-to-all(bf16[4,4,16,1536]{3,2,1,0:T(8,128)(2,1)S(1)} %broadcast_in_dim.26), channel_id=1, replica_groups=mesh['sp_f'=4,'sp_n'=4,'sp_x'=4,'sp_c'=2,'tp'=4] {'sp_n'}, dimensions={0} | all-to-all | bytes 1572864 | tf_op jit(solution)/shard_map/all_to_all | solution.py:49
  55.6 0.1 slice.22
  55.7 0.3 broadcast_in_dim.27
  55.9 0.0 copy-start.7
  55.9 0.0 copy-start.10
  56.0 27.6 %all_to_all.49.mine_ref = bf16[4,4,4,16,1024]{4,3,2,1,0:T(8,128)(2,1)S(1)} all-to-all(bf16[4,4,4,16,1024]{4,3,2,1,0:T(8,128)(2,1)S(1)} %broadcast_in_dim.27), channel_id=1, replica_groups=mesh['sp_f'=4,'sp_n'=4,'sp_x'=4,'sp_c'=2,'tp'=4] {'sp_x'}, dimensions={0} | all-to-all | bytes 4194304 | tf_op jit(solution)/shard_map/all_to_all | solution.py:49
  83.6 0.0 copy-start
  83.6 1.9 collective-permute-start.4
  85.5 0.0 copy-done.7
  85.5 3.5 %collective-permute-start = (bf16[128,2048]{1,0:T(8,128)(2,1)S(1)}, bf16[128,2048]{1,0:T(8,128)(2,1)S(1)}, u32[]{:S(2)}, u32[]{:S(2)}) collective-permute-start(bf16[128,2048]{1,0:T(8,128)(2,1)S(1)} %copy-done.7), channel_id=1, source_target_pairs={{0,1},{1,2},{2,3},{3,0},{4,5},{5,6},{6,7},{7,4},{8,9},{9,10},{10,1... | collective-permute-start | bytes 1572872 | tf_op jit(solution)/shard_map/ppermute | solution.py:57
  89.0 3.6 %collective-permute-start.1 = (bf16[128,2048]{1,0:T(8,128)(2,1)S(1)}, bf16[128,2048]{1,0:T(8,128)(2,1)S(1)}, u32[]{:S(2)}, u32[]{:S(2)}) collective-permute-start(bf16[128,2048]{1,0:T(8,128)(2,1)S(1)} %copy-done.7), channel_id=1, source_target_pairs={{0,3},{1,0},{2,1},{3,2},{4,7},{5,4},{6,5},{7,6},{8,11},{9,8},{10,9... | collective-permute-start | bytes 1572872 | tf_op jit(solution)/shard_map/ppermute | solution.py:58
  92.6 10.4 %collective-permute-done.before_ref = bf16[128,2048]{1,0:T(8,128)(2,1)S(1)} collective-permute-done((bf16[128,2048]{1,0:T(8,128)(2,1)S(1)}, bf16[128,2048]{1,0:T(8,128)(2,1)S(1)}, u32[]{:S(2)}, u32[]{:S(2)}) %collective-permute-start) | collective-permute-done | bytes 524320 | tf_op jit(solution)/shard_map/ppermute | solution.py:57
  103.0 0.0 copy-start.2
  103.0 0.8 slice.20
  103.8 2.2 collective-permute-start.2
  106.0 0.0 collective-permute-done.1.after_ref
  106.0 0.0 copy-start.3
  106.0 0.8 copy-done.3
  106.8 0.7 slice.21
  107.5 4.8 %collective-permute-start.3 = (bf16[64,2048]{1,0:T(8,128)(2,1)}, bf16[64,2048]{1,0:T(8,128)(2,1)}, u32[]{:S(2)}, u32[]{:S(2)}) collective-permute-start(bf16[64,2048]{1,0:T(8,128)(2,1)} %slice.21), channel_id=1, source_target_pairs={{0,3},{1,0},{2,1},{3,2},{4,7},{5,4},{6,5},{7,6},{8,11},{9,8},{10,9... | collective-permute-start | bytes 786440 | tf_op jit(solution)/shard_map/ppermute | solution.py:60
  112.4 0.0 copy-done.10
  112.4 0.9 copy.12
  113.3 0.6 stack.23.info_ref
  113.9 1.2 collective-permute-done.2.low_ref
  115.1 2.7 %collective-permute-done.3.high_ref = bf16[64,2048]{1,0:T(8,128)(2,1)} collective-permute-done((bf16[64,2048]{1,0:T(8,128)(2,1)}, bf16[64,2048]{1,0:T(8,128)(2,1)}, u32[]{:S(2)}, u32[]{:S(2)}) %collective-permute-start.3) | collective-permute-done | bytes 262176 | tf_op jit(solution)/shard_map/ppermute | solution.py:60
  117.8 0.0 collective-permute-done.4.other_ref
  117.8 0.0 copy-done
  117.8 0.0 copy-done.2
  117.8 7.8 %shard_map.109 = (bf16[512,2048]{1,0:T(8,128)(2,1)}, bf16[512,256]{1,0:T(8,128)(2,1)}, f32[512,256]{1,0:T(8,128)}, f32[512,256]{1,0:T(8,128)}, f32[4,128,256]{2,1,0:T(8,128)}, /*index=5*/f32[128,512]{1,0:T(8,128)}) custom-call(s32[5]{0:T(128)} %stack.23.info_ref, bf16[128,2048]{1,0:T(8,128)(2,1)} %own_ref.1, bf16[128,2048]{1,0:T(8,128)(2,1)} %copy-done.2, ...), custom_call_target="tpu_custom_call" | custom-call | flops 1073741824 | bytes 8388608 | tf_op jit(solution)/shard_map/pallas_call | solution.py:300
  125.6 5.4 %all-to-all-start.3 = ((f32[8,16,512]{2,1,0:T(8,128)}), f32[8,16,512]{2,1,0:T(8,128)S(1)}, u32[]{:S(2)}, u32[]{:S(2)}) async-start(f32[8,16,512]{2,1,0:T(8,128)} %bitcast.17), calls=%async_computation.3 | async-start | bytes 524288 | tf_op jit(solution)/shard_map/all_to_all | solution.py:401
  131.0 5.4 %all-to-all-done.3.got_ref = f32[8,16,512]{2,1,0:T(8,128)S(1)} async-done(((f32[8,16,512]{2,1,0:T(8,128)}), f32[8,16,512]{2,1,0:T(8,128)S(1)}, u32[]{:S(2)}, u32[]{:S(2)}) %all-to-all-start.3) | async-done | bytes 262176 | tf_op jit(solution)/shard_map/all_to_all | solution.py:401
  136.4 0.0 copy-start.5
  136.4 1.1 broadcast_in_dim.31
  137.5 5.6 %all-to-all-start.6 = ((bf16[4,4,4,16,512]{4,3,2,1,0:T(8,128)(2,1)}), bf16[4,4,4,16,512]{4,3,2,1,0:T(8,128)(2,1)S(1)}, u32[]{:S(2)}, u32[]{:S(2)}) async-start(bf16[4,4,4,16,512]{4,3,2,1,0:T(8,128)(2,1)} %broadcast_in_dim.31), calls=%async_computation.6 | async-start | bytes 2097152 | tf_op jit(solution)/shard_map/all_to_all | solution.py:49
  143.1 0.0 copy-done.5
  143.1 1.6 shard_map.110
  144.7 11.3 %all-to-all-done.6.mine_ref = bf16[4,4,4,16,512]{4,3,2,1,0:T(8,128)(2,1)S(1)} async-done(((bf16[4,4,4,16,512]{4,3,2,1,0:T(8,128)(2,1)}), bf16[4,4,4,16,512]{4,3,2,1,0:T(8,128)(2,1)S(1)}, u32[]{:S(2)}, u32[]{:S(2)}) %all-to-all-start.6) | async-done | bytes 1048608 | tf_op jit(solution)/shard_map/all_to_all | solution.py:49
  156.0 0.0 copy-start.1
  156.0 1.4 broadcast_in_dim.29
  157.5 4.6 %all-to-all-start.4 = ((bf16[16,32,256]{2,1,0:T(8,128)(2,1)}), bf16[16,32,256]{2,1,0:T(8,128)(2,1)S(1)}, u32[]{:S(2)}, u32[]{:S(2)}) async-start(bf16[16,32,256]{2,1,0:T(8,128)(2,1)} %broadcast_in_dim.29), calls=%async_computation.4 | async-start | bytes 524288 | tf_op jit(solution)/shard_map/all_to_all | solution.py:49
  162.1 1.9 collective-permute-start.6
  164.0 15.5 %all-to-all-done.4.totals_ref = bf16[16,32,256]{2,1,0:T(8,128)(2,1)S(1)} async-done(((bf16[16,32,256]{2,1,0:T(8,128)(2,1)}), bf16[16,32,256]{2,1,0:T(8,128)(2,1)S(1)}, u32[]{:S(2)}, u32[]{:S(2)}) %all-to-all-start.4) | async-done | bytes 262176 | tf_op jit(solution)/shard_map/all_to_all | solution.py:49
  179.6 0.0 copy-start.4
  179.6 0.7 copy-done.4
  180.3 1.8 shard_map.111
  182.0 5.4 %all-to-all-start.5 = ((f32[8,16,256]{2,1,0:T(8,128)}), f32[8,16,256]{2,1,0:T(8,128)S(1)}, u32[]{:S(2)}, u32[]{:S(2)}) async-start(f32[8,16,256]{2,1,0:T(8,128)} %shard_map.111), calls=%async_computation.5 | async-start | bytes 262144 | tf_op jit(solution)/shard_map/all_to_all | solution.py:426
  187.4 7.8 %shard_map.112 = (bf16[512,256]{1,0:T(8,128)(2,1)}, f32[512,256]{1,0:T(8,128)}, f32[512,256]{1,0:T(8,128)}) custom-call(s32[5]{0:T(128)} %stack.23.info_ref, bf16[512,2048]{1,0:T(8,128)(2,1)} %get-tuple-element.23.normed_ref, bf16[4,4,4,16,1024]{4,3,2,1,0:T(8,128)(2,1)} %copy-done, bf16[4,4,4,16,1024]{4,3,2,1,0:T(8,128)(2,1)} %collective-permute-done.4.other_ref, ...), custom_call_target="tpu_custom_call" | custom-call | flops 1073741824 | bytes 8388608 | tf_op jit(solution)/shard_map/pallas_call | solution.py:300
  195.2 0.0 copy-done.1
  195.2 0.7 slice.18
  195.9 2.0 collective-permute-start.5
  197.9 0.0 collective-permute-done.6.other_ref
  198.0 0.0 copy-start.6
  198.0 2.9 %collective-permute-done.5.rim_ref = bf16[16,256]{1,0:T(8,128)(2,1)S(1)} collective-permute-done((bf16[16,256]{1,0:T(8,128)(2,1)S(1)}, bf16[16,256]{1,0:T(8,128)(2,1)S(1)}, u32[]{:S(2)}, u32[]{:S(2)}) %collective-permute-start.5) | collective-permute-done | bytes 8224 | tf_op jit(solution)/shard_map/ppermute | solution.py:444
  200.9 0.0 copy-start.9
  200.9 0.0 all-to-all-done.5
  200.9 0.0 copy-done.6
  200.9 0.6 copy-done.9
  201.5 0.1 copy-done.8
  201.5 6.5 %shard_map.113 = bf16[512,2048]{1,0:T(8,128)(2,1)} custom-call(s32[5]{0:T(128)} %stack.23.info_ref, f32[128,256]{1,0:T(8,128)} %bitcast.16, f32[4,128,256]{2,1,0:T(8,128)} %get-tuple-element.21.growth_ref, f32[512,256]{1,0:T(8,128)} %get-tuple-element.22.cum_ref, f32[512,256]{1,0:T(8,128)} %get-tuple-element.26.decayed_ref, ...), custom_call_target="tpu_custom_call" | custom-call | flops 1073741824 | bytes 8388608 | tf_op jit(solution)/shard_map/pallas_call | solution.py:300
  208.0 30.9 %all_to_all.50 = bf16[4,128,2048]{2,1,0:T(8,128)(2,1)S(1)} all-to-all(bf16[4,128,2048]{2,1,0:T(8,128)(2,1)} %bitcast.14), channel_id=1, replica_groups=mesh['sp_f'=4,'sp_n'=4,'sp_x'=4,'sp_c'=2,'tp'=4] {'tp'}, dimensions={0} | all-to-all | bytes 4194304 | tf_op jit(solution)/shard_map/all_to_all | solution.py:463
  238.9 1.3 reduce_sum.12
  (3 shorter events, 0.0 us)
Async XLA Ops:
  55.9 29.6 %copy-start.7 = (bf16[128,2048]{1,0:T(8,128)(2,1)S(1)}, bf16[128,2048]{1,0:T(8,128)(2,1)}, u32[]{:S(2)}) copy-start(bf16[128,2048]{1,0:T(8,128)(2,1)} %own_ref.1) | copy-start | bytes 1572868
  55.9 56.4 %copy-start.10 = (f32[2,512]{1,0:T(2,128)S(1)}, f32[2,512]{1,0:T(2,128)}, u32[]{:S(2)}) copy-start(f32[2,512]{1,0:T(2,128)} %param.18) | copy-start | bytes 12292
  83.6 34.2 %copy-start = (bf16[4,4,4,16,1024]{4,3,2,1,0:T(8,128)(2,1)}, bf16[4,4,4,16,1024]{4,3,2,1,0:T(8,128)(2,1)S(1)}, u32[]{:S(2)}) copy-start(bf16[4,4,4,16,1024]{4,3,2,1,0:T(8,128)(2,1)S(1)} %all_to_all.49.mine_ref) | copy-start | bytes 6291460
  83.6 34.2 %collective-permute-start.4 = (bf16[4,4,4,16,1024]{4,3,2,1,0:T(8,128)(2,1)S(1)}, bf16[4,4,4,16,1024]{4,3,2,1,0:T(8,128)(2,1)}, u32[]{:S(2)}, u32[]{:S(2)}) collective-permute-start(bf16[4,4,4,16,1024]{4,3,2,1,0:T(8,128)(2,1)S(1)} %all_to_all.49.mine_ref), channel_id=1, source_target_pairs={{0,4},{4,0},{1,5},{5,1},{2,6},{6,2},{3,7},{7,3},{8,12},{12,8},{9,1... | collective-permute-start | bytes 6291464 | tf_op jit(solution)/shard_map/ppermute | solution.py:325
  85.5 17.5 %collective-permute-start = (bf16[128,2048]{1,0:T(8,128)(2,1)S(1)}, bf16[128,2048]{1,0:T(8,128)(2,1)S(1)}, u32[]{:S(2)}, u32[]{:S(2)}) collective-permute-start(bf16[128,2048]{1,0:T(8,128)(2,1)S(1)} %copy-done.7), channel_id=1, source_target_pairs={{0,1},{1,2},{2,3},{3,0},{4,5},{5,6},{6,7},{7,4},{8,9},{9,10},{10,1... | collective-permute-start | bytes 1572872 | tf_op jit(solution)/shard_map/ppermute | solution.py:57
  89.0 17.0 %collective-permute-start.1 = (bf16[128,2048]{1,0:T(8,128)(2,1)S(1)}, bf16[128,2048]{1,0:T(8,128)(2,1)S(1)}, u32[]{:S(2)}, u32[]{:S(2)}) collective-permute-start(bf16[128,2048]{1,0:T(8,128)(2,1)S(1)} %copy-done.7), channel_id=1, source_target_pairs={{0,3},{1,0},{2,1},{3,2},{4,7},{5,4},{6,5},{7,6},{8,11},{9,8},{10,9... | collective-permute-start | bytes 1572872 | tf_op jit(solution)/shard_map/ppermute | solution.py:58
  103.0 14.8 %copy-start.2 = (bf16[128,2048]{1,0:T(8,128)(2,1)}, bf16[128,2048]{1,0:T(8,128)(2,1)S(1)}, u32[]{:S(2)}) copy-start(bf16[128,2048]{1,0:T(8,128)(2,1)S(1)} %collective-permute-done.before_ref) | copy-start | bytes 1572868
  103.8 11.3 %collective-permute-start.2 = (bf16[64,2048]{1,0:T(8,128)(2,1)}, bf16[64,2048]{1,0:T(8,128)(2,1)}, u32[]{:S(2)}, u32[]{:S(2)}) collective-permute-start(bf16[64,2048]{1,0:T(8,128)(2,1)} %slice.20), channel_id=1, source_target_pairs={{0,1},{1,2},{2,3},{3,0},{4,5},{5,6},{6,7},{7,4},{8,9},{9,10},{10,1... | collective-permute-start | bytes 786440 | tf_op jit(solution)/shard_map/ppermute | solution.py:59
  106.0 0.8 copy-start.3
  107.5 10.3 %collective-permute-start.3 = (bf16[64,2048]{1,0:T(8,128)(2,1)}, bf16[64,2048]{1,0:T(8,128)(2,1)}, u32[]{:S(2)}, u32[]{:S(2)}) collective-permute-start(bf16[64,2048]{1,0:T(8,128)(2,1)} %slice.21), channel_id=1, source_target_pairs={{0,3},{1,0},{2,1},{3,2},{4,7},{5,4},{6,5},{7,6},{8,11},{9,8},{10,9... | collective-permute-start | bytes 786440 | tf_op jit(solution)/shard_map/ppermute | solution.py:60
  125.6 10.8 %all-to-all-start.3 = ((f32[8,16,512]{2,1,0:T(8,128)}), f32[8,16,512]{2,1,0:T(8,128)S(1)}, u32[]{:S(2)}, u32[]{:S(2)}) async-start(f32[8,16,512]{2,1,0:T(8,128)} %bitcast.17), calls=%async_computation.3 | async-start | bytes 524288 | tf_op jit(solution)/shard_map/all_to_all | solution.py:401
  136.4 6.7 %copy-start.5 = (f32[8,16,512]{2,1,0:T(8,128)}, f32[8,16,512]{2,1,0:T(8,128)S(1)}, u32[]{:S(2)}) copy-start(f32[8,16,512]{2,1,0:T(8,128)S(1)} %all-to-all-done.3.got_ref) | copy-start | bytes 786436
  137.5 18.5 %all-to-all-start.6 = ((bf16[4,4,4,16,512]{4,3,2,1,0:T(8,128)(2,1)}), bf16[4,4,4,16,512]{4,3,2,1,0:T(8,128)(2,1)S(1)}, u32[]{:S(2)}, u32[]{:S(2)}) async-start(bf16[4,4,4,16,512]{4,3,2,1,0:T(8,128)(2,1)} %broadcast_in_dim.31), calls=%async_computation.6 | async-start | bytes 2097152 | tf_op jit(solution)/shard_map/all_to_all | solution.py:49
  156.0 39.2 %copy-start.1 = (bf16[4,4,4,16,512]{4,3,2,1,0:T(8,128)(2,1)}, bf16[4,4,4,16,512]{4,3,2,1,0:T(8,128)(2,1)S(1)}, u32[]{:S(2)}) copy-start(bf16[4,4,4,16,512]{4,3,2,1,0:T(8,128)(2,1)S(1)} %all-to-all-done.6.mine_ref) | copy-start | bytes 3145732
  157.5 22.1 %all-to-all-start.4 = ((bf16[16,32,256]{2,1,0:T(8,128)(2,1)}), bf16[16,32,256]{2,1,0:T(8,128)(2,1)S(1)}, u32[]{:S(2)}, u32[]{:S(2)}) async-start(bf16[16,32,256]{2,1,0:T(8,128)(2,1)} %broadcast_in_dim.29), calls=%async_computation.4 | async-start | bytes 524288 | tf_op jit(solution)/shard_map/all_to_all | solution.py:49
  162.1 35.9 %collective-permute-start.6 = (bf16[4,4,4,16,512]{4,3,2,1,0:T(8,128)(2,1)S(1)}, bf16[4,4,4,16,512]{4,3,2,1,0:T(8,128)(2,1)S(1)}, u32[]{:S(2)}, u32[]{:S(2)}) collective-permute-start(bf16[4,4,4,16,512]{4,3,2,1,0:T(8,128)(2,1)S(1)} %all-to-all-done.6.mine_ref), channel_id=1, source_target_pairs={{0,4},{4,0},{1,5},{5,1},{2,6},{6,2},{3,7},{7,3},{8,12},{12,8},{9,1... | collective-permute-start | bytes 3145736 | tf_op jit(solution)/shard_map/ppermute | solution.py:325
  179.6 0.7 copy-start.4
  182.0 18.9 %all-to-all-start.5 = ((f32[8,16,256]{2,1,0:T(8,128)}), f32[8,16,256]{2,1,0:T(8,128)S(1)}, u32[]{:S(2)}, u32[]{:S(2)}) async-start(f32[8,16,256]{2,1,0:T(8,128)} %shard_map.111), calls=%async_computation.5 | async-start | bytes 262144 | tf_op jit(solution)/shard_map/all_to_all | solution.py:426
  195.9 5.0 %collective-permute-start.5 = (bf16[16,256]{1,0:T(8,128)(2,1)S(1)}, bf16[16,256]{1,0:T(8,128)(2,1)S(1)}, u32[]{:S(2)}, u32[]{:S(2)}) collective-permute-start(bf16[16,256]{1,0:T(8,128)(2,1)S(1)} %slice.18), channel_id=1, source_target_pairs={{0,4},{4,8},{8,12},{12,16},{16,20},{20,24},{24,28},{28,32},{32,36}... | collective-permute-start | bytes 24584 | tf_op jit(solution)/shard_map/ppermute | solution.py:444
  198.0 2.9 %copy-start.6 = (bf16[4,4,4,16,512]{4,3,2,1,0:T(8,128)(2,1)}, bf16[4,4,4,16,512]{4,3,2,1,0:T(8,128)(2,1)S(1)}, u32[]{:S(2)}) copy-start(bf16[4,4,4,16,512]{4,3,2,1,0:T(8,128)(2,1)S(1)} %collective-permute-done.6.other_ref) | copy-start | bytes 3145732
  200.9 0.6 copy-start.9
  200.9 0.6 copy-start.8

commit v3 on v2

--- a/solution.py
+++ b/solution.py
@@ -51,30 +51,25 @@
 
 def ring_gather(x, axis):
     n = lax.axis_size(axis)
-    up = [(i, (i + 1) % n) for i in range(n)]
-    down = [(i, (i - 1) % n) for i in range(n)]
-    half = x.shape[0] // 2
-    before = lax.ppermute(x, axis, up)
-    after = lax.ppermute(x, axis, down)
-    far_low = lax.ppermute(before[:half], axis, up)
-    far_high = lax.ppermute(after[half:], axis, down)
-    return x, before, after, far_low, far_high
+    pieces = [x]
+    for shift in (1, -1, -2):
+        pieces.append(lax.ppermute(x, axis, [(i, (i + shift) % n) for i in range(n)]))
+    return pieces
 
 
 def places(index, n):
     return [index, lax.rem(index + n - 1, n), lax.rem(index + 1, n), lax.rem(index + 2, n)]
 
 
-def fetches(core, mine_ref, other_ref, lanes, whole_ref, sems):
-    nx, near = mine_ref.shape[:2]
+def fetches(core, across, near, mine_ref, other_ref, lanes, whole_ref, sems):
     copies = []
-    for x in range(nx):
-        for n in range(near):
+    for i, x in enumerate(across):
+        for j, n in enumerate(near):
             for side, from_ref in enumerate((mine_ref, other_ref)):
                 to = core if side == 0 else 1 - core
                 copies.append(
                     pltpu.make_async_copy(
-                        from_ref.at[x, n, :, :, lanes],
+                        from_ref.at[i, j, :, :, lanes],
                         whole_ref.at[:, n, x, to],
                         sems.at[len(copies)],
                     )
@@ -97,8 +92,7 @@
     own_ref,
     before_ref,
     after_ref,
-    low_ref,
-    high_ref,
+    far_ref,
     gain_ref,
     mine_ref,
     other_ref,
@@ -116,7 +110,16 @@
 ):
     rows, _ = normed_ref.shape
     cols = gap_ref.shape[1]
-    copies = fetches(info_ref[0], mine_ref, other_ref, slice(0, 2 * cols), whole_ref, sems)
+    copies = fetches(
+        info_ref[0],
+        range(mine_ref.shape[0]),
+        range(mine_ref.shape[1]),
+        mine_ref,
+        other_ref,
+        slice(None),
+        whole_ref,
+        sems,
+    )
     started(copies)
     block = own_ref.shape[0]
     own, before, after, far = places(info_ref[1], rows // block)
@@ -128,17 +131,13 @@
         normed_ref[at, :] = (floats * scale * gain_ref[...]).astype(BF)
 
     def norm_all(i, carry):
-        for from_ref, place in ((own_ref, own), (before_ref, before), (after_ref, after)):
-            norm(from_ref, place * block, i)
+        norm(own_ref, own * block, i)
+        norm(before_ref, before * block, i)
+        norm(after_ref, after * block, i)
+        norm(far_ref, far * block, i)
         return carry
 
-    def norm_far(i, carry):
-        norm(low_ref, far * block, i)
-        norm(high_ref, far * block + block // 2, i)
-        return carry
-
     lax.fori_loop(0, block // 32, norm_all, 0)
-    lax.fori_loop(0, block // 64, norm_far, 0)
     finished(copies)
     both_ref[...] = dot(normed_ref[...], whole_ref[...].reshape(-1, 2 * cols))
     row = lax.broadcasted_iota(jnp.int32, (CHUNK, CHUNK), 0)
@@ -187,9 +186,11 @@
         state = state * jnp.exp(fade) + got_ref[d, :, :cols]
         faded = faded + fade
     high = faded.astype(BF).astype(F32)
-    row = lax.broadcasted_iota(jnp.int32, (16, cols), 0)
-    total_ref[:rows, :] = state.astype(BF)
-    total_ref[rows:, :] = jnp.where(row == 0, high, jnp.where(row == 1, faded - high, 0.0)).astype(BF)
+    row = lax.broadcasted_iota(jnp.int32, (8, cols), 0)
+    fades = jnp.where(row == 0, high, jnp.where(row == 1, faded - high, 0.0))
+    total = jnp.concatenate([state, fades], axis=0).astype(BF)
+    for z in range(total_ref.shape[0]):
+        total_ref[z] = total
 
 
 def depth_kernel(info_ref, totals_ref, before_ref, faded_ref, start_ref):
@@ -220,7 +221,16 @@
     both_ref,
 ):
     rows, cols = values_ref.shape
-    copies = fetches(info_ref[0], mine_ref, other_ref, slice(2 * cols, 4 * cols), whole_ref, sems)
+    copies = fetches(
+        info_ref[0],
+        places(info_ref[3], mine_ref.shape[0]),
+        places(info_ref[5], mine_ref.shape[1]),
+        mine_ref,
+        other_ref,
+        slice(0, 2 * cols),
+        whole_ref,
+        sems,
+    )
     started(copies)
     finished(copies)
     both_ref[...] = dot(normed_ref[...], whole_ref[...].reshape(-1, 2 * cols))
@@ -257,7 +267,16 @@
     mixed_ref,
 ):
     rows, cols = cum_ref.shape
-    copies = fetches(info_ref[0], mine_ref, other_ref, slice(0, 2 * cols), whole_ref, sems)
+    copies = fetches(
+        info_ref[0],
+        places(info_ref[3], mine_ref.shape[0]),
+        places(info_ref[5], mine_ref.shape[1]),
+        mine_ref,
+        other_ref,
+        slice(2 * cols, 4 * cols),
+        whole_ref,
+        sems,
+    )
     started(copies)
     group = info_ref[1]
     padded = jnp.concatenate([rim_ref[...], pooled_ref[...]], axis=0).astype(F32)
@@ -350,6 +369,7 @@
             lax.axis_index(SP) * rows,
             lax.axis_index(ACROSS),
             lax.axis_index(DEPTH),
+            lax.axis_index(NEAR),
         ]
     ).astype(jnp.int32)
 
@@ -363,15 +383,16 @@
         recur_out_weight.T,
     )
     weights = sent_to_all(weights, FAR)
-    weights = sent_to_all(weights, NEAR)
-    inner = sent_to_all(weights[..., : 4 * cols], ACROSS)
-    inner_other = over_cores(inner)
-    outer = sent_to_all(weights[..., 4 * cols :], ACROSS)
-    outer_other = over_cores(outer)
-    blocks = outer.shape[2], outer.shape[1], outer.shape[0], 2, outer.shape[3], 2 * cols
+    first = sent_to_all(weights[..., : 2 * cols], NEAR)
+    first = sent_to_all(first, ACROSS)
+    first_other = over_cores(first)
+    rest = jnp.stack(ring_gather(weights[..., 2 * cols :], DEPTH))
+    rest = jnp.stack(ring_gather(rest, ACROSS))
+    rest_other = over_cores(rest)
+    blocks = first.shape[2], first.shape[1], first.shape[0], 2, first.shape[3], 2 * cols
     whole = [
         pltpu.VMEM(blocks, BF),
-        pltpu.SemaphoreType.DMA((2 * outer.shape[0] * outer.shape[1],)),
+        pltpu.SemaphoreType.DMA((2 * first.shape[0] * first.shape[1],)),
     ]
 
     normed, values, opened, cum, growth, payload = call(
@@ -390,8 +411,8 @@
         info,
         *pieces,
         norm_gain[None, :],
-        inner,
-        inner_other,
+        first,
+        first_other,
         forget_gap[None, :],
         decay_shift.T,
     )
@@ -404,14 +425,14 @@
         [
             shape((plane, slab, cols), F32),
             shape((plane, cols), F32),
-            shape((slab + 16, cols), BF),
+            shape((lax.axis_size(DEPTH), slab + 8, cols), BF),
         ],
         [],
         1 << 20,
         1 << 19,
         got.reshape(plane, slab, 2 * cols),
     )
-    totals = sent_to_all(total, DEPTH)
+    totals = lax.all_to_all(total, DEPTH, split_axis=0, concat_axis=0, tiled=True)
     start = call(
         depth_kernel,
         shape((plane, slab, cols), F32),
@@ -434,8 +455,8 @@
         8 << 20,
         info,
         normed,
-        inner,
-        inner_other,
+        rest,
+        rest_other,
         values,
         opened,
         cum,
@@ -457,8 +478,8 @@
         pooled,
         rim,
         out_gain[None, :],
-        outer,
-        outer_other,
+        rest,
+        rest_other,
     )
     parts = lax.all_to_all(
         part.reshape(tp, rows // tp, width), "tp", split_axis=0, concat_axis=0, tiled=True

time: 242 us -> 228 us (0.942)
  waiting for transfers between devices: 49.5 us -> 38.6 us
  blocking collectives: 113 us -> 106 us
  starting transfers between devices: 40.9 us -> 45.3 us
  local copies, waits for them, and re-layouts: 8.79 us -> 5.14 us
  other arithmetic: 2.09 us -> 4.76 us
    all_to_all x3 -> x2, blocking collectives: 82.4 us -> 43.4 us  [sent_to_all(): return lax.all_to_all(copies, axis, split_axis=0, concat_axis=0, tiled=True)]
    all_to_all x0 -> x2, blocking collectives: none -> 32.6 us  [the longest x1 22.5 us: layer(): lax.all_to_all(total, DEPTH, split_axis=0, concat_axis=0, tiled=True)]
    all_to_all x2 -> x1, waiting for transfers between devices: 26.8 us -> 0.01 us  [sent_to_all(): return lax.all_to_all(copies, axis, split_axis=0, concat_axis=0, tiled=True)]
    ppermute x4 -> x9, waiting for transfers between devices: 14.4 us -> 35.6 us  [ring_gather(): lax.ppermute(x, axis, [(i, (i + shift) % n) for i in range(n)])]
    ppermute x4 -> x9, starting transfers between devices: 14.1 us -> 29.3 us  [ring_gather(): lax.ppermute(x, axis, [(i, (i + shift) % n) for i in range(n)])]
    all_to_all x1 -> x0, starting transfers between devices: 5.43 us -> none  [layer(): lax.all_to_all(payload, PLANE, split_axis=0, concat_axis=0, tiled=True)]
    all_to_all x1 -> x0, waiting for transfers between devices: 5.4 us -> none  [layer(): lax.all_to_all(payload, PLANE, split_axis=0, concat_axis=0, tiled=True)]
    all_to_all x2 -> x1, starting transfers between devices: 10.2 us -> 4.77 us  [sent_to_all(): return lax.all_to_all(copies, axis, split_axis=0, concat_axis=0, tiled=True)]
  transfers between devices with their start and end apart: 11 -> 14, of which waited for: 7 -> 9; matrix products, arithmetic and copies ran while one was open for 2% -> 2% of each run, Pallas kernels for 5% -> 8%
where the time goes in v3:
time: 228 us; the launch traced here: 225 us
  blocking collectives  106 us (46%)
  starting transfers between devices  45.3 us (20%)
  waiting for transfers between devices  38.6 us (17%)
  Pallas kernels  25 us (11%)
  local copies, waits for them, and re-layouts  5.14 us (2%)
  other arithmetic  4.76 us (2%)
    all_to_all x2, blocking collectives, sent_to_all(): return lax.all_to_all(copies, axis, split_axis=0, concat_axis=0, tiled=True)  43.4 us
    ppermute x9, waiting for transfers between devices, ring_gather(): lax.ppermute(x, axis, [(i, (i + shift) % n) for i in range(n)])  35.6 us
    all_to_all x1, blocking collectives, layer(): lax.all_to_all(part.reshape(tp, rows // tp, width), 'tp', split_axis=0, c...  29.9 us
    ppermute x9, starting transfers between devices, ring_gather(): lax.ppermute(x, axis, [(i, (i + shift) % n) for i in range(n)])  29.3 us
    pallas_call x5, Pallas kernels, call(): pl.pallas_call(kernel, out_shape=outs, in_specs=[SMEM if a.dtype == jnp.i...  25 us
    all_to_all x1, blocking collectives, layer(): lax.all_to_all(total, DEPTH, split_axis=0, concat_axis=0, tiled=True)  22.5 us
    all_to_all x1, blocking collectives, layer(): lax.all_to_all(payload, PLANE, split_axis=0, concat_axis=0, tiled=True)  10.1 us
    all_to_all x1, starting transfers between devices, layer(): lax.all_to_all(start.reshape(RDIM, cols), PLANE, split_axis=0, concat_axi...  5.37 us
  transfers between devices with their start and end apart: 14, of which 9 were waited for; matrix products, arithmetic and copies ran while one was open for 2% of the time, Pallas kernels for 8%

profile of v3, /device:TPU:6, one launch (start us, length us, event | category | flops | bytes accessed | tf_op | source)
XLA Modules:
  0.0 224.9 jit_solution(5048439111457435400)
XLA Ops:
  0.0 0.8 pad_add_fusion
  0.8 31.8 %all_to_all.42 = bf16[4,16,1536]{2,1,0:T(8,128)(2,1)S(1)} all-to-all(bf16[4,16,1536]{2,1,0:T(8,128)(2,1)S(1)} %broadcast_in_dim.19), channel_id=1, replica_groups=mesh['sp_f'=4,'sp_n'=4,'sp_x'=4,'sp_c'=2,'tp'=4] {'sp_f'}, dimensions={0} | all-to-all | bytes 393216 | tf_op jit(solution)/shard_map/all_to_all | solution.py:49
  32.7 11.5 %all_to_all.43 = bf16[4,4,16,512]{3,2,1,0:T(8,128)(2,1)S(1)} all-to-all(bf16[4,4,16,512]{3,2,1,0:T(8,128)(2,1)S(1)} %broadcast_in_dim.20), channel_id=1, replica_groups=mesh['sp_f'=4,'sp_n'=4,'sp_x'=4,'sp_c'=2,'tp'=4] {'sp_n'}, dimensions={0} | all-to-all | bytes 524288 | tf_op jit(solution)/shard_map/all_to_all | solution.py:49
  44.2 1.1 broadcast_in_dim.21
  45.4 4.8 %all-to-all-start.2 = ((bf16[4,4,4,16,512]{4,3,2,1,0:T(8,128)(2,1)}), bf16[4,4,4,16,512]{4,3,2,1,0:T(8,128)(2,1)S(1)}, u32[]{:S(2)}, u32[]{:S(2)}) async-start(bf16[4,4,4,16,512]{4,3,2,1,0:T(8,128)(2,1)} %broadcast_in_dim.21), calls=%async_computation.2 | async-start | bytes 2097152 | tf_op jit(solution)/shard_map/all_to_all | solution.py:49
  50.1 2.1 collective-permute-start.6
  52.2 3.7 %collective-permute-start.5 = (bf16[4,16,1024]{2,1,0:T(8,128)(2,1)S(1)}, bf16[4,16,1024]{2,1,0:T(8,128)(2,1)S(1)}, u32[]{:S(2)}, u32[]{:S(2)}) collective-permute-start(bf16[4,16,1024]{2,1,0:T(8,128)(2,1)S(1)} %get-tuple-element.32), channel_id=1, source_target_pairs={{0,480},{32,0},{64,32},{96,64},{128,96},{160,128},{192,160},{224,1... | collective-permute-start | bytes 393224 | tf_op jit(solution)/shard_map/ppermute | solution.py:56
  55.9 2.2 collective-permute-start.4
  58.1 2.4 %collective-permute-done.6 = bf16[4,16,1024]{2,1,0:T(8,128)(2,1)S(1)} collective-permute-done((bf16[4,16,1024]{2,1,0:T(8,128)(2,1)S(1)}, bf16[4,16,1024]{2,1,0:T(8,128)(2,1)S(1)}, u32[]{:S(2)}, u32[]{:S(2)}) %collective-permute-start.6) | collective-permute-done | bytes 131104 | tf_op jit(solution)/shard_map/ppermute | solution.py:56
  60.5 0.4 collective-permute-done.5
  61.0 3.0 %collective-permute-done.4 = bf16[4,16,1024]{2,1,0:T(8,128)(2,1)S(1)} collective-permute-done((bf16[4,16,1024]{2,1,0:T(8,128)(2,1)S(1)}, bf16[4,16,1024]{2,1,0:T(8,128)(2,1)S(1)}, u32[]{:S(2)}, u32[]{:S(2)}) %collective-permute-start.4) | collective-permute-done | bytes 131104 | tf_op jit(solution)/shard_map/ppermute | solution.py:56
  64.0 0.9 fusion
  64.8 3.4 %collective-permute-start.9 = (bf16[4,4,16,1024]{3,2,1,0:T(8,128)(2,1)S(1)}, bf16[4,4,16,1024]{3,2,1,0:T(8,128)(2,1)S(1)}, u32[]{:S(2)}, u32[]{:S(2)}) collective-permute-start(bf16[4,4,16,1024]{3,2,1,0:T(8,128)(2,1)S(1)} %get-tuple-element.30), channel_id=1, source_target_pairs={{0,16},{8,24},{16,0},{24,8},{1,17},{9,25},{17,1},{25,9},{2,18},{10... | collective-permute-start | bytes 1572872 | tf_op jit(solution)/shard_map/ppermute | solution.py:56
  68.2 1.9 collective-permute-start.8
  70.1 5.1 %collective-permute-start.7 = (bf16[4,4,16,1024]{3,2,1,0:T(8,128)(2,1)S(1)}, bf16[4,4,16,1024]{3,2,1,0:T(8,128)(2,1)S(1)}, u32[]{:S(2)}, u32[]{:S(2)}) collective-permute-start(bf16[4,4,16,1024]{3,2,1,0:T(8,128)(2,1)S(1)} %get-tuple-element.30), channel_id=1, source_target_pairs={{0,8},{8,16},{16,24},{24,0},{1,9},{9,17},{17,25},{25,1},{2,10},{10... | collective-permute-start | bytes 1572872 | tf_op jit(solution)/shard_map/ppermute | solution.py:56
  75.3 0.0 all-to-all-done.2.mine_ref
  75.3 0.0 copy-start.1
  75.3 1.9 collective-permute-start.3
  77.2 5.8 %collective-permute-done.9 = bf16[4,4,16,1024]{3,2,1,0:T(8,128)(2,1)S(1)} collective-permute-done((bf16[4,4,16,1024]{3,2,1,0:T(8,128)(2,1)S(1)}, bf16[4,4,16,1024]{3,2,1,0:T(8,128)(2,1)S(1)}, u32[]{:S(2)}, u32[]{:S(2)}) %collective-permute-start.9) | collective-permute-done | bytes 524320 | tf_op jit(solution)/shard_map/ppermute | solution.py:56
  83.0 0.0 copy-start.3
  83.0 6.3 %collective-permute-done.8 = bf16[4,4,16,1024]{3,2,1,0:T(8,128)(2,1)S(1)} collective-permute-done((bf16[4,4,16,1024]{3,2,1,0:T(8,128)(2,1)S(1)}, bf16[4,4,16,1024]{3,2,1,0:T(8,128)(2,1)S(1)}, u32[]{:S(2)}, u32[]{:S(2)}) %collective-permute-start.8) | collective-permute-done | bytes 524320 | tf_op jit(solution)/shard_map/ppermute | solution.py:56
  89.3 0.0 copy-start.4
  89.3 0.0 collective-permute-done.7
  89.3 0.0 copy-start.5
  89.3 0.0 copy-done.3
  89.3 0.8 copy-done.4
  90.1 0.2 copy-done.5
  90.3 0.0 copy-start.7
  90.3 1.8 pad_maximum_fusion.mine_ref
  92.1 0.0 copy-done.1
  92.1 0.0 copy-start
  92.1 1.9 collective-permute-start.10
  94.1 3.5 %collective-permute-start = (bf16[128,2048]{1,0:T(8,128)(2,1)}, bf16[128,2048]{1,0:T(8,128)(2,1)}, u32[]{:S(2)}, u32[]{:S(2)}) collective-permute-start(bf16[128,2048]{1,0:T(8,128)(2,1)} %own_ref.1), channel_id=1, source_target_pairs={{0,1},{1,2},{2,3},{3,0},{4,5},{5,6},{6,7},{7,4},{8,9},{9,10},{10,1... | collective-permute-start | bytes 1572872 | tf_op jit(solution)/shard_map/ppermute | solution.py:56
  97.6 3.6 %collective-permute-start.1 = (bf16[128,2048]{1,0:T(8,128)(2,1)}, bf16[128,2048]{1,0:T(8,128)(2,1)}, u32[]{:S(2)}, u32[]{:S(2)}) collective-permute-start(bf16[128,2048]{1,0:T(8,128)(2,1)} %own_ref.1), channel_id=1, source_target_pairs={{0,3},{1,0},{2,1},{3,2},{4,7},{5,4},{6,5},{7,6},{8,11},{9,8},{10,9... | collective-permute-start | bytes 1572872 | tf_op jit(solution)/shard_map/ppermute | solution.py:56
  101.1 3.9 %collective-permute-start.2 = (bf16[128,2048]{1,0:T(8,128)(2,1)}, bf16[128,2048]{1,0:T(8,128)(2,1)}, u32[]{:S(2)}, u32[]{:S(2)}) collective-permute-start(bf16[128,2048]{1,0:T(8,128)(2,1)} %own_ref.1), channel_id=1, source_target_pairs={{0,2},{1,3},{2,0},{3,1},{4,6},{5,7},{6,4},{7,5},{8,10},{9,11},{10,... | collective-permute-start | bytes 1572872 | tf_op jit(solution)/shard_map/ppermute | solution.py:56
  105.1 0.0 copy-done.7
  105.1 0.9 copy.12
  105.9 0.7 stack.57.info_ref
  106.6 5.3 %collective-permute-done.before_ref = bf16[128,2048]{1,0:T(8,128)(2,1)} collective-permute-done((bf16[128,2048]{1,0:T(8,128)(2,1)}, bf16[128,2048]{1,0:T(8,128)(2,1)}, u32[]{:S(2)}, u32[]{:S(2)}) %collective-permute-start) | collective-permute-done | bytes 524320 | tf_op jit(solution)/shard_map/ppermute | solution.py:56
  111.9 2.7 %collective-permute-done.1.after_ref = bf16[128,2048]{1,0:T(8,128)(2,1)} collective-permute-done((bf16[128,2048]{1,0:T(8,128)(2,1)}, bf16[128,2048]{1,0:T(8,128)(2,1)}, u32[]{:S(2)}, u32[]{:S(2)}) %collective-permute-start.1) | collective-permute-done | bytes 524320 | tf_op jit(solution)/shard_map/ppermute | solution.py:56
  114.6 9.7 %collective-permute-done.2.far_ref = bf16[128,2048]{1,0:T(8,128)(2,1)} collective-permute-done((bf16[128,2048]{1,0:T(8,128)(2,1)}, bf16[128,2048]{1,0:T(8,128)(2,1)}, u32[]{:S(2)}, u32[]{:S(2)}) %collective-permute-start.2) | collective-permute-done | bytes 524320 | tf_op jit(solution)/shard_map/ppermute | solution.py:56
  124.3 0.0 collective-permute-done.3.other_ref
  124.3 7.6 %shard_map.109 = (bf16[512,2048]{1,0:T(8,128)(2,1)}, bf16[512,256]{1,0:T(8,128)(2,1)}, f32[512,256]{1,0:T(8,128)}, f32[512,256]{1,0:T(8,128)}, f32[4,128,256]{2,1,0:T(8,128)}, /*index=5*/f32[128,512]{1,0:T(8,128)}) custom-call(s32[6]{0:T(128)} %stack.57.info_ref, bf16[128,2048]{1,0:T(8,128)(2,1)} %own_ref.1, ...), custom_call_target="tpu_custom_call" | custom-call | flops 1073741824 | bytes 8388608 | tf_op jit(solution)/shard_map/pallas_call | solution.py:319
  131.9 0.0 copy-done
  131.9 10.1 %all_to_all.44.got_ref = f32[8,16,512]{2,1,0:T(8,128)} all-to-all(f32[8,16,512]{2,1,0:T(8,128)} %bitcast.31), channel_id=1, replica_groups=mesh['sp_f'=4,'sp_n'=4,'sp_x'=4,'sp_c'=2,'tp'=4] {'sp_x','sp_c'}, dimensions={0} | all-to-all | bytes 524288 | tf_op jit(solution)/shard_map/all_to_all | solution.py:422
  142.0 1.7 shard_map.110
  143.7 22.5 %all_to_all.45.totals_ref = bf16[16,24,256]{2,1,0:T(8,128)(2,1)} all-to-all(bf16[16,24,256]{2,1,0:T(8,128)(2,1)} %get-tuple-element.18), channel_id=1, replica_groups=mesh['sp_f'=4,'sp_n'=4,'sp_x'=4,'sp_c'=2,'tp'=4] {'sp_f','sp_n'}, dimensions={0} | all-to-all | bytes 393216 | tf_op jit(solution)/shard_map/all_to_all | solution.py:435
  166.3 1.7 shard_map.111
  168.0 5.4 %all-to-all-start.5 = ((f32[8,16,256]{2,1,0:T(8,128)}), f32[8,16,256]{2,1,0:T(8,128)S(1)}, u32[]{:S(2)}, u32[]{:S(2)}) async-start(f32[8,16,256]{2,1,0:T(8,128)} %shard_map.111), calls=%async_computation.5 | async-start | bytes 262144 | tf_op jit(solution)/shard_map/all_to_all | solution.py:447
  173.4 0.0 collective-permute-done.10.other_ref
  173.4 7.8 %shard_map.112 = (bf16[512,256]{1,0:T(8,128)(2,1)}, f32[512,256]{1,0:T(8,128)}, f32[512,256]{1,0:T(8,128)}) custom-call(s32[6]{0:T(128)} %stack.57.info_ref, bf16[512,2048]{1,0:T(8,128)(2,1)} %get-tuple-element.23.normed_ref, bf16[4,4,4,16,1024]{4,3,2,1,0:T(8,128)(2,1)} %copy-done, bf16[4,4,4,16,1024]{4,3,2,1,0:T(8,128)(2,1)} %collective-permute-done.10.other_ref, ...), custom_call_target="tpu_custom_call" | custom-call | flops 1073741824 | bytes 8388608 | tf_op jit(solution)/shard_map/pallas_call | solution.py:319
  181.2 0.7 slice.11
  181.9 2.0 collective-permute-start.11
  183.9 2.9 %collective-permute-done.11.rim_ref = bf16[16,256]{1,0:T(8,128)(2,1)S(1)} collective-permute-done((bf16[16,256]{1,0:T(8,128)(2,1)S(1)}, bf16[16,256]{1,0:T(8,128)(2,1)S(1)}, u32[]{:S(2)}, u32[]{:S(2)}) %collective-permute-start.11) | collective-permute-done | bytes 8224 | tf_op jit(solution)/shard_map/ppermute | solution.py:465
  186.9 0.0 copy-start.6
  186.9 0.0 all-to-all-done.5
  186.9 0.0 copy-start.2
  186.9 0.6 copy-done.6
  187.5 0.1 copy-done.2
  187.5 6.2 %shard_map.113 = bf16[512,2048]{1,0:T(8,128)(2,1)} custom-call(s32[6]{0:T(128)} %stack.57.info_ref, f32[128,256]{1,0:T(8,128)} %bitcast.27, f32[4,128,256]{2,1,0:T(8,128)} %get-tuple-element.21.growth_ref, f32[512,256]{1,0:T(8,128)} %get-tuple-element.22.cum_ref, f32[512,256]{1,0:T(8,128)} %get-tuple-element.26.decayed_ref, ...), custom_call_target="tpu_custom_call" | custom-call | flops 1073741824 | bytes 8388608 | tf_op jit(solution)/shard_map/pallas_call | solution.py:319
  193.7 29.9 %all_to_all.46 = bf16[4,128,2048]{2,1,0:T(8,128)(2,1)S(1)} all-to-all(bf16[4,128,2048]{2,1,0:T(8,128)(2,1)} %bitcast.25), channel_id=1, replica_groups=mesh['sp_f'=4,'sp_n'=4,'sp_x'=4,'sp_c'=2,'tp'=4] {'tp'}, dimensions={0} | all-to-all | bytes 4194304 | tf_op jit(solution)/shard_map/all_to_all | solution.py:484
  223.6 1.3 reduce_sum.12
  (4 shorter events, 0.1 us)
Async XLA Ops:
  45.4 29.9 %all-to-all-start.2 = ((bf16[4,4,4,16,512]{4,3,2,1,0:T(8,128)(2,1)}), bf16[4,4,4,16,512]{4,3,2,1,0:T(8,128)(2,1)S(1)}, u32[]{:S(2)}, u32[]{:S(2)}) async-start(bf16[4,4,4,16,512]{4,3,2,1,0:T(8,128)(2,1)} %broadcast_in_dim.21), calls=%async_computation.2 | async-start | bytes 2097152 | tf_op jit(solution)/shard_map/all_to_all | solution.py:49
  50.1 10.4 %collective-permute-start.6 = (bf16[4,16,1024]{2,1,0:T(8,128)(2,1)S(1)}, bf16[4,16,1024]{2,1,0:T(8,128)(2,1)S(1)}, u32[]{:S(2)}, u32[]{:S(2)}) collective-permute-start(bf16[4,16,1024]{2,1,0:T(8,128)(2,1)S(1)} %get-tuple-element.32), channel_id=1, source_target_pairs={{0,448},{32,480},{64,0},{96,32},{128,64},{160,96},{192,128},{224,1... | collective-permute-start | bytes 393224 | tf_op jit(solution)/shard_map/ppermute | solution.py:56
  52.2 8.7 %collective-permute-start.5 = (bf16[4,16,1024]{2,1,0:T(8,128)(2,1)S(1)}, bf16[4,16,1024]{2,1,0:T(8,128)(2,1)S(1)}, u32[]{:S(2)}, u32[]{:S(2)}) collective-permute-start(bf16[4,16,1024]{2,1,0:T(8,128)(2,1)S(1)} %get-tuple-element.32), channel_id=1, source_target_pairs={{0,480},{32,0},{64,32},{96,64},{128,96},{160,128},{192,160},{224,1... | collective-permute-start | bytes 393224 | tf_op jit(solution)/shard_map/ppermute | solution.py:56
  55.9 8.1 %collective-permute-start.4 = (bf16[4,16,1024]{2,1,0:T(8,128)(2,1)S(1)}, bf16[4,16,1024]{2,1,0:T(8,128)(2,1)S(1)}, u32[]{:S(2)}, u32[]{:S(2)}) collective-permute-start(bf16[4,16,1024]{2,1,0:T(8,128)(2,1)S(1)} %get-tuple-element.32), channel_id=1, source_target_pairs={{0,32},{32,64},{64,96},{96,128},{128,160},{160,192},{192,224},{224... | collective-permute-start | bytes 393224 | tf_op jit(solution)/shard_map/ppermute | solution.py:56
  64.8 18.2 %collective-permute-start.9 = (bf16[4,4,16,1024]{3,2,1,0:T(8,128)(2,1)S(1)}, bf16[4,4,16,1024]{3,2,1,0:T(8,128)(2,1)S(1)}, u32[]{:S(2)}, u32[]{:S(2)}) collective-permute-start(bf16[4,4,16,1024]{3,2,1,0:T(8,128)(2,1)S(1)} %get-tuple-element.30), channel_id=1, source_target_pairs={{0,16},{8,24},{16,0},{24,8},{1,17},{9,25},{17,1},{25,9},{2,18},{10... | collective-permute-start | bytes 1572872 | tf_op jit(solution)/shard_map/ppermute | solution.py:56
  68.2 21.1 %collective-permute-start.8 = (bf16[4,4,16,1024]{3,2,1,0:T(8,128)(2,1)S(1)}, bf16[4,4,16,1024]{3,2,1,0:T(8,128)(2,1)S(1)}, u32[]{:S(2)}, u32[]{:S(2)}) collective-permute-start(bf16[4,4,16,1024]{3,2,1,0:T(8,128)(2,1)S(1)} %get-tuple-element.30), channel_id=1, source_target_pairs={{0,24},{8,0},{16,8},{24,16},{1,25},{9,1},{17,9},{25,17},{2,26},{10... | collective-permute-start | bytes 1572872 | tf_op jit(solution)/shard_map/ppermute | solution.py:56
  70.1 19.2 %collective-permute-start.7 = (bf16[4,4,16,1024]{3,2,1,0:T(8,128)(2,1)S(1)}, bf16[4,4,16,1024]{3,2,1,0:T(8,128)(2,1)S(1)}, u32[]{:S(2)}, u32[]{:S(2)}) collective-permute-start(bf16[4,4,16,1024]{3,2,1,0:T(8,128)(2,1)S(1)} %get-tuple-element.30), channel_id=1, source_target_pairs={{0,8},{8,16},{16,24},{24,0},{1,9},{9,17},{17,25},{25,1},{2,10},{10... | collective-permute-start | bytes 1572872 | tf_op jit(solution)/shard_map/ppermute | solution.py:56
  75.3 16.8 %copy-start.1 = (bf16[4,4,4,16,512]{4,3,2,1,0:T(8,128)(2,1)}, bf16[4,4,4,16,512]{4,3,2,1,0:T(8,128)(2,1)S(1)}, u32[]{:S(2)}) copy-start(bf16[4,4,4,16,512]{4,3,2,1,0:T(8,128)(2,1)S(1)} %all-to-all-done.2.mine_ref) | copy-start | bytes 3145732
  75.3 49.0 %collective-permute-start.3 = (bf16[4,4,4,16,512]{4,3,2,1,0:T(8,128)(2,1)S(1)}, bf16[4,4,4,16,512]{4,3,2,1,0:T(8,128)(2,1)}, u32[]{:S(2)}, u32[]{:S(2)}) collective-permute-start(bf16[4,4,4,16,512]{4,3,2,1,0:T(8,128)(2,1)S(1)} %all-to-all-done.2.mine_ref), channel_id=1, source_target_pairs={{0,4},{4,0},{1,5},{5,1},{2,6},{6,2},{3,7},{7,3},{8,12},{12,8},{9,1... | collective-permute-start | bytes 3145736 | tf_op jit(solution)/shard_map/ppermute | solution.py:344
  83.0 6.3 %copy-start.3 = (bf16[4,4,16,1024]{3,2,1,0:T(8,128)(2,1)}, bf16[4,4,16,1024]{3,2,1,0:T(8,128)(2,1)S(1)}, u32[]{:S(2)}) copy-start(bf16[4,4,16,1024]{3,2,1,0:T(8,128)(2,1)S(1)} %collective-permute-done.9) | copy-start | bytes 1572868
  89.3 0.8 copy-start.4
  89.3 1.0 copy-start.5
  90.3 14.7 %copy-start.7 = (f32[2,512]{1,0:T(2,128)S(1)}, f32[2,512]{1,0:T(2,128)}, u32[]{:S(2)}) copy-start(f32[2,512]{1,0:T(2,128)} %param.18) | copy-start | bytes 12292
  92.1 39.8 %copy-start = (bf16[4,4,4,16,1024]{4,3,2,1,0:T(8,128)(2,1)}, bf16[4,4,4,16,1024]{4,3,2,1,0:T(8,128)(2,1)S(1)}, u32[]{:S(2)}) copy-start(bf16[4,4,4,16,1024]{4,3,2,1,0:T(8,128)(2,1)S(1)} %pad_maximum_fusion.mine_ref) | copy-start | bytes 6291460
  92.1 81.3 %collective-permute-start.10 = (bf16[4,4,4,16,1024]{4,3,2,1,0:T(8,128)(2,1)S(1)}, bf16[4,4,4,16,1024]{4,3,2,1,0:T(8,128)(2,1)}, u32[]{:S(2)}, u32[]{:S(2)}) collective-permute-start(bf16[4,4,4,16,1024]{4,3,2,1,0:T(8,128)(2,1)S(1)} %pad_maximum_fusion.mine_ref), channel_id=1, source_target_pairs={{0,4},{4,0},{1,5},{5,1},{2,6},{6,2},{3,7},{7,3},{8,12},{12,8},{9,1... | collective-permute-start | bytes 6291464 | tf_op jit(solution)/shard_map/ppermute | solution.py:344
  94.1 17.8 %collective-permute-start = (bf16[128,2048]{1,0:T(8,128)(2,1)}, bf16[128,2048]{1,0:T(8,128)(2,1)}, u32[]{:S(2)}, u32[]{:S(2)}) collective-permute-start(bf16[128,2048]{1,0:T(8,128)(2,1)} %own_ref.1), channel_id=1, source_target_pairs={{0,1},{1,2},{2,3},{3,0},{4,5},{5,6},{6,7},{7,4},{8,9},{9,10},{10,1... | collective-permute-start | bytes 1572872 | tf_op jit(solution)/shard_map/ppermute | solution.py:56
  97.6 17.0 %collective-permute-start.1 = (bf16[128,2048]{1,0:T(8,128)(2,1)}, bf16[128,2048]{1,0:T(8,128)(2,1)}, u32[]{:S(2)}, u32[]{:S(2)}) collective-permute-start(bf16[128,2048]{1,0:T(8,128)(2,1)} %own_ref.1), channel_id=1, source_target_pairs={{0,3},{1,0},{2,1},{3,2},{4,7},{5,4},{6,5},{7,6},{8,11},{9,8},{10,9... | collective-permute-start | bytes 1572872 | tf_op jit(solution)/shard_map/ppermute | solution.py:56
  101.1 23.2 %collective-permute-start.2 = (bf16[128,2048]{1,0:T(8,128)(2,1)}, bf16[128,2048]{1,0:T(8,128)(2,1)}, u32[]{:S(2)}, u32[]{:S(2)}) collective-permute-start(bf16[128,2048]{1,0:T(8,128)(2,1)} %own_ref.1), channel_id=1, source_target_pairs={{0,2},{1,3},{2,0},{3,1},{4,6},{5,7},{6,4},{7,5},{8,10},{9,11},{10,... | collective-permute-start | bytes 1572872 | tf_op jit(solution)/shard_map/ppermute | solution.py:56
  168.0 18.8 %all-to-all-start.5 = ((f32[8,16,256]{2,1,0:T(8,128)}), f32[8,16,256]{2,1,0:T(8,128)S(1)}, u32[]{:S(2)}, u32[]{:S(2)}) async-start(f32[8,16,256]{2,1,0:T(8,128)} %shard_map.111), calls=%async_computation.5 | async-start | bytes 262144 | tf_op jit(solution)/shard_map/all_to_all | solution.py:447
  181.9 5.0 %collective-permute-start.11 = (bf16[16,256]{1,0:T(8,128)(2,1)S(1)}, bf16[16,256]{1,0:T(8,128)(2,1)S(1)}, u32[]{:S(2)}, u32[]{:S(2)}) collective-permute-start(bf16[16,256]{1,0:T(8,128)(2,1)S(1)} %slice.11), channel_id=1, source_target_pairs={{0,4},{4,8},{8,12},{12,16},{16,20},{20,24},{24,28},{28,32},{32,36}... | collective-permute-start | bytes 24584 | tf_op jit(solution)/shard_map/ppermute | solution.py:465
  186.9 0.6 copy-start.6
  186.9 0.7 copy-start.2

commit v4 on v3

--- a/solution.py
+++ b/solution.py
@@ -87,6 +87,17 @@
         copy.wait()
 
 
+def fade_rows(faded):
+    high = faded.astype(BF).astype(F32)
+    row = lax.broadcasted_iota(jnp.int32, (8, faded.shape[1]), 0)
+    return jnp.where(row == 0, high, jnp.where(row == 1, faded - high, 0.0))
+
+
+def fade_of(block):
+    rows = block.shape[0]
+    return block[rows - 8 : rows - 7] + block[rows - 7 : rows - 6]
+
+
 def state_kernel(
     info_ref,
     own_ref,
@@ -98,7 +109,7 @@
     other_ref,
     gap_ref,
     shift_ref,
-    normed_ref,
+    normed_out_ref,
     values_ref,
     opened_ref,
     cum_ref,
@@ -107,9 +118,19 @@
     whole_ref,
     sems,
     both_ref,
+    tokens_ref,
+    normed_ref,
+    token_sems,
 ):
     rows, _ = normed_ref.shape
     cols = gap_ref.shape[1]
+    block = own_ref.shape[0]
+    spots = places(info_ref[1], rows // block)
+    token_copies = [
+        pltpu.make_async_copy(from_ref, tokens_ref.at[k], token_sems.at[k])
+        for k, from_ref in enumerate((own_ref, before_ref, after_ref, far_ref))
+    ]
+    started(token_copies)
     copies = fetches(
         info_ref[0],
         range(mine_ref.shape[0]),
@@ -121,30 +142,27 @@
         sems,
     )
     started(copies)
-    block = own_ref.shape[0]
-    own, before, after, far = places(info_ref[1], rows // block)
-
-    def norm(from_ref, start, i):
-        floats = from_ref[pl.ds(pl.multiple_of(i * 32, 32), 32), :].astype(F32)
-        scale = lax.rsqrt(jnp.mean(floats * floats, axis=-1, keepdims=True) + EPSILON)
-        at = pl.ds(pl.multiple_of(start + i * 32, 32), 32)
-        normed_ref[at, :] = (floats * scale * gain_ref[...]).astype(BF)
-
-    def norm_all(i, carry):
-        norm(own_ref, own * block, i)
-        norm(before_ref, before * block, i)
-        norm(after_ref, after * block, i)
-        norm(far_ref, far * block, i)
-        return carry
-
-    lax.fori_loop(0, block // 32, norm_all, 0)
+    for k, spot in enumerate(spots):
+        token_copies[k].wait()
+
+        def norm(i, carry):
+            floats = tokens_ref[k, pl.ds(pl.multiple_of(i * 32, 32), 32), :].astype(F32)
+            scale = lax.rsqrt(jnp.mean(floats * floats, axis=-1, keepdims=True) + EPSILON)
+            at = pl.ds(pl.multiple_of(spot * block + i * 32, 32), 32)
+            normed_ref[at, :] = (floats * scale * gain_ref[...]).astype(BF)
+            return carry
+
+        lax.fori_loop(0, block // 32, norm, 0)
+    handing = pltpu.make_async_copy(normed_ref, normed_out_ref, token_sems.at[len(spots)])
+    handing.start()
     finished(copies)
     both_ref[...] = dot(normed_ref[...], whole_ref[...].reshape(-1, 2 * cols))
     row = lax.broadcasted_iota(jnp.int32, (CHUNK, CHUNK), 0)
     col = lax.broadcasted_iota(jnp.int32, (CHUNK, CHUNK), 1)
     tril = (row >= col).astype(BF)
-    heads = cols // RDIM
-    for h in range(heads):
+    plane, height, _ = payload_ref.shape
+    slab = height - 8
+    for h in range(cols // RDIM):
         lanes = slice(h * RDIM, (h + 1) * RDIM)
         state = jnp.zeros((RDIM, RDIM), F32)
         faded = jnp.zeros((1, RDIM), F32)
@@ -153,7 +171,8 @@
             pre = both_ref[at, lanes].astype(BF).astype(F32)
             values = both_ref[at, cols + h * RDIM : cols + (h + 1) * RDIM].astype(BF)
             opened = gap_ref[:, lanes] / (1.0 + jnp.exp(pre))
-            decay = jnp.log1p(-opened) + shift_ref[at, h : h + 1]
+            shift = jnp.broadcast_to(shift_ref[h : h + 1, at], (RDIM, CHUNK)).T
+            decay = jnp.log1p(-opened) + shift
             d0, d1 = halves(decay)
             d2 = (decay - d0.astype(F32) - d1.astype(F32)).astype(BF)
             cum = dot(tril, d0) + (dot(tril, d1) + dot(tril, d2))
@@ -165,8 +184,11 @@
             growth_ref[c, :, lanes] = growth
             state = state * jnp.exp(total) + growth
             faded = faded + total
-        payload_ref[:, lanes] = state
-        payload_ref[:, cols + h * RDIM : cols + (h + 1) * RDIM] = jnp.broadcast_to(faded, (RDIM, RDIM))
+        fades = fade_rows(faded)
+        for d in range(plane):
+            block_d = jnp.concatenate([state[d * slab : (d + 1) * slab], fades], axis=0)
+            payload_ref[d, :, lanes] = block_d.astype(BF)
+    handing.wait()
 
 
 def dot_left_t(values, key):
@@ -175,20 +197,17 @@
 
 
 def plane_kernel(got_ref, before_ref, faded_ref, total_ref):
-    rows = got_ref.shape[1]
-    cols = before_ref.shape[2]
+    _, rows, cols = before_ref.shape
     state = jnp.zeros((rows, cols), F32)
     faded = jnp.zeros((1, cols), F32)
     for d in range(got_ref.shape[0]):
-        fade = got_ref[d, :1, cols:]
+        got = got_ref[d].astype(F32)
+        fade = fade_of(got)
         before_ref[d] = state
         faded_ref[d : d + 1, :] = faded
-        state = state * jnp.exp(fade) + got_ref[d, :, :cols]
+        state = state * jnp.exp(fade) + got[:rows]
         faded = faded + fade
-    high = faded.astype(BF).astype(F32)
-    row = lax.broadcasted_iota(jnp.int32, (8, cols), 0)
-    fades = jnp.where(row == 0, high, jnp.where(row == 1, faded - high, 0.0))
-    total = jnp.concatenate([state, fades], axis=0).astype(BF)
+    total = jnp.concatenate([state, fade_rows(faded)], axis=0).astype(BF)
     for z in range(total_ref.shape[0]):
         total_ref[z] = total
 
@@ -199,10 +218,10 @@
     state = jnp.zeros((rows, cols), F32)
     for z in range(planes):
         got = totals_ref[z].astype(F32)
-        fade = got[rows : rows + 1] + got[rows + 1 : rows + 2]
-        state = jnp.where(z < info_ref[4], state * jnp.exp(fade) + got[:rows], state)
+        new = state * jnp.exp(fade_of(got)) + got[:rows]
+        state = jnp.where(z < info_ref[4], new, state)
     for d in range(devices):
-        start_ref[d] = before_ref[d] + jnp.exp(faded_ref[d : d + 1, :]) * state
+        start_ref[d] = (before_ref[d] + jnp.exp(faded_ref[d : d + 1, :]) * state).astype(BF)
 
 
 def inner_kernel(
@@ -219,8 +238,12 @@
     whole_ref,
     sems,
     both_ref,
+    held_ref,
+    held_sem,
 ):
     rows, cols = values_ref.shape
+    bringing = pltpu.make_async_copy(normed_ref, held_ref, held_sem.at[0])
+    bringing.start()
     copies = fetches(
         info_ref[0],
         places(info_ref[3], mine_ref.shape[0]),
@@ -233,7 +256,8 @@
     )
     started(copies)
     finished(copies)
-    both_ref[...] = dot(normed_ref[...], whole_ref[...].reshape(-1, 2 * cols))
+    bringing.wait()
+    both_ref[...] = dot(held_ref[...], whole_ref[...].reshape(-1, 2 * cols))
     pooled_ref[...] = both_ref[:, cols:].astype(BF)
     row = lax.broadcasted_iota(jnp.int32, (CHUNK, CHUNK), 0)
     col = lax.broadcasted_iota(jnp.int32, (CHUNK, CHUNK), 1)
@@ -291,7 +315,7 @@
     mixed_ref[:, :cols] = (chosen[RIM:] / divisor - padded[RIM:]).astype(BF)
     for h in range(cols // RDIM):
         lanes = slice(h * RDIM, (h + 1) * RDIM)
-        state = start_ref[:, lanes]
+        state = start_ref[:, lanes].astype(F32)
         for c in range(rows // CHUNK):
             at = slice(c * CHUNK, (c + 1) * CHUNK)
             heard = heard_ref[at, lanes] + dot_wide(decayed_ref[at, lanes], state, NT)
@@ -315,12 +339,18 @@
 HBM = pl.BlockSpec(memory_space=pltpu.HBM)
 
 
-def call(kernel, outs, scratch, flops, moved, *args):
+def spec_of(a):
+    if a.dtype == jnp.int32:
+        return SMEM
+    return HBM if a.size * a.dtype.itemsize >= 1 << 19 and a.dtype == BF else VMEM
+
+
+def call(kernel, outs, scratch, flops, moved, *args, out_specs=None):
     return pl.pallas_call(
         kernel,
         out_shape=outs,
-        in_specs=[SMEM if a.dtype == jnp.int32 else HBM if a.ndim == 5 else VMEM for a in args],
-        out_specs=jax.tree.map(lambda _: VMEM, outs),
+        in_specs=[spec_of(a) for a in args],
+        out_specs=out_specs or jax.tree.map(lambda _: VMEM, outs),
         scratch_shapes=scratch,
         cost_estimate=pl.CostEstimate(flops=flops, bytes_accessed=moved, transcendentals=0),
     )(*args)
@@ -395,6 +425,8 @@
         pltpu.SemaphoreType.DMA((2 * first.shape[0] * first.shape[1],)),
     ]
 
+    plane = lax.axis_size(PLANE)
+    slab = RDIM // plane
     normed, values, opened, cum, growth, payload = call(
         state_kernel,
         [
@@ -403,9 +435,15 @@
             shape((rows, cols), F32),
             shape((rows, cols), F32),
             shape((rows // CHUNK, RDIM, cols), F32),
-            shape((RDIM, 2 * cols), F32),
+            shape((plane, slab + 8, cols), BF),
         ],
-        [*whole, pltpu.VMEM((rows, 2 * cols), F32)],
+        [
+            *whole,
+            pltpu.VMEM((rows, 2 * cols), F32),
+            pltpu.VMEM((tp, rows // tp, width), BF),
+            pltpu.VMEM((rows, width), BF),
+            pltpu.SemaphoreType.DMA((tp + 1,)),
+        ],
         4 * rows * width * cols,
         8 << 20,
         info,
@@ -414,11 +452,9 @@
         first,
         first_other,
         forget_gap[None, :],
-        decay_shift.T,
-    )
-
-    plane = lax.axis_size(PLANE)
-    slab = RDIM // plane
+        decay_shift,
+        out_specs=[HBM, VMEM, VMEM, VMEM, VMEM, VMEM],
+    )
     got = lax.all_to_all(payload, PLANE, split_axis=0, concat_axis=0, tiled=True)
     before, faded, total = call(
         plane_kernel,
@@ -430,12 +466,12 @@
         [],
         1 << 20,
         1 << 19,
-        got.reshape(plane, slab, 2 * cols),
+        got,
     )
     totals = lax.all_to_all(total, DEPTH, split_axis=0, concat_axis=0, tiled=True)
     start = call(
         depth_kernel,
-        shape((plane, slab, cols), F32),
+        shape((plane, slab, cols), BF),
         [],
         1 << 20,
         1 << 19,
@@ -450,7 +486,12 @@
     pooled, decayed, heard = call(
         inner_kernel,
         [shape((rows, cols), BF), shape((rows, cols), F32), shape((rows, cols), F32)],
-        [*whole, pltpu.VMEM((rows, 2 * cols), F32)],
+        [
+            *whole,
+            pltpu.VMEM((rows, 2 * cols), F32),
+            pltpu.VMEM((rows, width), BF),
+            pltpu.SemaphoreType.DMA((1,)),
+        ],
         4 * rows * width * cols,
         8 << 20,
         info,

time: 228 us -> 226 us (level)
  blocking collectives: 106 us -> 93.1 us
  starting transfers between devices: 45.3 us -> 51.6 us
  waiting for transfers between devices: 38.6 us -> 43.1 us
    all_to_all x2 -> x1, blocking collectives: 43.4 us -> 31.8 us  [sent_to_all(): return lax.all_to_all(copies, axis, split_axis=0, concat_axis=0, tiled=True)]
    all_to_all x1 -> x2, waiting for transfers between devices: 0.01 us -> 5.52 us  [sent_to_all(): return lax.all_to_all(copies, axis, split_axis=0, concat_axis=0, tiled=True)]
    all_to_all x1 -> x2, starting transfers between devices: 4.77 us -> 9.12 us  [sent_to_all(): return lax.all_to_all(copies, axis, split_axis=0, concat_axis=0, tiled=True)]
  transfers between devices with their start and end apart: 14 -> 15, of which waited for: 9 -> 10; matrix products, arithmetic and copies ran while one was open for 2% -> 2% of each run, Pallas kernels for 8% -> 9%
where the time goes in v4:
time: 226 us; the launch traced here: 224 us
  blocking collectives  93.1 us (41%)
  starting transfers between devices  51.6 us (23%)
  waiting for transfers between devices  43.1 us (19%)
  Pallas kernels  26.7 us (12%)
  other arithmetic  4.75 us (2%)
  local copies, waits for them, and re-layouts  4.23 us (2%)
    ppermute x9, waiting for transfers between devices, ring_gather(): lax.ppermute(x, axis, [(i, (i + shift) % n) for i in range(n)])  34.6 us
    all_to_all x1, blocking collectives, sent_to_all(): return lax.all_to_all(copies, axis, split_axis=0, concat_axis=0, tiled=True)  31.8 us
    ppermute x9, starting transfers between devices, ring_gather(): lax.ppermute(x, axis, [(i, (i + shift) % n) for i in range(n)])  31.3 us
    all_to_all x1, blocking collectives, layer(): lax.all_to_all(part.reshape(tp, rows // tp, width), 'tp', split_axis=0, c...  29.9 us
    pallas_call x5, Pallas kernels, call(): pl.pallas_call(kernel, out_shape=outs, in_specs=[spec_of(a) for a in args...  26.7 us
    all_to_all x1, blocking collectives, layer(): lax.all_to_all(total, DEPTH, split_axis=0, concat_axis=0, tiled=True)  22.8 us
    all_to_all x2, starting transfers between devices, sent_to_all(): return lax.all_to_all(copies, axis, split_axis=0, concat_axis=0, tiled=True)  9.12 us
    all_to_all x1, blocking collectives, layer(): lax.all_to_all(payload, PLANE, split_axis=0, concat_axis=0, tiled=True)  8.62 us
  transfers between devices with their start and end apart: 15, of which 10 were waited for; matrix products, arithmetic and copies ran while one was open for 2% of the time, Pallas kernels for 9%

profile of v4, /device:TPU:6, one launch (start us, length us, event | category | flops | bytes accessed | tf_op | source)
XLA Modules:
  0.0 223.7 jit_solution(8869005074455790531)
XLA Ops:
  0.0 0.8 pad_add_fusion
  0.8 31.8 %all_to_all.38 = bf16[4,16,1536]{2,1,0:T(8,128)(2,1)S(1)} all-to-all(bf16[4,16,1536]{2,1,0:T(8,128)(2,1)S(1)} %broadcast_in_dim.19), channel_id=1, replica_groups=mesh['sp_f'=4,'sp_n'=4,'sp_x'=4,'sp_c'=2,'tp'=4] {'sp_f'}, dimensions={0} | all-to-all | bytes 393216 | tf_op jit(solution)/shard_map/all_to_all | solution.py:49
  32.6 0.7 broadcast_in_dim.20
  33.4 4.6 %all-to-all-start.1 = ((bf16[4,4,16,512]{3,2,1,0:T(8,128)(2,1)}), bf16[4,4,16,512]{3,2,1,0:T(8,128)(2,1)S(1)}, u32[]{:S(2)}, u32[]{:S(2)}) async-start(bf16[4,4,16,512]{3,2,1,0:T(8,128)(2,1)} %broadcast_in_dim.20), calls=%async_computation.1 | async-start | bytes 524288 | tf_op jit(solution)/shard_map/all_to_all | solution.py:49
  38.0 4.2 %collective-permute-start.6 = (bf16[4,16,1024]{2,1,0:T(8,128)(2,1)S(1)}, bf16[4,16,1024]{2,1,0:T(8,128)(2,1)S(1)}, u32[]{:S(2)}, u32[]{:S(2)}) collective-permute-start(bf16[4,16,1024]{2,1,0:T(8,128)(2,1)S(1)} %get-tuple-element.32), channel_id=1, source_target_pairs={{0,448},{32,480},{64,0},{96,32},{128,64},{160,96},{192,128},{224,1... | collective-permute-start | bytes 393224 | tf_op jit(solution)/shard_map/ppermute | solution.py:56
  42.2 2.5 %collective-permute-start.5 = (bf16[4,16,1024]{2,1,0:T(8,128)(2,1)S(1)}, bf16[4,16,1024]{2,1,0:T(8,128)(2,1)S(1)}, u32[]{:S(2)}, u32[]{:S(2)}) collective-permute-start(bf16[4,16,1024]{2,1,0:T(8,128)(2,1)S(1)} %get-tuple-element.32), channel_id=1, source_target_pairs={{0,480},{32,0},{64,32},{96,64},{128,96},{160,128},{192,160},{224,1... | collective-permute-start | bytes 393224 | tf_op jit(solution)/shard_map/ppermute | solution.py:56
  44.6 3.4 %collective-permute-start.4 = (bf16[4,16,1024]{2,1,0:T(8,128)(2,1)S(1)}, bf16[4,16,1024]{2,1,0:T(8,128)(2,1)S(1)}, u32[]{:S(2)}, u32[]{:S(2)}) collective-permute-start(bf16[4,16,1024]{2,1,0:T(8,128)(2,1)S(1)} %get-tuple-element.32), channel_id=1, source_target_pairs={{0,32},{32,64},{64,96},{96,128},{128,160},{160,192},{192,224},{224... | collective-permute-start | bytes 393224 | tf_op jit(solution)/shard_map/ppermute | solution.py:56
  48.0 4.2 %collective-permute-done.6 = bf16[4,16,1024]{2,1,0:T(8,128)(2,1)S(1)} collective-permute-done((bf16[4,16,1024]{2,1,0:T(8,128)(2,1)S(1)}, bf16[4,16,1024]{2,1,0:T(8,128)(2,1)S(1)}, u32[]{:S(2)}, u32[]{:S(2)}) %collective-permute-start.6) | collective-permute-done | bytes 131104 | tf_op jit(solution)/shard_map/ppermute | solution.py:56
  52.2 0.0 collective-permute-done.5
  52.2 0.5 collective-permute-done.4
  52.7 0.9 fusion
  53.6 3.3 %collective-permute-start.9 = (bf16[4,4,16,1024]{3,2,1,0:T(8,128)(2,1)S(1)}, bf16[4,4,16,1024]{3,2,1,0:T(8,128)(2,1)S(1)}, u32[]{:S(2)}, u32[]{:S(2)}) collective-permute-start(bf16[4,4,16,1024]{3,2,1,0:T(8,128)(2,1)S(1)} %get-tuple-element.30), channel_id=1, source_target_pairs={{0,16},{8,24},{16,0},{24,8},{1,17},{9,25},{17,1},{25,9},{2,18},{10... | collective-permute-start | bytes 1572872 | tf_op jit(solution)/shard_map/ppermute | solution.py:56
  56.9 1.9 collective-permute-start.8
  58.8 5.1 %collective-permute-start.7 = (bf16[4,4,16,1024]{3,2,1,0:T(8,128)(2,1)S(1)}, bf16[4,4,16,1024]{3,2,1,0:T(8,128)(2,1)}, u32[]{:S(2)}, u32[]{:S(2)}) collective-permute-start(bf16[4,4,16,1024]{3,2,1,0:T(8,128)(2,1)S(1)} %get-tuple-element.30), channel_id=1, source_target_pairs={{0,8},{8,16},{16,24},{24,0},{1,9},{9,17},{17,25},{25,1},{2,10},{10... | collective-permute-start | bytes 1572872 | tf_op jit(solution)/shard_map/ppermute | solution.py:56
  64.0 0.0 all-to-all-done.1
  64.0 1.1 broadcast_in_dim.21
  65.1 4.5 %all-to-all-start.2 = ((bf16[4,4,4,16,512]{4,3,2,1,0:T(8,128)(2,1)}), bf16[4,4,4,16,512]{4,3,2,1,0:T(8,128)(2,1)S(1)}, u32[]{:S(2)}, u32[]{:S(2)}) async-start(bf16[4,4,4,16,512]{4,3,2,1,0:T(8,128)(2,1)} %broadcast_in_dim.21), calls=%async_computation.2 | async-start | bytes 2097152 | tf_op jit(solution)/shard_map/all_to_all | solution.py:49
  69.6 2.2 collective-permute-done.9
  71.8 0.0 copy-start.2
  71.8 8.7 %collective-permute-done.8 = bf16[4,4,16,1024]{3,2,1,0:T(8,128)(2,1)S(1)} collective-permute-done((bf16[4,4,16,1024]{3,2,1,0:T(8,128)(2,1)S(1)}, bf16[4,4,16,1024]{3,2,1,0:T(8,128)(2,1)S(1)}, u32[]{:S(2)}, u32[]{:S(2)}) %collective-permute-start.8) | collective-permute-done | bytes 524320 | tf_op jit(solution)/shard_map/ppermute | solution.py:56
  80.5 0.0 copy-start.3
  80.5 0.4 collective-permute-done.7
  80.9 0.0 copy-done.2
  80.9 0.4 copy-done.3
  81.3 1.8 pad_maximum_fusion.mine_ref
  83.1 0.0 copy-start
  83.1 1.9 collective-permute-start.10
  85.0 5.5 %all-to-all-done.2.mine_ref = bf16[4,4,4,16,512]{4,3,2,1,0:T(8,128)(2,1)S(1)} async-done(((bf16[4,4,4,16,512]{4,3,2,1,0:T(8,128)(2,1)}), bf16[4,4,4,16,512]{4,3,2,1,0:T(8,128)(2,1)S(1)}, u32[]{:S(2)}, u32[]{:S(2)}) %all-to-all-start.2) | async-done | bytes 1048608 | tf_op jit(solution)/shard_map/all_to_all | solution.py:49
  90.5 0.0 copy-start.1
  90.5 1.9 collective-permute-start.3
  92.5 3.5 %collective-permute-start = (bf16[128,2048]{1,0:T(8,128)(2,1)}, bf16[128,2048]{1,0:T(8,128)(2,1)}, u32[]{:S(2)}, u32[]{:S(2)}) collective-permute-start(bf16[128,2048]{1,0:T(8,128)(2,1)} %own_ref.1), channel_id=1, source_target_pairs={{0,1},{1,2},{2,3},{3,0},{4,5},{5,6},{6,7},{7,4},{8,9},{9,10},{10,1... | collective-permute-start | bytes 1572872 | tf_op jit(solution)/shard_map/ppermute | solution.py:56
  96.0 3.6 %collective-permute-start.1 = (bf16[128,2048]{1,0:T(8,128)(2,1)}, bf16[128,2048]{1,0:T(8,128)(2,1)}, u32[]{:S(2)}, u32[]{:S(2)}) collective-permute-start(bf16[128,2048]{1,0:T(8,128)(2,1)} %own_ref.1), channel_id=1, source_target_pairs={{0,3},{1,0},{2,1},{3,2},{4,7},{5,4},{6,5},{7,6},{8,11},{9,8},{10,9... | collective-permute-start | bytes 1572872 | tf_op jit(solution)/shard_map/ppermute | solution.py:56
  99.5 3.9 %collective-permute-start.2 = (bf16[128,2048]{1,0:T(8,128)(2,1)}, bf16[128,2048]{1,0:T(8,128)(2,1)}, u32[]{:S(2)}, u32[]{:S(2)}) collective-permute-start(bf16[128,2048]{1,0:T(8,128)(2,1)} %own_ref.1), channel_id=1, source_target_pairs={{0,2},{1,3},{2,0},{3,1},{4,6},{5,7},{6,4},{7,5},{8,10},{9,11},{10,... | collective-permute-start | bytes 1572872 | tf_op jit(solution)/shard_map/ppermute | solution.py:56
  103.5 0.6 stack.57.info_ref
  104.1 6.2 %collective-permute-done.before_ref = bf16[128,2048]{1,0:T(8,128)(2,1)} collective-permute-done((bf16[128,2048]{1,0:T(8,128)(2,1)}, bf16[128,2048]{1,0:T(8,128)(2,1)}, u32[]{:S(2)}, u32[]{:S(2)}) %collective-permute-start) | collective-permute-done | bytes 524320 | tf_op jit(solution)/shard_map/ppermute | solution.py:56
  110.3 2.7 %collective-permute-done.1.after_ref = bf16[128,2048]{1,0:T(8,128)(2,1)} collective-permute-done((bf16[128,2048]{1,0:T(8,128)(2,1)}, bf16[128,2048]{1,0:T(8,128)(2,1)}, u32[]{:S(2)}, u32[]{:S(2)}) %collective-permute-start.1) | collective-permute-done | bytes 524320 | tf_op jit(solution)/shard_map/ppermute | solution.py:56
  113.0 9.7 %collective-permute-done.2.far_ref = bf16[128,2048]{1,0:T(8,128)(2,1)} collective-permute-done((bf16[128,2048]{1,0:T(8,128)(2,1)}, bf16[128,2048]{1,0:T(8,128)(2,1)}, u32[]{:S(2)}, u32[]{:S(2)}) %collective-permute-start.2) | collective-permute-done | bytes 524320 | tf_op jit(solution)/shard_map/ppermute | solution.py:56
  122.7 0.0 collective-permute-done.3.other_ref
  122.7 0.0 copy-done.1
  122.7 9.5 %shard_map.109 = (bf16[512,2048]{1,0:T(8,128)(2,1)}, bf16[512,256]{1,0:T(8,128)(2,1)}, f32[512,256]{1,0:T(8,128)}, f32[512,256]{1,0:T(8,128)}, f32[4,128,256]{2,1,0:T(8,128)}, /*index=5*/bf16[8,24,256]{2,1,0:T(8,128)(2,1)}) custom-call(s32[6]{0:T(128)} %stack.57.info_ref, bf16[128,2048]{1,0:T(8,128)(2,1)} %own_ref.1, ...), custom_call_target="tpu_custom_call" | custom-call | flops 1073741824 | bytes 8388608 | tf_op jit(solution)/shard_map/pallas_call | solution.py:349
  132.2 0.0 copy-done
  132.2 8.6 %all_to_all.39.got_ref = bf16[8,24,256]{2,1,0:T(8,128)(2,1)} all-to-all(bf16[8,24,256]{2,1,0:T(8,128)(2,1)} %get-tuple-element.17), channel_id=1, replica_groups=mesh['sp_f'=4,'sp_n'=4,'sp_x'=4,'sp_c'=2,'tp'=4] {'sp_x','sp_c'}, dimensions={0} | all-to-all | bytes 196608 | tf_op jit(solution)/shard_map/all_to_all | solution.py:458
  140.9 1.7 shard_map.110
  142.5 22.8 %all_to_all.40.totals_ref = bf16[16,24,256]{2,1,0:T(8,128)(2,1)} all-to-all(bf16[16,24,256]{2,1,0:T(8,128)(2,1)} %get-tuple-element.18), channel_id=1, replica_groups=mesh['sp_f'=4,'sp_n'=4,'sp_x'=4,'sp_c'=2,'tp'=4] {'sp_f','sp_n'}, dimensions={0} | all-to-all | bytes 393216 | tf_op jit(solution)/shard_map/all_to_all | solution.py:471
  165.3 1.7 shard_map.111
  167.0 5.4 %all-to-all-start.5 = ((bf16[8,16,256]{2,1,0:T(8,128)(2,1)}), bf16[8,16,256]{2,1,0:T(8,128)(2,1)S(1)}, u32[]{:S(2)}, u32[]{:S(2)}) async-start(bf16[8,16,256]{2,1,0:T(8,128)(2,1)} %shard_map.111), calls=%async_computation.5 | async-start | bytes 131072 | tf_op jit(solution)/shard_map/all_to_all | solution.py:483
  172.4 0.0 collective-permute-done.10.other_ref
  172.4 7.7 %shard_map.112 = (bf16[512,256]{1,0:T(8,128)(2,1)}, f32[512,256]{1,0:T(8,128)}, f32[512,256]{1,0:T(8,128)}) custom-call(s32[6]{0:T(128)} %stack.57.info_ref, bf16[512,2048]{1,0:T(8,128)(2,1)} %get-tuple-element.23.normed_ref, bf16[4,4,4,16,1024]{4,3,2,1,0:T(8,128)(2,1)} %copy-done, bf16[4,4,4,16,1024]{4,3,2,1,0:T(8,128)(2,1)} %collective-permute-done.10.other_ref, ...), custom_call_target="tpu_custom_call" | custom-call | flops 1073741824 | bytes 8388608 | tf_op jit(solution)/shard_map/pallas_call | solution.py:349
  180.1 0.7 slice.11
  180.8 2.0 collective-permute-start.11
  182.8 2.9 %collective-permute-done.11.rim_ref = bf16[16,256]{1,0:T(8,128)(2,1)S(1)} collective-permute-done((bf16[16,256]{1,0:T(8,128)(2,1)S(1)}, bf16[16,256]{1,0:T(8,128)(2,1)S(1)}, u32[]{:S(2)}, u32[]{:S(2)}) %collective-permute-start.11) | collective-permute-done | bytes 8224 | tf_op jit(solution)/shard_map/ppermute | solution.py:506
  185.7 0.0 copy-start.5
  185.7 0.0 all-to-all-done.5
  185.7 0.0 copy-start.4
  185.7 0.6 copy-done.5
  186.3 0.0 copy-done.4
  186.4 6.2 %shard_map.113 = bf16[512,2048]{1,0:T(8,128)(2,1)} custom-call(s32[6]{0:T(128)} %stack.57.info_ref, bf16[128,256]{1,0:T(8,128)(2,1)} %bitcast.26, f32[4,128,256]{2,1,0:T(8,128)} %get-tuple-element.21.growth_ref, f32[512,256]{1,0:T(8,128)} %get-tuple-element.22.cum_ref, f32[512,256]{1,0:T(8,128)} %get-tuple-element.26.decayed_ref, ...), custom_call_target="tpu_custom_call" | custom-call | flops 1073741824 | bytes 8388608 | tf_op jit(solution)/shard_map/pallas_call | solution.py:349
  192.5 29.9 %all_to_all.41 = bf16[4,128,2048]{2,1,0:T(8,128)(2,1)S(1)} all-to-all(bf16[4,128,2048]{2,1,0:T(8,128)(2,1)} %bitcast.23), channel_id=1, replica_groups=mesh['sp_f'=4,'sp_n'=4,'sp_x'=4,'sp_c'=2,'tp'=4] {'tp'}, dimensions={0} | all-to-all | bytes 4194304 | tf_op jit(solution)/shard_map/all_to_all | solution.py:525
  222.4 1.3 reduce_sum.12
  (3 shorter events, 0.0 us)
Async XLA Ops:
  33.4 30.6 %all-to-all-start.1 = ((bf16[4,4,16,512]{3,2,1,0:T(8,128)(2,1)}), bf16[4,4,16,512]{3,2,1,0:T(8,128)(2,1)S(1)}, u32[]{:S(2)}, u32[]{:S(2)}) async-start(bf16[4,4,16,512]{3,2,1,0:T(8,128)(2,1)} %broadcast_in_dim.20), calls=%async_computation.1 | async-start | bytes 524288 | tf_op jit(solution)/shard_map/all_to_all | solution.py:49
  38.0 14.2 %collective-permute-start.6 = (bf16[4,16,1024]{2,1,0:T(8,128)(2,1)S(1)}, bf16[4,16,1024]{2,1,0:T(8,128)(2,1)S(1)}, u32[]{:S(2)}, u32[]{:S(2)}) collective-permute-start(bf16[4,16,1024]{2,1,0:T(8,128)(2,1)S(1)} %get-tuple-element.32), channel_id=1, source_target_pairs={{0,448},{32,480},{64,0},{96,32},{128,64},{160,96},{192,128},{224,1... | collective-permute-start | bytes 393224 | tf_op jit(solution)/shard_map/ppermute | solution.py:56
  42.2 10.1 %collective-permute-start.5 = (bf16[4,16,1024]{2,1,0:T(8,128)(2,1)S(1)}, bf16[4,16,1024]{2,1,0:T(8,128)(2,1)S(1)}, u32[]{:S(2)}, u32[]{:S(2)}) collective-permute-start(bf16[4,16,1024]{2,1,0:T(8,128)(2,1)S(1)} %get-tuple-element.32), channel_id=1, source_target_pairs={{0,480},{32,0},{64,32},{96,64},{128,96},{160,128},{192,160},{224,1... | collective-permute-start | bytes 393224 | tf_op jit(solution)/shard_map/ppermute | solution.py:56
  44.6 8.1 %collective-permute-start.4 = (bf16[4,16,1024]{2,1,0:T(8,128)(2,1)S(1)}, bf16[4,16,1024]{2,1,0:T(8,128)(2,1)S(1)}, u32[]{:S(2)}, u32[]{:S(2)}) collective-permute-start(bf16[4,16,1024]{2,1,0:T(8,128)(2,1)S(1)} %get-tuple-element.32), channel_id=1, source_target_pairs={{0,32},{32,64},{64,96},{96,128},{128,160},{160,192},{192,224},{224... | collective-permute-start | bytes 393224 | tf_op jit(solution)/shard_map/ppermute | solution.py:56
  53.6 18.2 %collective-permute-start.9 = (bf16[4,4,16,1024]{3,2,1,0:T(8,128)(2,1)S(1)}, bf16[4,4,16,1024]{3,2,1,0:T(8,128)(2,1)S(1)}, u32[]{:S(2)}, u32[]{:S(2)}) collective-permute-start(bf16[4,4,16,1024]{3,2,1,0:T(8,128)(2,1)S(1)} %get-tuple-element.30), channel_id=1, source_target_pairs={{0,16},{8,24},{16,0},{24,8},{1,17},{9,25},{17,1},{25,9},{2,18},{10... | collective-permute-start | bytes 1572872 | tf_op jit(solution)/shard_map/ppermute | solution.py:56
  56.9 23.6 %collective-permute-start.8 = (bf16[4,4,16,1024]{3,2,1,0:T(8,128)(2,1)S(1)}, bf16[4,4,16,1024]{3,2,1,0:T(8,128)(2,1)S(1)}, u32[]{:S(2)}, u32[]{:S(2)}) collective-permute-start(bf16[4,4,16,1024]{3,2,1,0:T(8,128)(2,1)S(1)} %get-tuple-element.30), channel_id=1, source_target_pairs={{0,24},{8,0},{16,8},{24,16},{1,25},{9,1},{17,9},{25,17},{2,26},{10... | collective-permute-start | bytes 1572872 | tf_op jit(solution)/shard_map/ppermute | solution.py:56
  58.8 22.1 %collective-permute-start.7 = (bf16[4,4,16,1024]{3,2,1,0:T(8,128)(2,1)S(1)}, bf16[4,4,16,1024]{3,2,1,0:T(8,128)(2,1)}, u32[]{:S(2)}, u32[]{:S(2)}) collective-permute-start(bf16[4,4,16,1024]{3,2,1,0:T(8,128)(2,1)S(1)} %get-tuple-element.30), channel_id=1, source_target_pairs={{0,8},{8,16},{16,24},{24,0},{1,9},{9,17},{17,25},{25,1},{2,10},{10... | collective-permute-start | bytes 1572872 | tf_op jit(solution)/shard_map/ppermute | solution.py:56
  65.1 25.4 %all-to-all-start.2 = ((bf16[4,4,4,16,512]{4,3,2,1,0:T(8,128)(2,1)}), bf16[4,4,4,16,512]{4,3,2,1,0:T(8,128)(2,1)S(1)}, u32[]{:S(2)}, u32[]{:S(2)}) async-start(bf16[4,4,4,16,512]{4,3,2,1,0:T(8,128)(2,1)} %broadcast_in_dim.21), calls=%async_computation.2 | async-start | bytes 2097152 | tf_op jit(solution)/shard_map/all_to_all | solution.py:49
  71.8 9.1 %copy-start.2 = (bf16[4,4,16,1024]{3,2,1,0:T(8,128)(2,1)}, bf16[4,4,16,1024]{3,2,1,0:T(8,128)(2,1)S(1)}, u32[]{:S(2)}) copy-start(bf16[4,4,16,1024]{3,2,1,0:T(8,128)(2,1)S(1)} %collective-permute-done.9) | copy-start | bytes 1572868
  80.5 0.8 copy-start.3
  83.1 49.1 %copy-start = (bf16[4,4,4,16,1024]{4,3,2,1,0:T(8,128)(2,1)}, bf16[4,4,4,16,1024]{4,3,2,1,0:T(8,128)(2,1)S(1)}, u32[]{:S(2)}) copy-start(bf16[4,4,4,16,1024]{4,3,2,1,0:T(8,128)(2,1)S(1)} %pad_maximum_fusion.mine_ref) | copy-start | bytes 6291460
  83.1 89.3 %collective-permute-start.10 = (bf16[4,4,4,16,1024]{4,3,2,1,0:T(8,128)(2,1)S(1)}, bf16[4,4,4,16,1024]{4,3,2,1,0:T(8,128)(2,1)}, u32[]{:S(2)}, u32[]{:S(2)}) collective-permute-start(bf16[4,4,4,16,1024]{4,3,2,1,0:T(8,128)(2,1)S(1)} %pad_maximum_fusion.mine_ref), channel_id=1, source_target_pairs={{0,4},{4,0},{1,5},{5,1},{2,6},{6,2},{3,7},{7,3},{8,12},{12,8},{9,1... | collective-permute-start | bytes 6291464 | tf_op jit(solution)/shard_map/ppermute | solution.py:374
  90.5 32.2 %copy-start.1 = (bf16[4,4,4,16,512]{4,3,2,1,0:T(8,128)(2,1)}, bf16[4,4,4,16,512]{4,3,2,1,0:T(8,128)(2,1)S(1)}, u32[]{:S(2)}) copy-start(bf16[4,4,4,16,512]{4,3,2,1,0:T(8,128)(2,1)S(1)} %all-to-all-done.2.mine_ref) | copy-start | bytes 3145732
  90.5 32.1 %collective-permute-start.3 = (bf16[4,4,4,16,512]{4,3,2,1,0:T(8,128)(2,1)S(1)}, bf16[4,4,4,16,512]{4,3,2,1,0:T(8,128)(2,1)}, u32[]{:S(2)}, u32[]{:S(2)}) collective-permute-start(bf16[4,4,4,16,512]{4,3,2,1,0:T(8,128)(2,1)S(1)} %all-to-all-done.2.mine_ref), channel_id=1, source_target_pairs={{0,4},{4,0},{1,5},{5,1},{2,6},{6,2},{3,7},{7,3},{8,12},{12,8},{9,1... | collective-permute-start | bytes 3145736 | tf_op jit(solution)/shard_map/ppermute | solution.py:374
  92.5 17.8 %collective-permute-start = (bf16[128,2048]{1,0:T(8,128)(2,1)}, bf16[128,2048]{1,0:T(8,128)(2,1)}, u32[]{:S(2)}, u32[]{:S(2)}) collective-permute-start(bf16[128,2048]{1,0:T(8,128)(2,1)} %own_ref.1), channel_id=1, source_target_pairs={{0,1},{1,2},{2,3},{3,0},{4,5},{5,6},{6,7},{7,4},{8,9},{9,10},{10,1... | collective-permute-start | bytes 1572872 | tf_op jit(solution)/shard_map/ppermute | solution.py:56
  96.0 17.0 %collective-permute-start.1 = (bf16[128,2048]{1,0:T(8,128)(2,1)}, bf16[128,2048]{1,0:T(8,128)(2,1)}, u32[]{:S(2)}, u32[]{:S(2)}) collective-permute-start(bf16[128,2048]{1,0:T(8,128)(2,1)} %own_ref.1), channel_id=1, source_target_pairs={{0,3},{1,0},{2,1},{3,2},{4,7},{5,4},{6,5},{7,6},{8,11},{9,8},{10,9... | collective-permute-start | bytes 1572872 | tf_op jit(solution)/shard_map/ppermute | solution.py:56
  99.5 23.2 %collective-permute-start.2 = (bf16[128,2048]{1,0:T(8,128)(2,1)}, bf16[128,2048]{1,0:T(8,128)(2,1)}, u32[]{:S(2)}, u32[]{:S(2)}) collective-permute-start(bf16[128,2048]{1,0:T(8,128)(2,1)} %own_ref.1), channel_id=1, source_target_pairs={{0,2},{1,3},{2,0},{3,1},{4,6},{5,7},{6,4},{7,5},{8,10},{9,11},{10,... | collective-permute-start | bytes 1572872 | tf_op jit(solution)/shard_map/ppermute | solution.py:56
  167.0 18.7 %all-to-all-start.5 = ((bf16[8,16,256]{2,1,0:T(8,128)(2,1)}), bf16[8,16,256]{2,1,0:T(8,128)(2,1)S(1)}, u32[]{:S(2)}, u32[]{:S(2)}) async-start(bf16[8,16,256]{2,1,0:T(8,128)(2,1)} %shard_map.111), calls=%async_computation.5 | async-start | bytes 131072 | tf_op jit(solution)/shard_map/all_to_all | solution.py:483
  180.8 5.0 %collective-permute-start.11 = (bf16[16,256]{1,0:T(8,128)(2,1)S(1)}, bf16[16,256]{1,0:T(8,128)(2,1)S(1)}, u32[]{:S(2)}, u32[]{:S(2)}) collective-permute-start(bf16[16,256]{1,0:T(8,128)(2,1)S(1)} %slice.11), channel_id=1, source_target_pairs={{0,4},{4,8},{8,12},{12,16},{16,20},{20,24},{24,28},{28,32},{32,36}... | collective-permute-start | bytes 24584 | tf_op jit(solution)/shard_map/ppermute | solution.py:506
  185.7 0.6 copy-start.5
  185.7 0.6 copy-start.4

commit v5 on v4

--- a/solution.py
+++ b/solution.py
@@ -145,14 +145,11 @@
     for k, spot in enumerate(spots):
         token_copies[k].wait()
 
-        def norm(i, carry):
-            floats = tokens_ref[k, pl.ds(pl.multiple_of(i * 32, 32), 32), :].astype(F32)
+        for i in range(block // 32):
+            floats = tokens_ref[k, i * 32 : (i + 1) * 32, :].astype(F32)
             scale = lax.rsqrt(jnp.mean(floats * floats, axis=-1, keepdims=True) + EPSILON)
             at = pl.ds(pl.multiple_of(spot * block + i * 32, 32), 32)
             normed_ref[at, :] = (floats * scale * gain_ref[...]).astype(BF)
-            return carry
-
-        lax.fori_loop(0, block // 32, norm, 0)
     handing = pltpu.make_async_copy(normed_ref, normed_out_ref, token_sems.at[len(spots)])
     handing.start()
     finished(copies)

time: 226 us -> 225 us (level)
  no operation moved by 1% of the time
where the time goes in v5:
time: 225 us; the launch traced here: 223 us
  blocking collectives  93.1 us (41%)
  starting transfers between devices  51.6 us (23%)
  waiting for transfers between devices  43.1 us (19%)
  Pallas kernels  25.5 us (11%)
  other arithmetic  4.75 us (2%)
  local copies, waits for them, and re-layouts  4.23 us (2%)
    ppermute x9, waiting for transfers between devices, ring_gather(): lax.ppermute(x, axis, [(i, (i + shift) % n) for i in range(n)])  34.6 us
    all_to_all x1, blocking collectives, sent_to_all(): return lax.all_to_all(copies, axis, split_axis=0, concat_axis=0, tiled=True)  31.8 us
    ppermute x9, starting transfers between devices, ring_gather(): lax.ppermute(x, axis, [(i, (i + shift) % n) for i in range(n)])  31.3 us
    all_to_all x1, blocking collectives, layer(): lax.all_to_all(part.reshape(tp, rows // tp, width), 'tp', split_axis=0, c...  29.9 us
    pallas_call x5, Pallas kernels, call(): pl.pallas_call(kernel, out_shape=outs, in_specs=[spec_of(a) for a in args...  25.5 us
    all_to_all x1, blocking collectives, layer(): lax.all_to_all(total, DEPTH, split_axis=0, concat_axis=0, tiled=True)  22.8 us
    all_to_all x2, starting transfers between devices, sent_to_all(): return lax.all_to_all(copies, axis, split_axis=0, concat_axis=0, tiled=True)  9.12 us
    all_to_all x1, blocking collectives, layer(): lax.all_to_all(payload, PLANE, split_axis=0, concat_axis=0, tiled=True)  8.62 us
  transfers between devices with their start and end apart: 15, of which 10 were waited for; matrix products, arithmetic and copies ran while one was open for 2% of the time, Pallas kernels for 9%

profile of v5, /device:TPU:6, one launch (start us, length us, event | category | flops | bytes accessed | tf_op | source)
XLA Modules:
  0.0 222.5 jit_solution(8677495717730610505)
XLA Ops:
  0.0 0.8 pad_add_fusion
  0.8 31.8 %all_to_all.38 = bf16[4,16,1536]{2,1,0:T(8,128)(2,1)S(1)} all-to-all(bf16[4,16,1536]{2,1,0:T(8,128)(2,1)S(1)} %broadcast_in_dim.19), channel_id=1, replica_groups=mesh['sp_f'=4,'sp_n'=4,'sp_x'=4,'sp_c'=2,'tp'=4] {'sp_f'}, dimensions={0} | all-to-all | bytes 393216 | tf_op jit(solution)/shard_map/all_to_all | solution.py:49
  32.6 0.7 broadcast_in_dim.20
  33.4 4.6 %all-to-all-start.1 = ((bf16[4,4,16,512]{3,2,1,0:T(8,128)(2,1)}), bf16[4,4,16,512]{3,2,1,0:T(8,128)(2,1)S(1)}, u32[]{:S(2)}, u32[]{:S(2)}) async-start(bf16[4,4,16,512]{3,2,1,0:T(8,128)(2,1)} %broadcast_in_dim.20), calls=%async_computation.1 | async-start | bytes 524288 | tf_op jit(solution)/shard_map/all_to_all | solution.py:49
  38.0 4.2 %collective-permute-start.6 = (bf16[4,16,1024]{2,1,0:T(8,128)(2,1)S(1)}, bf16[4,16,1024]{2,1,0:T(8,128)(2,1)S(1)}, u32[]{:S(2)}, u32[]{:S(2)}) collective-permute-start(bf16[4,16,1024]{2,1,0:T(8,128)(2,1)S(1)} %get-tuple-element.32), channel_id=1, source_target_pairs={{0,448},{32,480},{64,0},{96,32},{128,64},{160,96},{192,128},{224,1... | collective-permute-start | bytes 393224 | tf_op jit(solution)/shard_map/ppermute | solution.py:56
  42.2 2.5 %collective-permute-start.5 = (bf16[4,16,1024]{2,1,0:T(8,128)(2,1)S(1)}, bf16[4,16,1024]{2,1,0:T(8,128)(2,1)S(1)}, u32[]{:S(2)}, u32[]{:S(2)}) collective-permute-start(bf16[4,16,1024]{2,1,0:T(8,128)(2,1)S(1)} %get-tuple-element.32), channel_id=1, source_target_pairs={{0,480},{32,0},{64,32},{96,64},{128,96},{160,128},{192,160},{224,1... | collective-permute-start | bytes 393224 | tf_op jit(solution)/shard_map/ppermute | solution.py:56
  44.6 3.4 %collective-permute-start.4 = (bf16[4,16,1024]{2,1,0:T(8,128)(2,1)S(1)}, bf16[4,16,1024]{2,1,0:T(8,128)(2,1)S(1)}, u32[]{:S(2)}, u32[]{:S(2)}) collective-permute-start(bf16[4,16,1024]{2,1,0:T(8,128)(2,1)S(1)} %get-tuple-element.32), channel_id=1, source_target_pairs={{0,32},{32,64},{64,96},{96,128},{128,160},{160,192},{192,224},{224... | collective-permute-start | bytes 393224 | tf_op jit(solution)/shard_map/ppermute | solution.py:56
  48.0 4.2 %collective-permute-done.6 = bf16[4,16,1024]{2,1,0:T(8,128)(2,1)S(1)} collective-permute-done((bf16[4,16,1024]{2,1,0:T(8,128)(2,1)S(1)}, bf16[4,16,1024]{2,1,0:T(8,128)(2,1)S(1)}, u32[]{:S(2)}, u32[]{:S(2)}) %collective-permute-start.6) | collective-permute-done | bytes 131104 | tf_op jit(solution)/shard_map/ppermute | solution.py:56
  52.2 0.0 collective-permute-done.5
  52.2 0.5 collective-permute-done.4
  52.7 0.9 fusion
  53.6 3.3 %collective-permute-start.9 = (bf16[4,4,16,1024]{3,2,1,0:T(8,128)(2,1)S(1)}, bf16[4,4,16,1024]{3,2,1,0:T(8,128)(2,1)S(1)}, u32[]{:S(2)}, u32[]{:S(2)}) collective-permute-start(bf16[4,4,16,1024]{3,2,1,0:T(8,128)(2,1)S(1)} %get-tuple-element.30), channel_id=1, source_target_pairs={{0,16},{8,24},{16,0},{24,8},{1,17},{9,25},{17,1},{25,9},{2,18},{10... | collective-permute-start | bytes 1572872 | tf_op jit(solution)/shard_map/ppermute | solution.py:56
  56.9 1.9 collective-permute-start.8
  58.8 5.1 %collective-permute-start.7 = (bf16[4,4,16,1024]{3,2,1,0:T(8,128)(2,1)S(1)}, bf16[4,4,16,1024]{3,2,1,0:T(8,128)(2,1)}, u32[]{:S(2)}, u32[]{:S(2)}) collective-permute-start(bf16[4,4,16,1024]{3,2,1,0:T(8,128)(2,1)S(1)} %get-tuple-element.30), channel_id=1, source_target_pairs={{0,8},{8,16},{16,24},{24,0},{1,9},{9,17},{17,25},{25,1},{2,10},{10... | collective-permute-start | bytes 1572872 | tf_op jit(solution)/shard_map/ppermute | solution.py:56
  64.0 0.0 all-to-all-done.1
  64.0 1.1 broadcast_in_dim.21
  65.1 4.5 %all-to-all-start.2 = ((bf16[4,4,4,16,512]{4,3,2,1,0:T(8,128)(2,1)}), bf16[4,4,4,16,512]{4,3,2,1,0:T(8,128)(2,1)S(1)}, u32[]{:S(2)}, u32[]{:S(2)}) async-start(bf16[4,4,4,16,512]{4,3,2,1,0:T(8,128)(2,1)} %broadcast_in_dim.21), calls=%async_computation.2 | async-start | bytes 2097152 | tf_op jit(solution)/shard_map/all_to_all | solution.py:49
  69.6 2.2 collective-permute-done.9
  71.8 0.0 copy-start.2
  71.8 8.7 %collective-permute-done.8 = bf16[4,4,16,1024]{3,2,1,0:T(8,128)(2,1)S(1)} collective-permute-done((bf16[4,4,16,1024]{3,2,1,0:T(8,128)(2,1)S(1)}, bf16[4,4,16,1024]{3,2,1,0:T(8,128)(2,1)S(1)}, u32[]{:S(2)}, u32[]{:S(2)}) %collective-permute-start.8) | collective-permute-done | bytes 524320 | tf_op jit(solution)/shard_map/ppermute | solution.py:56
  80.5 0.0 copy-start.3
  80.5 0.4 collective-permute-done.7
  80.9 0.0 copy-done.2
  80.9 0.4 copy-done.3
  81.3 1.8 pad_maximum_fusion.mine_ref
  83.1 0.0 copy-start
  83.1 1.9 collective-permute-start.10
  85.0 5.5 %all-to-all-done.2.mine_ref = bf16[4,4,4,16,512]{4,3,2,1,0:T(8,128)(2,1)S(1)} async-done(((bf16[4,4,4,16,512]{4,3,2,1,0:T(8,128)(2,1)}), bf16[4,4,4,16,512]{4,3,2,1,0:T(8,128)(2,1)S(1)}, u32[]{:S(2)}, u32[]{:S(2)}) %all-to-all-start.2) | async-done | bytes 1048608 | tf_op jit(solution)/shard_map/all_to_all | solution.py:49
  90.5 0.0 copy-start.1
  90.5 1.9 collective-permute-start.3
  92.5 3.5 %collective-permute-start = (bf16[128,2048]{1,0:T(8,128)(2,1)}, bf16[128,2048]{1,0:T(8,128)(2,1)}, u32[]{:S(2)}, u32[]{:S(2)}) collective-permute-start(bf16[128,2048]{1,0:T(8,128)(2,1)} %own_ref.1), channel_id=1, source_target_pairs={{0,1},{1,2},{2,3},{3,0},{4,5},{5,6},{6,7},{7,4},{8,9},{9,10},{10,1... | collective-permute-start | bytes 1572872 | tf_op jit(solution)/shard_map/ppermute | solution.py:56
  96.0 3.6 %collective-permute-start.1 = (bf16[128,2048]{1,0:T(8,128)(2,1)}, bf16[128,2048]{1,0:T(8,128)(2,1)}, u32[]{:S(2)}, u32[]{:S(2)}) collective-permute-start(bf16[128,2048]{1,0:T(8,128)(2,1)} %own_ref.1), channel_id=1, source_target_pairs={{0,3},{1,0},{2,1},{3,2},{4,7},{5,4},{6,5},{7,6},{8,11},{9,8},{10,9... | collective-permute-start | bytes 1572872 | tf_op jit(solution)/shard_map/ppermute | solution.py:56
  99.5 3.9 %collective-permute-start.2 = (bf16[128,2048]{1,0:T(8,128)(2,1)}, bf16[128,2048]{1,0:T(8,128)(2,1)}, u32[]{:S(2)}, u32[]{:S(2)}) collective-permute-start(bf16[128,2048]{1,0:T(8,128)(2,1)} %own_ref.1), channel_id=1, source_target_pairs={{0,2},{1,3},{2,0},{3,1},{4,6},{5,7},{6,4},{7,5},{8,10},{9,11},{10,... | collective-permute-start | bytes 1572872 | tf_op jit(solution)/shard_map/ppermute | solution.py:56
  103.5 0.6 stack.57.info_ref
  104.1 6.2 %collective-permute-done.before_ref = bf16[128,2048]{1,0:T(8,128)(2,1)} collective-permute-done((bf16[128,2048]{1,0:T(8,128)(2,1)}, bf16[128,2048]{1,0:T(8,128)(2,1)}, u32[]{:S(2)}, u32[]{:S(2)}) %collective-permute-start) | collective-permute-done | bytes 524320 | tf_op jit(solution)/shard_map/ppermute | solution.py:56
  110.3 2.7 %collective-permute-done.1.after_ref = bf16[128,2048]{1,0:T(8,128)(2,1)} collective-permute-done((bf16[128,2048]{1,0:T(8,128)(2,1)}, bf16[128,2048]{1,0:T(8,128)(2,1)}, u32[]{:S(2)}, u32[]{:S(2)}) %collective-permute-start.1) | collective-permute-done | bytes 524320 | tf_op jit(solution)/shard_map/ppermute | solution.py:56
  113.0 9.7 %collective-permute-done.2.far_ref = bf16[128,2048]{1,0:T(8,128)(2,1)} collective-permute-done((bf16[128,2048]{1,0:T(8,128)(2,1)}, bf16[128,2048]{1,0:T(8,128)(2,1)}, u32[]{:S(2)}, u32[]{:S(2)}) %collective-permute-start.2) | collective-permute-done | bytes 524320 | tf_op jit(solution)/shard_map/ppermute | solution.py:56
  122.7 0.0 collective-permute-done.3.other_ref
  122.7 0.0 copy-done.1
  122.7 8.3 %shard_map.109 = (bf16[512,2048]{1,0:T(8,128)(2,1)}, bf16[512,256]{1,0:T(8,128)(2,1)}, f32[512,256]{1,0:T(8,128)}, f32[512,256]{1,0:T(8,128)}, f32[4,128,256]{2,1,0:T(8,128)}, /*index=5*/bf16[8,24,256]{2,1,0:T(8,128)(2,1)}) custom-call(s32[6]{0:T(128)} %stack.57.info_ref, bf16[128,2048]{1,0:T(8,128)(2,1)} %own_ref.1, ...), custom_call_target="tpu_custom_call" | custom-call | flops 1073741824 | bytes 8388608 | tf_op jit(solution)/shard_map/pallas_call | solution.py:346
  131.0 0.0 copy-done
  131.0 8.6 %all_to_all.39.got_ref = bf16[8,24,256]{2,1,0:T(8,128)(2,1)} all-to-all(bf16[8,24,256]{2,1,0:T(8,128)(2,1)} %get-tuple-element.17), channel_id=1, replica_groups=mesh['sp_f'=4,'sp_n'=4,'sp_x'=4,'sp_c'=2,'tp'=4] {'sp_x','sp_c'}, dimensions={0} | all-to-all | bytes 196608 | tf_op jit(solution)/shard_map/all_to_all | solution.py:455
  139.6 1.7 shard_map.110
  141.3 22.8 %all_to_all.40.totals_ref = bf16[16,24,256]{2,1,0:T(8,128)(2,1)} all-to-all(bf16[16,24,256]{2,1,0:T(8,128)(2,1)} %get-tuple-element.18), channel_id=1, replica_groups=mesh['sp_f'=4,'sp_n'=4,'sp_x'=4,'sp_c'=2,'tp'=4] {'sp_f','sp_n'}, dimensions={0} | all-to-all | bytes 393216 | tf_op jit(solution)/shard_map/all_to_all | solution.py:468
  164.1 1.7 shard_map.111
  165.8 5.4 %all-to-all-start.5 = ((bf16[8,16,256]{2,1,0:T(8,128)(2,1)}), bf16[8,16,256]{2,1,0:T(8,128)(2,1)S(1)}, u32[]{:S(2)}, u32[]{:S(2)}) async-start(bf16[8,16,256]{2,1,0:T(8,128)(2,1)} %shard_map.111), calls=%async_computation.5 | async-start | bytes 131072 | tf_op jit(solution)/shard_map/all_to_all | solution.py:480
  171.2 0.0 collective-permute-done.10.other_ref
  171.2 7.7 %shard_map.112 = (bf16[512,256]{1,0:T(8,128)(2,1)}, f32[512,256]{1,0:T(8,128)}, f32[512,256]{1,0:T(8,128)}) custom-call(s32[6]{0:T(128)} %stack.57.info_ref, bf16[512,2048]{1,0:T(8,128)(2,1)} %get-tuple-element.23.normed_ref, bf16[4,4,4,16,1024]{4,3,2,1,0:T(8,128)(2,1)} %copy-done, bf16[4,4,4,16,1024]{4,3,2,1,0:T(8,128)(2,1)} %collective-permute-done.10.other_ref, ...), custom_call_target="tpu_custom_call" | custom-call | flops 1073741824 | bytes 8388608 | tf_op jit(solution)/shard_map/pallas_call | solution.py:346
  178.9 0.7 slice.11
  179.6 2.0 collective-permute-start.11
  181.6 2.9 %collective-permute-done.11.rim_ref = bf16[16,256]{1,0:T(8,128)(2,1)S(1)} collective-permute-done((bf16[16,256]{1,0:T(8,128)(2,1)S(1)}, bf16[16,256]{1,0:T(8,128)(2,1)S(1)}, u32[]{:S(2)}, u32[]{:S(2)}) %collective-permute-start.11) | collective-permute-done | bytes 8224 | tf_op jit(solution)/shard_map/ppermute | solution.py:503
  184.5 0.0 copy-start.5
  184.5 0.0 all-to-all-done.5
  184.5 0.0 copy-start.4
  184.5 0.6 copy-done.5
  185.1 0.0 copy-done.4
  185.2 6.2 %shard_map.113 = bf16[512,2048]{1,0:T(8,128)(2,1)} custom-call(s32[6]{0:T(128)} %stack.57.info_ref, bf16[128,256]{1,0:T(8,128)(2,1)} %bitcast.26, f32[4,128,256]{2,1,0:T(8,128)} %get-tuple-element.21.growth_ref, f32[512,256]{1,0:T(8,128)} %get-tuple-element.22.cum_ref, f32[512,256]{1,0:T(8,128)} %get-tuple-element.26.decayed_ref, ...), custom_call_target="tpu_custom_call" | custom-call | flops 1073741824 | bytes 8388608 | tf_op jit(solution)/shard_map/pallas_call | solution.py:346
  191.3 29.9 %all_to_all.41 = bf16[4,128,2048]{2,1,0:T(8,128)(2,1)S(1)} all-to-all(bf16[4,128,2048]{2,1,0:T(8,128)(2,1)} %bitcast.23), channel_id=1, replica_groups=mesh['sp_f'=4,'sp_n'=4,'sp_x'=4,'sp_c'=2,'tp'=4] {'tp'}, dimensions={0} | all-to-all | bytes 4194304 | tf_op jit(solution)/shard_map/all_to_all | solution.py:522
  221.2 1.3 reduce_sum.12
  (3 shorter events, 0.0 us)
Async XLA Ops:
  33.4 30.6 %all-to-all-start.1 = ((bf16[4,4,16,512]{3,2,1,0:T(8,128)(2,1)}), bf16[4,4,16,512]{3,2,1,0:T(8,128)(2,1)S(1)}, u32[]{:S(2)}, u32[]{:S(2)}) async-start(bf16[4,4,16,512]{3,2,1,0:T(8,128)(2,1)} %broadcast_in_dim.20), calls=%async_computation.1 | async-start | bytes 524288 | tf_op jit(solution)/shard_map/all_to_all | solution.py:49
  38.0 14.2 %collective-permute-start.6 = (bf16[4,16,1024]{2,1,0:T(8,128)(2,1)S(1)}, bf16[4,16,1024]{2,1,0:T(8,128)(2,1)S(1)}, u32[]{:S(2)}, u32[]{:S(2)}) collective-permute-start(bf16[4,16,1024]{2,1,0:T(8,128)(2,1)S(1)} %get-tuple-element.32), channel_id=1, source_target_pairs={{0,448},{32,480},{64,0},{96,32},{128,64},{160,96},{192,128},{224,1... | collective-permute-start | bytes 393224 | tf_op jit(solution)/shard_map/ppermute | solution.py:56
  42.2 10.1 %collective-permute-start.5 = (bf16[4,16,1024]{2,1,0:T(8,128)(2,1)S(1)}, bf16[4,16,1024]{2,1,0:T(8,128)(2,1)S(1)}, u32[]{:S(2)}, u32[]{:S(2)}) collective-permute-start(bf16[4,16,1024]{2,1,0:T(8,128)(2,1)S(1)} %get-tuple-element.32), channel_id=1, source_target_pairs={{0,480},{32,0},{64,32},{96,64},{128,96},{160,128},{192,160},{224,1... | collective-permute-start | bytes 393224 | tf_op jit(solution)/shard_map/ppermute | solution.py:56
  44.6 8.1 %collective-permute-start.4 = (bf16[4,16,1024]{2,1,0:T(8,128)(2,1)S(1)}, bf16[4,16,1024]{2,1,0:T(8,128)(2,1)S(1)}, u32[]{:S(2)}, u32[]{:S(2)}) collective-permute-start(bf16[4,16,1024]{2,1,0:T(8,128)(2,1)S(1)} %get-tuple-element.32), channel_id=1, source_target_pairs={{0,32},{32,64},{64,96},{96,128},{128,160},{160,192},{192,224},{224... | collective-permute-start | bytes 393224 | tf_op jit(solution)/shard_map/ppermute | solution.py:56
  53.6 18.2 %collective-permute-start.9 = (bf16[4,4,16,1024]{3,2,1,0:T(8,128)(2,1)S(1)}, bf16[4,4,16,1024]{3,2,1,0:T(8,128)(2,1)S(1)}, u32[]{:S(2)}, u32[]{:S(2)}) collective-permute-start(bf16[4,4,16,1024]{3,2,1,0:T(8,128)(2,1)S(1)} %get-tuple-element.30), channel_id=1, source_target_pairs={{0,16},{8,24},{16,0},{24,8},{1,17},{9,25},{17,1},{25,9},{2,18},{10... | collective-permute-start | bytes 1572872 | tf_op jit(solution)/shard_map/ppermute | solution.py:56
  56.9 23.6 %collective-permute-start.8 = (bf16[4,4,16,1024]{3,2,1,0:T(8,128)(2,1)S(1)}, bf16[4,4,16,1024]{3,2,1,0:T(8,128)(2,1)S(1)}, u32[]{:S(2)}, u32[]{:S(2)}) collective-permute-start(bf16[4,4,16,1024]{3,2,1,0:T(8,128)(2,1)S(1)} %get-tuple-element.30), channel_id=1, source_target_pairs={{0,24},{8,0},{16,8},{24,16},{1,25},{9,1},{17,9},{25,17},{2,26},{10... | collective-permute-start | bytes 1572872 | tf_op jit(solution)/shard_map/ppermute | solution.py:56
  58.8 22.1 %collective-permute-start.7 = (bf16[4,4,16,1024]{3,2,1,0:T(8,128)(2,1)S(1)}, bf16[4,4,16,1024]{3,2,1,0:T(8,128)(2,1)}, u32[]{:S(2)}, u32[]{:S(2)}) collective-permute-start(bf16[4,4,16,1024]{3,2,1,0:T(8,128)(2,1)S(1)} %get-tuple-element.30), channel_id=1, source_target_pairs={{0,8},{8,16},{16,24},{24,0},{1,9},{9,17},{17,25},{25,1},{2,10},{10... | collective-permute-start | bytes 1572872 | tf_op jit(solution)/shard_map/ppermute | solution.py:56
  65.1 25.4 %all-to-all-start.2 = ((bf16[4,4,4,16,512]{4,3,2,1,0:T(8,128)(2,1)}), bf16[4,4,4,16,512]{4,3,2,1,0:T(8,128)(2,1)S(1)}, u32[]{:S(2)}, u32[]{:S(2)}) async-start(bf16[4,4,4,16,512]{4,3,2,1,0:T(8,128)(2,1)} %broadcast_in_dim.21), calls=%async_computation.2 | async-start | bytes 2097152 | tf_op jit(solution)/shard_map/all_to_all | solution.py:49
  71.8 9.1 %copy-start.2 = (bf16[4,4,16,1024]{3,2,1,0:T(8,128)(2,1)}, bf16[4,4,16,1024]{3,2,1,0:T(8,128)(2,1)S(1)}, u32[]{:S(2)}) copy-start(bf16[4,4,16,1024]{3,2,1,0:T(8,128)(2,1)S(1)} %collective-permute-done.9) | copy-start | bytes 1572868
  80.5 0.8 copy-start.3
  83.1 47.9 %copy-start = (bf16[4,4,4,16,1024]{4,3,2,1,0:T(8,128)(2,1)}, bf16[4,4,4,16,1024]{4,3,2,1,0:T(8,128)(2,1)S(1)}, u32[]{:S(2)}) copy-start(bf16[4,4,4,16,1024]{4,3,2,1,0:T(8,128)(2,1)S(1)} %pad_maximum_fusion.mine_ref) | copy-start | bytes 6291460
  83.1 88.1 %collective-permute-start.10 = (bf16[4,4,4,16,1024]{4,3,2,1,0:T(8,128)(2,1)S(1)}, bf16[4,4,4,16,1024]{4,3,2,1,0:T(8,128)(2,1)}, u32[]{:S(2)}, u32[]{:S(2)}) collective-permute-start(bf16[4,4,4,16,1024]{4,3,2,1,0:T(8,128)(2,1)S(1)} %pad_maximum_fusion.mine_ref), channel_id=1, source_target_pairs={{0,4},{4,0},{1,5},{5,1},{2,6},{6,2},{3,7},{7,3},{8,12},{12,8},{9,1... | collective-permute-start | bytes 6291464 | tf_op jit(solution)/shard_map/ppermute | solution.py:371
  90.5 32.2 %copy-start.1 = (bf16[4,4,4,16,512]{4,3,2,1,0:T(8,128)(2,1)}, bf16[4,4,4,16,512]{4,3,2,1,0:T(8,128)(2,1)S(1)}, u32[]{:S(2)}) copy-start(bf16[4,4,4,16,512]{4,3,2,1,0:T(8,128)(2,1)S(1)} %all-to-all-done.2.mine_ref) | copy-start | bytes 3145732
  90.5 32.1 %collective-permute-start.3 = (bf16[4,4,4,16,512]{4,3,2,1,0:T(8,128)(2,1)S(1)}, bf16[4,4,4,16,512]{4,3,2,1,0:T(8,128)(2,1)}, u32[]{:S(2)}, u32[]{:S(2)}) collective-permute-start(bf16[4,4,4,16,512]{4,3,2,1,0:T(8,128)(2,1)S(1)} %all-to-all-done.2.mine_ref), channel_id=1, source_target_pairs={{0,4},{4,0},{1,5},{5,1},{2,6},{6,2},{3,7},{7,3},{8,12},{12,8},{9,1... | collective-permute-start | bytes 3145736 | tf_op jit(solution)/shard_map/ppermute | solution.py:371
  92.5 17.8 %collective-permute-start = (bf16[128,2048]{1,0:T(8,128)(2,1)}, bf16[128,2048]{1,0:T(8,128)(2,1)}, u32[]{:S(2)}, u32[]{:S(2)}) collective-permute-start(bf16[128,2048]{1,0:T(8,128)(2,1)} %own_ref.1), channel_id=1, source_target_pairs={{0,1},{1,2},{2,3},{3,0},{4,5},{5,6},{6,7},{7,4},{8,9},{9,10},{10,1... | collective-permute-start | bytes 1572872 | tf_op jit(solution)/shard_map/ppermute | solution.py:56
  96.0 17.0 %collective-permute-start.1 = (bf16[128,2048]{1,0:T(8,128)(2,1)}, bf16[128,2048]{1,0:T(8,128)(2,1)}, u32[]{:S(2)}, u32[]{:S(2)}) collective-permute-start(bf16[128,2048]{1,0:T(8,128)(2,1)} %own_ref.1), channel_id=1, source_target_pairs={{0,3},{1,0},{2,1},{3,2},{4,7},{5,4},{6,5},{7,6},{8,11},{9,8},{10,9... | collective-permute-start | bytes 1572872 | tf_op jit(solution)/shard_map/ppermute | solution.py:56
  99.5 23.2 %collective-permute-start.2 = (bf16[128,2048]{1,0:T(8,128)(2,1)}, bf16[128,2048]{1,0:T(8,128)(2,1)}, u32[]{:S(2)}, u32[]{:S(2)}) collective-permute-start(bf16[128,2048]{1,0:T(8,128)(2,1)} %own_ref.1), channel_id=1, source_target_pairs={{0,2},{1,3},{2,0},{3,1},{4,6},{5,7},{6,4},{7,5},{8,10},{9,11},{10,... | collective-permute-start | bytes 1572872 | tf_op jit(solution)/shard_map/ppermute | solution.py:56
  165.8 18.7 %all-to-all-start.5 = ((bf16[8,16,256]{2,1,0:T(8,128)(2,1)}), bf16[8,16,256]{2,1,0:T(8,128)(2,1)S(1)}, u32[]{:S(2)}, u32[]{:S(2)}) async-start(bf16[8,16,256]{2,1,0:T(8,128)(2,1)} %shard_map.111), calls=%async_computation.5 | async-start | bytes 131072 | tf_op jit(solution)/shard_map/all_to_all | solution.py:480
  179.6 5.0 %collective-permute-start.11 = (bf16[16,256]{1,0:T(8,128)(2,1)S(1)}, bf16[16,256]{1,0:T(8,128)(2,1)S(1)}, u32[]{:S(2)}, u32[]{:S(2)}) collective-permute-start(bf16[16,256]{1,0:T(8,128)(2,1)S(1)} %slice.11), channel_id=1, source_target_pairs={{0,4},{4,8},{8,12},{12,16},{16,20},{20,24},{24,28},{28,32},{32,36}... | collective-permute-start | bytes 24584 | tf_op jit(solution)/shard_map/ppermute | solution.py:503
  184.5 0.6 copy-start.5
  184.5 0.6 copy-start.4
